TPU v7x, 128 devices: a whole 4x4x4 slice. The times are simulated.
128 devices in a mesh: ep: 32 (over z, y, core), tp: 4 (over x).
Axes of the slice: x: 4, y: 4, z: 4, core: 2. Of those that a mesh axis runs over, the one named last changes fastest.
Arguments:
- tokens: bfloat16 [16384, 2048], P(('ep', 'tp')), may hold values from -6 to 6
- norm_gain: float32 [2048], replicated, may hold values from 0.1 to 1.9
- expert_ids: int32 [16384, 2], P('ep'), may hold values from 0 to 31, all different within a row; in each aligned block of 128 rows (0 to 127, 128 to 255, ...) at most 10 rows name the same one
- route_weight: float32 [16384, 2], P('ep'), may hold values from 0.1 to 1
- exp_gate: bfloat16 [32, 2048, 7168], P('ep', None, 'tp'), may hold values from -0.125 to 0.125
- exp_up: bfloat16 [32, 2048, 7168], P('ep', None, 'tp'), may hold values from -0.125 to 0.125
- exp_down: bfloat16 [32, 7168, 2048], P('ep', 'tp'), may hold values from -0.0625 to 0.0625
Outputs:
- mixed: bfloat16 [16384, 2048], P(('ep', 'tp'))
Inputs may be any that keep to these rules, and one draw needn't show every extreme that they name: `expert_ids`: A row names 2 different experts. Within each aligned block of 128 rows (the tokens of one device) no expert is named by more than 10 rows, and in some block one expert is named by exactly 10 rows.
All inputs are finite; a program needn't handle non-finite values.
Results may differ from a plain program's by a relative error of at most 0.012.
Values may be sent and summed in bfloat16 or wider, within the bound.
No kernel may reach another device: no remote copies, remote signals or barrier semaphores. Data moves between devices by JAX's collectives and lax.ppermute only.
A program may use at most 128 MiB of HBM per device.

v0:
```python
import functools

import jax
import jax.numpy as jnp
from jax import lax
from jax.experimental import pallas as pl
from jax.experimental.pallas import tpu as pltpu
from jax.sharding import Mesh
from jax.sharding import PartitionSpec as P


EP = ("ep_0", "ep_1", "ep_2")
EP_TP = ("ep_0", "ep_1", "ep_2", "tp")
CAP = 10
EARLY = 8
LATE = CAP - EARLY
OFFSETS = (0, -1, 1, 2)
UP_TILE = 256
DOWN_TILE = 1024
MIB = 2**20


norm_eps = 1e-05
VMEM_SPEC = pl.BlockSpec(memory_space=pltpu.VMEM)
HBM_SPEC = pl.BlockSpec(memory_space=pltpu.HBM)


def normalize(tokens, norm_gain):
    values = tokens.astype(jnp.float32)
    factor = lax.rsqrt(jnp.mean(values * values, axis=-1, keepdims=True) + norm_eps)
    return (values * factor * norm_gain).astype(jnp.bfloat16)


def shift(value, by):
    size = lax.axis_size("tp")
    return lax.ppermute(value, "tp", [(i, (i + by) % size) for i in range(size)])


def exchange(rows):
    ep_size = lax.axis_size(EP)
    tiles = rows.reshape(ep_size, rows.shape[0] // ep_size, rows.shape[1])
    return lax.all_to_all(tiles, EP, 0, 0, tiled=True).reshape(rows.shape)


def gather_tp(rows):
    half = rows.shape[0] // 2
    from_left = shift(rows, 1)
    from_right = shift(rows, -1)
    far_a = shift(from_left[:half], 1)
    far_b = shift(from_right[half:], -1)
    return rows, from_left, from_right, far_a, far_b


def add_rounded(a, b):
    return (a.astype(jnp.float32) + b.astype(jnp.float32)).astype(jnp.bfloat16)


def place(target, blocks):
    at = 0
    for b in blocks:
        target[at : at + b.shape[0], :] = b[...]
        at += b.shape[0]


def cut(value, outs, columns=slice(None)):
    at = 0
    for o in outs:
        o[:, columns] = value[at : at + o.shape[0]].astype(o.dtype)
        at += o.shape[0]


def expert_rows(rows, hidden, gates, ups, up_tiles, down_tile, outs):
    steps, downs = hidden.shape[1] // UP_TILE, outs[0].shape[1] // DOWN_TILE

    def cols(t, width):
        return pl.ds(pl.multiple_of(t * width, width), width)

    def multiply(t):
        w_gate, w_up = up_tiles(t)
        gate = jnp.dot(rows[...], w_gate[...], preferred_element_type=jnp.float32)
        up = jnp.dot(rows[...], w_up[...], preferred_element_type=jnp.float32)
        return gate, up

    def activate(t):
        gate, up = gates[t % 2], ups[t % 2]
        value = (gate / (1.0 + jnp.exp(-gate)) * up).astype(jnp.bfloat16)
        hidden[:, cols(t, UP_TILE)] = value

    def up_step(t, c):
        gate, up = multiply(t)
        activate(t - 1)
        gates[t % 2] = gate
        ups[t % 2] = up
        return c

    gates[0], ups[0] = multiply(0)
    lax.fori_loop(1, steps, up_step, 0)
    activate(steps - 1)

    def down_step(t, c):
        part = jnp.dot(hidden[...], down_tile(t)[...], preferred_element_type=jnp.float32)
        cut(part, outs, cols(t, DOWN_TILE))
        return c

    lax.fori_loop(0, downs, down_step, 0)


def stream_kernel(block, w_gate, w_up, w_down, out, gate_tiles, up_tiles, down_tiles, *scratch):
    rows, hidden, gates, ups, sems = scratch

    def load(kind, t):
        src, dst = ((w_gate, gate_tiles), (w_up, up_tiles), (w_down, down_tiles))[kind]
        width = dst.shape[2]
        at = pl.ds(pl.multiple_of(t * width, width), width)
        return pltpu.make_async_copy(src.at[0, :, at], dst.at[t], sems.at[kind, t])

    def start_up(t, c):
        load(0, t).start()
        load(1, t).start()
        return c

    def start_down(t, c):
        load(2, t).start()
        return c

    lax.fori_loop(0, gate_tiles.shape[0], start_up, 0)
    lax.fori_loop(0, down_tiles.shape[0], start_down, 0)
    place(rows, [block])

    def up_tiles_of(t):
        load(0, t).wait()
        load(1, t).wait()
        return gate_tiles.at[t], up_tiles.at[t]

    def down_tile_of(t):
        load(2, t).wait()
        return down_tiles.at[t]

    expert_rows(rows, hidden, gates, ups, up_tiles_of, down_tile_of, [out])


def kept_kernel(n_in, *refs):
    blocks = refs[:n_in]
    gate_tiles, up_tiles, down_tiles = refs[n_in : n_in + 3]
    outs = refs[n_in + 3 : -4]
    rows, hidden, gates, ups = refs[-4:]
    place(rows, blocks)
    expert_rows(
        rows,
        hidden,
        gates,
        ups,
        lambda t: (gate_tiles.at[t], up_tiles.at[t]),
        lambda t: down_tiles.at[t],
        outs,
    )


def expert_cost(m, d, ff, weights):
    return pl.CostEstimate(
        flops=6 * m * d * ff, bytes_accessed=6 * d * ff * weights + 4 * m * d, transcendentals=m * ff
    )


def row_buffers(m, d, ff):
    return [
        pltpu.VMEM((m, d), jnp.bfloat16),
        pltpu.VMEM((m, ff), jnp.bfloat16),
        pltpu.VMEM((2, m, UP_TILE), jnp.float32),
        pltpu.VMEM((2, m, UP_TILE), jnp.float32),
    ]


def expert_streamed(rows, weights, keep):
    d, ff = weights[0].shape[1:]
    m = rows.shape[0]
    steps, downs = ff // UP_TILE, d // DOWN_TILE
    tiles = [
        pltpu.VMEM((steps, d, UP_TILE), jnp.bfloat16),
        pltpu.VMEM((steps, d, UP_TILE), jnp.bfloat16),
        pltpu.VMEM((downs, ff, DOWN_TILE), jnp.bfloat16),
    ]
    return pl.pallas_call(
        stream_kernel,
        in_specs=[VMEM_SPEC] + [HBM_SPEC] * 3,
        out_specs=[VMEM_SPEC] * (4 if keep else 1),
        out_shape=[jax.ShapeDtypeStruct((m, d), jnp.bfloat16)] + (tiles if keep else []),
        scratch_shapes=([] if keep else tiles)
        + row_buffers(m, d, ff)
        + [pltpu.SemaphoreType.DMA((3, max(steps, downs)))],
        compiler_params=pltpu.CompilerParams(vmem_limit_bytes=(12 if keep else 34) * MIB),
        cost_estimate=expert_cost(m, d, ff, 1),
    )(rows, *(pltpu.with_memory_space_constraint(w, pltpu.HBM) for w in weights))


def expert_kept(blocks, sizes, tiles):
    steps, d = tiles[0].shape[:2]
    ff = steps * UP_TILE
    m = sum(b.shape[0] for b in blocks)
    return pl.pallas_call(
        functools.partial(kept_kernel, len(blocks)),
        in_specs=[VMEM_SPEC] * (len(blocks) + 3),
        out_specs=[VMEM_SPEC] * len(sizes),
        out_shape=[jax.ShapeDtypeStruct((s, d), jnp.bfloat16) for s in sizes],
        scratch_shapes=row_buffers(m, d, ff),
        compiler_params=pltpu.CompilerParams(vmem_limit_bytes=12 * MIB),
        cost_estimate=expert_cost(m, d, ff, 0),
    )(*blocks, *(pltpu.with_memory_space_constraint(w, pltpu.VMEM) for w in tiles))


def select_kernel(chosen, *refs):
    blocks, out, rows = refs[:-2], refs[-2], refs[-1]
    place(rows, blocks)
    out[...] = jnp.dot(chosen[...], rows[...], preferred_element_type=jnp.float32).astype(out.dtype)


def select_rows(chosen, blocks):
    d = blocks[0].shape[1]
    n, m = chosen.shape
    return pl.pallas_call(
        select_kernel,
        in_specs=[VMEM_SPEC] * (1 + len(blocks)),
        out_specs=VMEM_SPEC,
        out_shape=jax.ShapeDtypeStruct((n, d), jnp.bfloat16),
        scratch_shapes=[pltpu.VMEM((m, d), jnp.bfloat16)],
        compiler_params=pltpu.CompilerParams(vmem_limit_bytes=16 * MIB),
        cost_estimate=pl.CostEstimate(
            flops=2 * n * m * d, bytes_accessed=2 * d * (n + m), transcendentals=0
        ),
    )(chosen, *blocks)


def weigh_kernel(high, low, rows, *outs):
    value = jnp.dot(high[...], rows[...], preferred_element_type=jnp.float32)
    value = value + jnp.dot(low[...], rows[...], preferred_element_type=jnp.float32)
    cut(value, outs)


def weigh_rows(weights, rows, sizes):
    n, m = weights.shape
    d = rows.shape[1]
    high = weights.astype(jnp.bfloat16)
    low = (weights - high.astype(jnp.float32)).astype(jnp.bfloat16)
    return pl.pallas_call(
        weigh_kernel,
        in_specs=[VMEM_SPEC] * 3,
        out_specs=[VMEM_SPEC] * len(sizes),
        out_shape=[jax.ShapeDtypeStruct((s, d), jnp.bfloat16) for s in sizes],
        compiler_params=pltpu.CompilerParams(vmem_limit_bytes=24 * MIB),
        cost_estimate=pl.CostEstimate(
            flops=4 * n * m * d, bytes_accessed=2 * d * (n + m), transcendentals=0
        ),
    )(high, low, rows)


def finish_kernel(high, low, rows, own, near_a, near_b, far_a, far_b, out):
    value = jnp.dot(high[...], rows[...], preferred_element_type=jnp.float32)
    value = value + jnp.dot(low[...], rows[...], preferred_element_type=jnp.float32)
    value = value + own[...].astype(jnp.float32)
    half = out.shape[0] // 2
    top = near_a[...].astype(jnp.float32) + far_a[...].astype(jnp.float32)
    bottom = near_b[...].astype(jnp.float32) + far_b[...].astype(jnp.float32)
    out[:half, :] = (value[:half] + top).astype(out.dtype)
    out[half:, :] = (value[half:] + bottom).astype(out.dtype)


def finish(weights, rows, own, pieces):
    n, m = weights.shape
    d = rows.shape[1]
    high = weights.astype(jnp.bfloat16)
    low = (weights - high.astype(jnp.float32)).astype(jnp.bfloat16)
    return pl.pallas_call(
        finish_kernel,
        in_specs=[VMEM_SPEC] * 8,
        out_specs=VMEM_SPEC,
        out_shape=jax.ShapeDtypeStruct((n, d), jnp.bfloat16),
        compiler_params=pltpu.CompilerParams(vmem_limit_bytes=16 * MIB),
        cost_estimate=pl.CostEstimate(
            flops=4 * n * m * d, bytes_accessed=2 * d * (n + m), transcendentals=0
        ),
    )(high, low, rows, own, *pieces)


def send_near(to_left, to_right):
    got_bottom = shift(to_left, -1)
    got_top = shift(to_right, 1)
    return got_top, got_bottom


def send_far(far_top, far_bottom):
    return shift(far_top, -1), shift(far_bottom, 1)


def send_on(to_left, to_right, via_right, via_left):
    got_top = shift(add_rounded(to_left, via_right), -1)
    got_bottom = shift(add_rounded(to_right, via_left), 1)
    return got_top, got_bottom


def per_device(tokens, norm_gain, expert_ids, route_weight, exp_gate, exp_up, exp_down):
    experts_all = lax.axis_size(EP)
    tok_count, _ = tokens.shape
    half = tok_count // 2
    me = lax.axis_index("tp")
    size = lax.axis_size("tp")

    def block_of(value, by):
        return lax.dynamic_slice_in_dim(value, ((me + by + size) % size) * tok_count, tok_count, 0)

    def slots_of(ids):
        hits = ids.T[:, None, :] == jnp.arange(experts_all, dtype=jnp.int32)[:, None]
        named = jnp.any(hits, axis=0)
        at = jnp.arange(tok_count, dtype=jnp.int32)
        earlier = (at[:, None] < at[None, :]).astype(jnp.bfloat16)
        rank = jnp.dot(named.astype(jnp.bfloat16), earlier, preferred_element_type=jnp.float32)
        return jnp.where(named, rank.astype(jnp.int32), -1), hits

    own_ids = block_of(expert_ids, 0)
    own_slot, _ = slots_of(own_ids)
    normed = normalize(tokens, norm_gain)
    early = own_slot[:, None, :] == jnp.arange(EARLY, dtype=jnp.int32)[:, None]
    chosen = early.astype(jnp.bfloat16).reshape(experts_all * EARLY, tok_count)
    sent = jnp.dot(chosen, normed, preferred_element_type=jnp.float32).astype(jnp.bfloat16)
    arrived = exchange(sent)
    blocks = gather_tp(normed)
    arrived, blocks = lax.optimization_barrier((arrived, blocks))

    masks, masses = [], []
    for at, by in enumerate(OFFSETS):
        ids, weight = block_of(expert_ids, by), block_of(route_weight, by)
        slot, hits = slots_of(ids)
        masses.append(jnp.sum(jnp.where(hits, weight.T[:, None, :], 0.0), axis=0))
        wanted = jnp.full((len(OFFSETS), LATE), -2, jnp.int32)
        wanted = wanted.at[at].set(EARLY + jnp.arange(LATE, dtype=jnp.int32)).reshape(-1)
        masks.append(slot[:, None, :] == wanted[:, None])
    late = jnp.concatenate(masks, axis=2)
    late_rows = experts_all * len(OFFSETS) * LATE
    late_mass = jnp.where(late, jnp.concatenate(masses, axis=1)[:, None, :], 0.0)
    late_mass = late_mass.reshape(late_rows, len(OFFSETS) * tok_count)
    early_mass = jnp.where(early, masses[0][:, None, :], 0.0).reshape(experts_all * EARLY, tok_count)
    late_chosen = late.astype(jnp.bfloat16).reshape(late_rows, len(OFFSETS) * tok_count)
    late_arrived = exchange(select_rows(late_chosen, blocks))

    mid = arrived.shape[0] // 2
    top, bottom = arrived[:mid], arrived[mid:]
    left_top, right_bottom = shift(top, 1), shift(bottom, -1)
    left_bottom, right_top = shift(bottom, 1), shift(top, -1)
    far_top, far_bottom = shift(left_top, 1), shift(right_bottom, -1)
    weights = (exp_gate, exp_up, exp_down)
    own_part, *tiles = expert_streamed(arrived, weights, True)
    left_top, right_bottom, own_part = lax.optimization_barrier((left_top, right_bottom, own_part))
    first = expert_kept([left_top, right_bottom], [mid] * 2, tiles)
    left_bottom, right_top, first = lax.optimization_barrier((left_bottom, right_top, first))
    second = expert_kept([left_bottom, right_top], [mid] * 2, tiles)
    near = send_near(*second)
    far_top, far_bottom, first = lax.optimization_barrier((far_top, far_bottom, first))
    third = expert_kept([far_top, far_bottom], [mid] * 2, tiles)
    via = send_far(*third)
    late_arrived, _ = lax.optimization_barrier((late_arrived, third))
    (late_part,) = expert_streamed(late_arrived, weights, False)
    late_back = exchange(late_part)
    on = send_on(*first, *via)
    summed = jnp.concatenate(near, axis=0).astype(jnp.float32)
    summed = summed + jnp.concatenate(on, axis=0).astype(jnp.float32)
    summed = (summed + own_part.astype(jnp.float32)).astype(jnp.bfloat16)
    back = exchange(summed)

    late_back, _ = lax.optimization_barrier((late_back, summed))
    sums = weigh_rows(late_mass.T, late_back, [tok_count] + [half] * 6)
    token_own, left_top, left_bottom, right_top, right_bottom, far_top, far_bottom = sums
    token_via = send_far(far_top, far_bottom)
    token_near = send_near(left_bottom, right_top)
    token_on = send_on(left_top, right_bottom, *token_via)
    return finish(early_mass.T, back, token_own, token_near + token_on)


def solution(mesh):
    finer = Mesh(mesh.devices.reshape(4, 4, 2, mesh.shape["tp"]), ("ep_0", "ep_1", "ep_2", "tp"))
    return jax.shard_map(
        per_device,
        mesh=finer,
        in_specs=(
            P(EP_TP, None),
            P(),
            P(EP, None),
            P(EP, None),
            P(EP, None, "tp"),
            P(EP, None, "tp"),
            P(EP, "tp", None),
        ),
        out_specs=P(EP_TP, None),
        check_vma=False,
    )
```

profile of v0, /device:TPU:0, one launch (start us, length us, event | category | flops | bytes accessed | tf_op | source)
XLA Modules:
  0.0 176.1 jit_solution(16557096132247329592)
XLA Ops:
  2.5 2.9 %collective-permute-start.1 = (bf16[128,2048]{1,0:T(8,128)(2,1)S(1)}, bf16[128,2048]{1,0:T(8,128)(2,1)S(1)}, u32[]{:S(2)}, u32[]{:S(2)}) collective-permute-start(bf16[128,2048]{1,0:T(8,128)(2,1)S(1)} %fusion.7.refs_0_), channel_id=1, source_target_pairs={{0,3},{1,0},{2,1},{3,2},{4,7},{5,4},{6,5},{7,6},{8,11},{9,8},{10,9... | collective-permute-start | bytes 1572872 | tf_op jit(solution)/shard_map/ppermute | solution.py:36
  8.6 1.5 fusion
  10.0 8.3 %all-to-all-start = ((bf16[32,8,2048]{2,1,0:T(8,128)(2,1)}), bf16[32,8,2048]{2,1,0:T(8,128)(2,1)S(1)}, u32[]{:S(2)}, u32[]{:S(2)}) async-start(bf16[32,8,2048]{2,1,0:T(8,128)(2,1)} %fusion), calls=%async_computation | async-start | bytes 2097152 | tf_op jit(solution)/shard_map/all_to_all | solution.py:42
  20.8 3.2 %collective-permute-start.3 = (bf16[64,2048]{1,0:T(8,128)(2,1)}, bf16[64,2048]{1,0:T(8,128)(2,1)S(1)}, u32[]{:S(2)}, u32[]{:S(2)}) collective-permute-start(bf16[64,2048]{1,0:T(8,128)(2,1)} %slice.73), channel_id=1, source_target_pairs={{0,3},{1,0},{2,1},{3,2},{4,7},{5,4},{6,5},{7,6},{8,11},{9,8},{10,9... | collective-permute-start | bytes 786440 | tf_op jit(solution)/shard_map/ppermute | solution.py:36
  28.7 1.7 collective-permute-done.3.refs_4_
  30.4 4.0 %collective-permute-done.2.refs_3_ = bf16[64,2048]{1,0:T(8,128)(2,1)S(1)} collective-permute-done((bf16[64,2048]{1,0:T(8,128)(2,1)}, bf16[64,2048]{1,0:T(8,128)(2,1)S(1)}, u32[]{:S(2)}, u32[]{:S(2)}) %collective-permute-start.2) | collective-permute-done | bytes 262176 | tf_op jit(solution)/shard_map/ppermute | solution.py:36
  36.6 3.2 %collective-permute-start.7 = (bf16[128,2048]{1,0:T(8,128)(2,1)}, bf16[128,2048]{1,0:T(8,128)(2,1)}, u32[]{:S(2)}, u32[]{:S(2)}) collective-permute-start(bf16[128,2048]{1,0:T(8,128)(2,1)} %get-tuple-element.127), channel_id=1, source_target_pairs={{0,3},{1,0},{2,1},{3,2},{4,7},{5,4},{6,5},{7,6},{8,11},{9,8},{10,9... | collective-permute-start | bytes 1572872 | tf_op jit(solution)/shard_map/ppermute | solution.py:36
  39.9 3.3 %collective-permute-start.5 = (bf16[128,2048]{1,0:T(8,128)(2,1)}, bf16[128,2048]{1,0:T(8,128)(2,1)}, u32[]{:S(2)}, u32[]{:S(2)}) collective-permute-start(bf16[128,2048]{1,0:T(8,128)(2,1)} %get-tuple-element.128), channel_id=1, source_target_pairs={{0,3},{1,0},{2,1},{3,2},{4,7},{5,4},{6,5},{7,6},{8,11},{9,8},{10,9... | collective-permute-start | bytes 1572872 | tf_op jit(solution)/shard_map/ppermute | solution.py:36
  43.1 1.7 shard_map.77
  44.8 4.8 %all-to-all-start.2 = ((bf16[32,8,2048]{2,1,0:T(8,128)(2,1)}), bf16[32,8,2048]{2,1,0:T(8,128)(2,1)S(1)}, u32[]{:S(2)}, u32[]{:S(2)}) async-start(bf16[32,8,2048]{2,1,0:T(8,128)(2,1)} %bitcast.20), calls=%async_computation.2 | async-start | bytes 2097152 | tf_op jit(solution)/shard_map/all_to_all | solution.py:42
  49.6 9.1 %shard_map.73 = (bf16[256,2048]{1,0:T(8,128)(2,1)S(1)}, bf16[7,2048,256]{2,1,0:T(8,128)(2,1)S(1)}, bf16[7,2048,256]{2,1,0:T(8,128)(2,1)S(1)}, bf16[2,1792,1024]{2,1,0:T(8,128)(2,1)S(1)}) custom-call(bf16[256,2048]{1,0:T(8,128)(2,1)S(1)} %bitcast.58, bf16[1,2048,1792]{2,1,0:T(8,128)(2,1)} %w_gate.3, bf16[1,2048,1792]{2,1,0:T(8,128)(2,1)} %w_up.3, ...), custom_call_target="tpu_custom_call" | custom-call | flops 5637144576 | bytes 24117248 | tf_op jit(solution)/shard_map/pallas_call | solution.py:183
  58.8 7.5 %collective-permute-done.6.refs_0_ = bf16[128,2048]{1,0:T(8,128)(2,1)} collective-permute-done((bf16[128,2048]{1,0:T(8,128)(2,1)}, bf16[128,2048]{1,0:T(8,128)(2,1)}, u32[]{:S(2)}, u32[]{:S(2)}) %collective-permute-start.6) | collective-permute-done | bytes 524320 | tf_op jit(solution)/shard_map/ppermute | solution.py:36
  66.3 8.5 %shard_map.74 = (bf16[128,2048]{1,0:T(8,128)(2,1)S(1)}, bf16[128,2048]{1,0:T(8,128)(2,1)S(1)}) custom-call(bf16[128,2048]{1,0:T(8,128)(2,1)} %collective-permute-done.6.refs_0_, bf16[128,2048]{1,0:T(8,128)(2,1)} %collective-permute-done.7.refs_1_, bf16[7,2048,256]{2,1,0:T(8,128)(2,1)S(1)} %get-tuple-element.93.refs_2_, ...), custom_call_target="tpu_custom_call" | custom-call | flops 5637144576 | bytes 2097152 | tf_op jit(solution)/shard_map/pallas_call | solution.py:200
  76.4 2.0 %collective-permute-start.10 = (bf16[128,2048]{1,0:T(8,128)(2,1)}, bf16[128,2048]{1,0:T(8,128)(2,1)S(1)}, u32[]{:S(2)}, u32[]{:S(2)}) collective-permute-start(bf16[128,2048]{1,0:T(8,128)(2,1)} %collective-permute-done.6.refs_0_), channel_id=1, source_target_pairs={{0,1},{1,2},{2,3},{3,0},{4,5},{5,6},{6,7},{7,4},{8,9},{9,10},{10,1... | collective-permute-start | bytes 1572872 | tf_op jit(solution)/shard_map/ppermute | solution.py:36
  78.4 9.4 %shard_map.75 = (bf16[128,2048]{1,0:T(8,128)(2,1)}, bf16[128,2048]{1,0:T(8,128)(2,1)}) custom-call(bf16[128,2048]{1,0:T(8,128)(2,1)} %collective-permute-done.4.refs_0_, bf16[128,2048]{1,0:T(8,128)(2,1)} %collective-permute-done.5.refs_1_, bf16[7,2048,256]{2,1,0:T(8,128)(2,1)S(1)} %get-tuple-element.93.refs_2_, ...), custom_call_target="tpu_custom_call" | custom-call | flops 5637144576 | bytes 2097152 | tf_op jit(solution)/shard_map/pallas_call | solution.py:200
  87.8 3.2 %collective-permute-start.9 = (bf16[128,2048]{1,0:T(8,128)(2,1)}, bf16[128,2048]{1,0:T(8,128)(2,1)}, u32[]{:S(2)}, u32[]{:S(2)}) collective-permute-start(bf16[128,2048]{1,0:T(8,128)(2,1)} %get-tuple-element.101), channel_id=1, source_target_pairs={{0,3},{1,0},{2,1},{3,2},{4,7},{5,4},{6,5},{7,6},{8,11},{9,8},{10,9... | collective-permute-start | bytes 1572872 | tf_op jit(solution)/shard_map/ppermute | solution.py:36
  91.5 8.2 %shard_map.76 = (bf16[128,2048]{1,0:T(8,128)(2,1)}, bf16[128,2048]{1,0:T(8,128)(2,1)}) custom-call(bf16[128,2048]{1,0:T(8,128)(2,1)S(1)} %collective-permute-done.10.refs_0_, bf16[128,2048]{1,0:T(8,128)(2,1)S(1)} %collective-permute-done.11.refs_1_, bf16[7,2048,256]{2,1,0:T(8,128)(2,1)S(1)} %get-tuple-element.93.refs_2_, ...), custom_call_target="tpu_custom_call" | custom-call | flops 5637144576 | bytes 2097152 | tf_op jit(solution)/shard_map/pallas_call | solution.py:200
  99.7 2.0 %collective-permute-start.14 = (bf16[128,2048]{1,0:T(8,128)(2,1)}, bf16[128,2048]{1,0:T(8,128)(2,1)}, u32[]{:S(2)}, u32[]{:S(2)}) collective-permute-start(bf16[128,2048]{1,0:T(8,128)(2,1)} %get-tuple-element.109), channel_id=1, source_target_pairs={{0,1},{1,2},{2,3},{3,0},{4,5},{5,6},{6,7},{7,4},{8,9},{9,10},{10,1... | collective-permute-start | bytes 1572872 | tf_op jit(solution)/shard_map/ppermute | solution.py:36
  101.7 10.1 %shard_map.78 = bf16[256,2048]{1,0:T(8,128)(2,1)} custom-call(bf16[256,2048]{1,0:T(8,128)(2,1)S(1)} %bitcast.59, bf16[1,2048,1792]{2,1,0:T(8,128)(2,1)} %w_gate.3, bf16[1,2048,1792]{2,1,0:T(8,128)(2,1)} %w_up.3, bf16[1,1792,2048]{2,1,0:T(8,128)(2,1)} %w_down.3), custom_call_target="tpu_custom_call" | custom-call | flops 5637144576 | bytes 24117248 | tf_op jit(solution)/shard_map/pallas_call | solution.py:183
  111.8 5.0 %all-to-all-start.3 = ((bf16[32,8,2048]{2,1,0:T(8,128)(2,1)}), bf16[32,8,2048]{2,1,0:T(8,128)(2,1)S(1)}, u32[]{:S(2)}, u32[]{:S(2)}) async-start(bf16[32,8,2048]{2,1,0:T(8,128)(2,1)} %bitcast.22), calls=%async_computation.3 | async-start | bytes 2097152 | tf_op jit(solution)/shard_map/all_to_all | solution.py:42
  116.9 2.0 %add_convert_fusion.2 = bf16[128,2048]{1,0:T(8,128)(2,1)} fusion(bf16[128,2048]{1,0:T(8,128)(2,1)} %collective-permute-done.12, bf16[128,2048]{1,0:T(8,128)(2,1)S(1)} %copy-done.3), kind=kLoop, calls=%fused_computation.17 | loop fusion | flops 1048576 | bytes 1572864 | tf_op jit(solution)/shard_map/convert_element_type | solution.py:55
  120.1 2.0 %add_convert_fusion.1 = bf16[128,2048]{1,0:T(8,128)(2,1)} fusion(bf16[128,2048]{1,0:T(8,128)(2,1)} %collective-permute-done.14, bf16[128,2048]{1,0:T(8,128)(2,1)S(1)} %copy-done.1), kind=kLoop, calls=%fused_computation.16 | loop fusion | flops 1048576 | bytes 1572864 | tf_op jit(solution)/shard_map/convert_element_type | solution.py:55
  123.4 9.9 %collective-permute-done.13 = bf16[128,2048]{1,0:T(8,128)(2,1)} collective-permute-done((bf16[128,2048]{1,0:T(8,128)(2,1)}, bf16[128,2048]{1,0:T(8,128)(2,1)}, u32[]{:S(2)}, u32[]{:S(2)}) %collective-permute-start.13) | collective-permute-done | bytes 524320 | tf_op jit(solution)/shard_map/ppermute | solution.py:36
  133.3 4.1 %collective-permute-done.15 = bf16[128,2048]{1,0:T(8,128)(2,1)} collective-permute-done((bf16[128,2048]{1,0:T(8,128)(2,1)}, bf16[128,2048]{1,0:T(8,128)(2,1)}, u32[]{:S(2)}, u32[]{:S(2)}) %collective-permute-start.15) | collective-permute-done | bytes 524320 | tf_op jit(solution)/shard_map/ppermute | solution.py:36
  137.4 3.0 %add_convert_fusion = bf16[256,2048]{1,0:T(8,128)(2,1)} fusion(bf16[256,2048]{1,0:T(8,128)(2,1)S(1)} %get-tuple-element.110, bf16[128,2048]{1,0:T(8,128)(2,1)} %collective-permute-done.9, bf16[128,2048]{1,0:T(8,128)(2,1)} %collective-permute-done.8, bf16[128,2048]{1,0:T(8,128)(2,1)} %collective-permute-done.15, bf16[128,2048]{1,0:T(8,128)(2,1)} %collective-permute-done.13), kind=kLoop, calls=%fused_computation.2 | loop fusion | flops 6291456 | bytes 4194304 | tf_op jit(solution)/shard_map/convert_element_type | solution.py:365
  140.4 1.9 %shard_map.79 = (bf16[128,2048]{1,0:T(8,128)(2,1)S(1)}, bf16[64,2048]{1,0:T(8,128)(2,1)S(1)}, bf16[64,2048]{1,0:T(8,128)(2,1)S(1)}, bf16[64,2048]{1,0:T(8,128)(2...) custom-call(bf16[512,256]{1,0:T(8,128)(2,1)S(1)} %bitcast_convert_fusion.high, ...), custom_call_target="tpu_custom_call" | custom-call | flops 1073741824 | bytes 3145728 | tf_op jit(solution)/shard_map/pallas_call | solution.py:244
  143.1 7.4 %all-to-all-start.1 = ((bf16[32,8,2048]{2,1,0:T(8,128)(2,1)}), bf16[32,8,2048]{2,1,0:T(8,128)(2,1)S(1)}, u32[]{:S(2)}, u32[]{:S(2)}) async-start(bf16[32,8,2048]{2,1,0:T(8,128)(2,1)} %bitcast.62), calls=%async_computation.1 | async-start | bytes 2097152 | tf_op jit(solution)/shard_map/all_to_all | solution.py:42
  150.4 2.0 %collective-permute-start.16 = (bf16[64,2048]{1,0:T(8,128)(2,1)S(1)}, bf16[64,2048]{1,0:T(8,128)(2,1)S(1)}, u32[]{:S(2)}, u32[]{:S(2)}) collective-permute-start(bf16[64,2048]{1,0:T(8,128)(2,1)S(1)} %get-tuple-element.119), channel_id=1, source_target_pairs={{0,1},{1,2},{2,3},{3,0},{4,5},{5,6},{6,7},{7,4},{8,9},{9,10},{10,1... | collective-permute-start | bytes 786440 | tf_op jit(solution)/shard_map/ppermute | solution.py:36
  152.4 1.3 collective-permute-start.17
  155.4 2.6 %collective-permute-start.19 = (bf16[64,2048]{1,0:T(8,128)(2,1)S(1)}, bf16[64,2048]{1,0:T(8,128)(2,1)S(1)}, u32[]{:S(2)}, u32[]{:S(2)}) collective-permute-start(bf16[64,2048]{1,0:T(8,128)(2,1)S(1)} %add_convert_fusion.4), channel_id=1, source_target_pairs={{0,3},{1,0},{2,1},{3,2},{4,7},{5,4},{6,5},{7,6},{8,11},{9,8},{10,9... | collective-permute-start | bytes 786440 | tf_op jit(solution)/shard_map/ppermute | solution.py:36
  158.1 7.8 %collective-permute-done.20 = bf16[64,2048]{1,0:T(8,128)(2,1)S(1)} collective-permute-done((bf16[64,2048]{1,0:T(8,128)(2,1)}, bf16[64,2048]{1,0:T(8,128)(2,1)S(1)}, u32[]{:S(2)}, u32[]{:S(2)}) %collective-permute-start.20) | collective-permute-done | bytes 262176 | tf_op jit(solution)/shard_map/ppermute | solution.py:36
  166.7 8.1 %collective-permute-done.21.far_b = bf16[64,2048]{1,0:T(8,128)(2,1)S(1)} collective-permute-done((bf16[64,2048]{1,0:T(8,128)(2,1)S(1)}, bf16[64,2048]{1,0:T(8,128)(2,1)S(1)}, u32[]{:S(2)}, u32[]{:S(2)}) %collective-permute-start.21) | collective-permute-done | bytes 262176 | tf_op jit(solution)/shard_map/ppermute | solution.py:36
  (121 shorter events, 23.7 us)
Async XLA Ops:
  2.5 17.6 %collective-permute-start.1 = (bf16[128,2048]{1,0:T(8,128)(2,1)S(1)}, bf16[128,2048]{1,0:T(8,128)(2,1)S(1)}, u32[]{:S(2)}, u32[]{:S(2)}) collective-permute-start(bf16[128,2048]{1,0:T(8,128)(2,1)S(1)} %fusion.7.refs_0_), channel_id=1, source_target_pairs={{0,3},{1,0},{2,1},{3,2},{4,7},{5,4},{6,5},{7,6},{8,11},{9,8},{10,9... | collective-permute-start | bytes 1572872 | tf_op jit(solution)/shard_map/ppermute | solution.py:36
  5.4 18.6 %collective-permute-start = (bf16[128,2048]{1,0:T(8,128)(2,1)S(1)}, bf16[128,2048]{1,0:T(8,128)(2,1)S(1)}, u32[]{:S(2)}, u32[]{:S(2)}) collective-permute-start(bf16[128,2048]{1,0:T(8,128)(2,1)S(1)} %fusion.7.refs_0_), channel_id=1, source_target_pairs={{0,1},{1,2},{2,3},{3,0},{4,5},{5,6},{6,7},{7,4},{8,9},{9,10},{10,1... | collective-permute-start | bytes 1572872 | tf_op jit(solution)/shard_map/ppermute | solution.py:36
  6.2 12.4 %copy-start.14 = (s32[2,128]{1,0:T(2,128)}, s32[2,128]{1,0:T(2,128)S(1)}, u32[]{:S(2)}) copy-start(s32[2,128]{1,0:T(2,128)S(1)} %get-tuple-element.131) | copy-start | bytes 3076
  6.2 12.4 %copy-start.15 = (s32[2,128]{1,0:T(2,128)}, s32[2,128]{1,0:T(2,128)S(1)}, u32[]{:S(2)}) copy-start(s32[2,128]{1,0:T(2,128)S(1)} %get-tuple-element.132) | copy-start | bytes 3076
  8.6 10.7 %copy-start.11 = (pred[256,128]{0,1:T(32,128)(4,1)}, pred[256,128]{0,1:T(32,128)(4,1)S(1)}, u32[]{:S(2)}) copy-start(pred[256,128]{0,1:T(32,128)(4,1)S(1)} %get-tuple-element.126) | copy-start | bytes 98308
  10.0 25.5 %all-to-all-start = ((bf16[32,8,2048]{2,1,0:T(8,128)(2,1)}), bf16[32,8,2048]{2,1,0:T(8,128)(2,1)S(1)}, u32[]{:S(2)}, u32[]{:S(2)}) async-start(bf16[32,8,2048]{2,1,0:T(8,128)(2,1)} %fusion), calls=%async_computation | async-start | bytes 2097152 | tf_op jit(solution)/shard_map/all_to_all | solution.py:42
  20.8 9.6 %collective-permute-start.3 = (bf16[64,2048]{1,0:T(8,128)(2,1)}, bf16[64,2048]{1,0:T(8,128)(2,1)S(1)}, u32[]{:S(2)}, u32[]{:S(2)}) collective-permute-start(bf16[64,2048]{1,0:T(8,128)(2,1)} %slice.73), channel_id=1, source_target_pairs={{0,3},{1,0},{2,1},{3,2},{4,7},{5,4},{6,5},{7,6},{8,11},{9,8},{10,9... | collective-permute-start | bytes 786440 | tf_op jit(solution)/shard_map/ppermute | solution.py:36
  24.8 9.6 %collective-permute-start.2 = (bf16[64,2048]{1,0:T(8,128)(2,1)}, bf16[64,2048]{1,0:T(8,128)(2,1)S(1)}, u32[]{:S(2)}, u32[]{:S(2)}) collective-permute-start(bf16[64,2048]{1,0:T(8,128)(2,1)} %slice.72), channel_id=1, source_target_pairs={{0,1},{1,2},{2,3},{3,0},{4,5},{5,6},{6,7},{7,4},{8,9},{9,10},{10,1... | collective-permute-start | bytes 786440 | tf_op jit(solution)/shard_map/ppermute | solution.py:36
  36.6 22.2 %collective-permute-start.7 = (bf16[128,2048]{1,0:T(8,128)(2,1)}, bf16[128,2048]{1,0:T(8,128)(2,1)}, u32[]{:S(2)}, u32[]{:S(2)}) collective-permute-start(bf16[128,2048]{1,0:T(8,128)(2,1)} %get-tuple-element.127), channel_id=1, source_target_pairs={{0,3},{1,0},{2,1},{3,2},{4,7},{5,4},{6,5},{7,6},{8,11},{9,8},{10,9... | collective-permute-start | bytes 1572872 | tf_op jit(solution)/shard_map/ppermute | solution.py:36
  39.9 36.5 %collective-permute-start.4 = (bf16[128,2048]{1,0:T(8,128)(2,1)}, bf16[128,2048]{1,0:T(8,128)(2,1)}, u32[]{:S(2)}, u32[]{:S(2)}) collective-permute-start(bf16[128,2048]{1,0:T(8,128)(2,1)} %get-tuple-element.127), channel_id=1, source_target_pairs={{0,1},{1,2},{2,3},{3,0},{4,5},{5,6},{6,7},{7,4},{8,9},{9,10},{10,1... | collective-permute-start | bytes 1572872 | tf_op jit(solution)/shard_map/ppermute | solution.py:36
  39.9 26.4 %collective-permute-start.6 = (bf16[128,2048]{1,0:T(8,128)(2,1)}, bf16[128,2048]{1,0:T(8,128)(2,1)}, u32[]{:S(2)}, u32[]{:S(2)}) collective-permute-start(bf16[128,2048]{1,0:T(8,128)(2,1)} %get-tuple-element.128), channel_id=1, source_target_pairs={{0,1},{1,2},{2,3},{3,0},{4,5},{5,6},{6,7},{7,4},{8,9},{9,10},{10,1... | collective-permute-start | bytes 1572872 | tf_op jit(solution)/shard_map/ppermute | solution.py:36
  39.9 36.5 %collective-permute-start.5 = (bf16[128,2048]{1,0:T(8,128)(2,1)}, bf16[128,2048]{1,0:T(8,128)(2,1)}, u32[]{:S(2)}, u32[]{:S(2)}) collective-permute-start(bf16[128,2048]{1,0:T(8,128)(2,1)} %get-tuple-element.128), channel_id=1, source_target_pairs={{0,3},{1,0},{2,1},{3,2},{4,7},{5,4},{6,5},{7,6},{8,11},{9,8},{10,9... | collective-permute-start | bytes 1572872 | tf_op jit(solution)/shard_map/ppermute | solution.py:36
  44.8 56.9 %all-to-all-start.2 = ((bf16[32,8,2048]{2,1,0:T(8,128)(2,1)}), bf16[32,8,2048]{2,1,0:T(8,128)(2,1)S(1)}, u32[]{:S(2)}, u32[]{:S(2)}) async-start(bf16[32,8,2048]{2,1,0:T(8,128)(2,1)} %bitcast.20), calls=%async_computation.2 | async-start | bytes 2097152 | tf_op jit(solution)/shard_map/all_to_all | solution.py:42
  76.4 14.7 %collective-permute-start.11 = (bf16[128,2048]{1,0:T(8,128)(2,1)}, bf16[128,2048]{1,0:T(8,128)(2,1)S(1)}, u32[]{:S(2)}, u32[]{:S(2)}) collective-permute-start(bf16[128,2048]{1,0:T(8,128)(2,1)} %collective-permute-done.7.refs_1_), channel_id=1, source_target_pairs={{0,3},{1,0},{2,1},{3,2},{4,7},{5,4},{6,5},{7,6},{8,11},{9,8},{10,9... | collective-permute-start | bytes 1572872 | tf_op jit(solution)/shard_map/ppermute | solution.py:36
  76.4 15.1 %collective-permute-start.10 = (bf16[128,2048]{1,0:T(8,128)(2,1)}, bf16[128,2048]{1,0:T(8,128)(2,1)S(1)}, u32[]{:S(2)}, u32[]{:S(2)}) collective-permute-start(bf16[128,2048]{1,0:T(8,128)(2,1)} %collective-permute-done.6.refs_0_), channel_id=1, source_target_pairs={{0,1},{1,2},{2,3},{3,0},{4,5},{5,6},{6,7},{7,4},{8,9},{9,10},{10,1... | collective-permute-start | bytes 1572872 | tf_op jit(solution)/shard_map/ppermute | solution.py:36
  87.8 35.5 %collective-permute-start.8 = (bf16[128,2048]{1,0:T(8,128)(2,1)}, bf16[128,2048]{1,0:T(8,128)(2,1)}, u32[]{:S(2)}, u32[]{:S(2)}) collective-permute-start(bf16[128,2048]{1,0:T(8,128)(2,1)} %get-tuple-element.100), channel_id=1, source_target_pairs={{0,1},{1,2},{2,3},{3,0},{4,5},{5,6},{6,7},{7,4},{8,9},{9,10},{10,1... | collective-permute-start | bytes 1572872 | tf_op jit(solution)/shard_map/ppermute | solution.py:36
  87.8 35.5 %collective-permute-start.9 = (bf16[128,2048]{1,0:T(8,128)(2,1)}, bf16[128,2048]{1,0:T(8,128)(2,1)}, u32[]{:S(2)}, u32[]{:S(2)}) collective-permute-start(bf16[128,2048]{1,0:T(8,128)(2,1)} %get-tuple-element.101), channel_id=1, source_target_pairs={{0,3},{1,0},{2,1},{3,2},{4,7},{5,4},{6,5},{7,6},{8,11},{9,8},{10,9... | collective-permute-start | bytes 1572872 | tf_op jit(solution)/shard_map/ppermute | solution.py:36
  99.7 17.2 %collective-permute-start.12 = (bf16[128,2048]{1,0:T(8,128)(2,1)}, bf16[128,2048]{1,0:T(8,128)(2,1)}, u32[]{:S(2)}, u32[]{:S(2)}) collective-permute-start(bf16[128,2048]{1,0:T(8,128)(2,1)} %get-tuple-element.107), channel_id=1, source_target_pairs={{0,3},{1,0},{2,1},{3,2},{4,7},{5,4},{6,5},{7,6},{8,11},{9,8},{10,9... | collective-permute-start | bytes 1572872 | tf_op jit(solution)/shard_map/ppermute | solution.py:36
  99.7 20.4 %collective-permute-start.14 = (bf16[128,2048]{1,0:T(8,128)(2,1)}, bf16[128,2048]{1,0:T(8,128)(2,1)}, u32[]{:S(2)}, u32[]{:S(2)}) collective-permute-start(bf16[128,2048]{1,0:T(8,128)(2,1)} %get-tuple-element.109), channel_id=1, source_target_pairs={{0,1},{1,2},{2,3},{3,0},{4,5},{5,6},{6,7},{7,4},{8,9},{9,10},{10,1... | collective-permute-start | bytes 1572872 | tf_op jit(solution)/shard_map/ppermute | solution.py:36
  111.8 8.3 %copy-start.1 = (bf16[128,2048]{1,0:T(8,128)(2,1)S(1)}, bf16[128,2048]{1,0:T(8,128)(2,1)}, u32[]{:S(2)}) copy-start(bf16[128,2048]{1,0:T(8,128)(2,1)} %copy-done) | copy-start | bytes 1572868
  111.8 28.6 %all-to-all-start.3 = ((bf16[32,8,2048]{2,1,0:T(8,128)(2,1)}), bf16[32,8,2048]{2,1,0:T(8,128)(2,1)S(1)}, u32[]{:S(2)}, u32[]{:S(2)}) async-start(bf16[32,8,2048]{2,1,0:T(8,128)(2,1)} %bitcast.22), calls=%async_computation.3 | async-start | bytes 2097152 | tf_op jit(solution)/shard_map/all_to_all | solution.py:42
  118.9 14.4 %collective-permute-start.13 = (bf16[128,2048]{1,0:T(8,128)(2,1)}, bf16[128,2048]{1,0:T(8,128)(2,1)}, u32[]{:S(2)}, u32[]{:S(2)}) collective-permute-start(bf16[128,2048]{1,0:T(8,128)(2,1)} %add_convert_fusion.2), channel_id=1, source_target_pairs={{0,3},{1,0},{2,1},{3,2},{4,7},{5,4},{6,5},{7,6},{8,11},{9,8},{10,9... | collective-permute-start | bytes 1572872 | tf_op jit(solution)/shard_map/ppermute | solution.py:36
  122.1 15.3 %collective-permute-start.15 = (bf16[128,2048]{1,0:T(8,128)(2,1)}, bf16[128,2048]{1,0:T(8,128)(2,1)}, u32[]{:S(2)}, u32[]{:S(2)}) collective-permute-start(bf16[128,2048]{1,0:T(8,128)(2,1)} %add_convert_fusion.1), channel_id=1, source_target_pairs={{0,1},{1,2},{2,3},{3,0},{4,5},{5,6},{6,7},{7,4},{8,9},{9,10},{10,1... | collective-permute-start | bytes 1572872 | tf_op jit(solution)/shard_map/ppermute | solution.py:36
  143.1 23.6 %copy-start.6 = (f32[256,128]{0,1:T(8,128)S(1)}, f32[256,128]{0,1:T(8,128)}, u32[]{:S(2)}) copy-start(f32[256,128]{0,1:T(8,128)} %copy-done.5) | copy-start | bytes 393220
  143.1 23.6 %copy-start.12 = (pred[256,128]{0,1:T(32,128)(4,1)S(1)}, pred[256,128]{0,1:T(32,128)(4,1)}, u32[]{:S(2)}) copy-start(pred[256,128]{0,1:T(32,128)(4,1)} %copy-done.11) | copy-start | bytes 98308
  143.1 11.4 %collective-permute-start.18 = (bf16[64,2048]{1,0:T(8,128)(2,1)}, bf16[64,2048]{1,0:T(8,128)(2,1)}, u32[]{:S(2)}, u32[]{:S(2)}) collective-permute-start(bf16[64,2048]{1,0:T(8,128)(2,1)} %get-tuple-element.122), channel_id=1, source_target_pairs={{0,3},{1,0},{2,1},{3,2},{4,7},{5,4},{6,5},{7,6},{8,11},{9,8},{10,9... | collective-permute-start | bytes 786440 | tf_op jit(solution)/shard_map/ppermute | solution.py:36
  143.1 31.7 %all-to-all-start.1 = ((bf16[32,8,2048]{2,1,0:T(8,128)(2,1)}), bf16[32,8,2048]{2,1,0:T(8,128)(2,1)S(1)}, u32[]{:S(2)}, u32[]{:S(2)}) async-start(bf16[32,8,2048]{2,1,0:T(8,128)(2,1)} %bitcast.62), calls=%async_computation.1 | async-start | bytes 2097152 | tf_op jit(solution)/shard_map/all_to_all | solution.py:42
  150.4 16.2 %collective-permute-start.16 = (bf16[64,2048]{1,0:T(8,128)(2,1)S(1)}, bf16[64,2048]{1,0:T(8,128)(2,1)S(1)}, u32[]{:S(2)}, u32[]{:S(2)}) collective-permute-start(bf16[64,2048]{1,0:T(8,128)(2,1)S(1)} %get-tuple-element.119), channel_id=1, source_target_pairs={{0,1},{1,2},{2,3},{3,0},{4,5},{5,6},{6,7},{7,4},{8,9},{9,10},{10,1... | collective-permute-start | bytes 786440 | tf_op jit(solution)/shard_map/ppermute | solution.py:36
  152.4 14.3 %collective-permute-start.17 = (bf16[64,2048]{1,0:T(8,128)(2,1)S(1)}, bf16[64,2048]{1,0:T(8,128)(2,1)S(1)}, u32[]{:S(2)}, u32[]{:S(2)}) collective-permute-start(bf16[64,2048]{1,0:T(8,128)(2,1)S(1)} %get-tuple-element.120), channel_id=1, source_target_pairs={{0,3},{1,0},{2,1},{3,2},{4,7},{5,4},{6,5},{7,6},{8,11},{9,8},{10,9... | collective-permute-start | bytes 786440 | tf_op jit(solution)/shard_map/ppermute | solution.py:36
  153.7 12.1 %collective-permute-start.20 = (bf16[64,2048]{1,0:T(8,128)(2,1)}, bf16[64,2048]{1,0:T(8,128)(2,1)S(1)}, u32[]{:S(2)}, u32[]{:S(2)}) collective-permute-start(bf16[64,2048]{1,0:T(8,128)(2,1)} %copy-done.4), channel_id=1, source_target_pairs={{0,1},{1,2},{2,3},{3,0},{4,5},{5,6},{6,7},{7,4},{8,9},{9,10},{10,1... | collective-permute-start | bytes 786440 | tf_op jit(solution)/shard_map/ppermute | solution.py:36
  155.4 11.2 %collective-permute-start.19 = (bf16[64,2048]{1,0:T(8,128)(2,1)S(1)}, bf16[64,2048]{1,0:T(8,128)(2,1)S(1)}, u32[]{:S(2)}, u32[]{:S(2)}) collective-permute-start(bf16[64,2048]{1,0:T(8,128)(2,1)S(1)} %add_convert_fusion.4), channel_id=1, source_target_pairs={{0,3},{1,0},{2,1},{3,2},{4,7},{5,4},{6,5},{7,6},{8,11},{9,8},{10,9... | collective-permute-start | bytes 786440 | tf_op jit(solution)/shard_map/ppermute | solution.py:36
  165.9 8.9 %collective-permute-start.21 = (bf16[64,2048]{1,0:T(8,128)(2,1)S(1)}, bf16[64,2048]{1,0:T(8,128)(2,1)S(1)}, u32[]{:S(2)}, u32[]{:S(2)}) collective-permute-start(bf16[64,2048]{1,0:T(8,128)(2,1)S(1)} %add_convert_fusion.3), channel_id=1, source_target_pairs={{0,1},{1,2},{2,3},{3,0},{4,5},{5,6},{6,7},{7,4},{8,9},{9,10},{10,1... | collective-permute-start | bytes 786440 | tf_op jit(solution)/shard_map/ppermute | solution.py:36
  (10 other events, 37.0 us)
where the time goes:
time: 177 us; the launch traced here: 176 us
  starting transfers between devices  54.9 us (31%)
  Pallas kernels  50.3 us (28%)
  waiting for transfers between devices  44.8 us (25%)
  other arithmetic  14.2 us (8%)
  local copies, waits for them, and re-layouts  9.47 us (5%)
  matrix products  2 us (1%)
    ppermute x22, waiting for transfers between devices, shift(): lax.ppermute(value, 'tp', [(i, (i + by) % size) for i in range(size)])  43.6 us
    ppermute x22, starting transfers between devices, shift(): lax.ppermute(value, 'tp', [(i, (i + by) % size) for i in range(size)])  29.3 us
    pallas_call x3, Pallas kernels, expert_kept(): pl.pallas_call(functools.partial(kept_kernel, len(blocks)), in_specs=[VME...  26.1 us
    all_to_all x4, starting transfers between devices, exchange(): return lax.all_to_all(tiles, EP, 0, 0, tiled=True).reshape(rows.shape)  25.5 us
    pallas_call x2, Pallas kernels, expert_streamed(): pl.pallas_call(stream_kernel, in_specs=[VMEM_SPEC] + [HBM_SPEC] * 3, out_...  19.2 us
    convert_element_type x4, other arithmetic, add_rounded(): return (a.astype(jnp.float32) + b.astype(jnp.float32)).astype(jnp.bfloat16)  5.02 us
  transfers between devices with their start and end apart: 26, of which 9 were waited for; matrix products, arithmetic and copies ran while one was open for 11% of the time, Pallas kernels for 27%

commit v1 on v0

v1 whole, which is shorter than its diff:
```python
import functools

import jax
import jax.numpy as jnp
from jax import lax
from jax.experimental import pallas as pl
from jax.experimental.pallas import tpu as pltpu
from jax.sharding import Mesh
from jax.sharding import PartitionSpec as P


EP = ("ep_0", "ep_1", "ep_2")
EP_TP = ("ep_0", "ep_1", "ep_2", "tp")
CAP = 10
EARLY = 8
LATE = CAP - EARLY
OFFSETS = (0, -1, 1, 2)
UP_TILE = 256
DOWN_TILE = 1024
MIB = 2**20
LANES = 128


norm_eps = 1e-05
VMEM_SPEC = pl.BlockSpec(memory_space=pltpu.VMEM)
SMEM_SPEC = pl.BlockSpec(memory_space=pltpu.SMEM)
HBM_SPEC = pl.BlockSpec(memory_space=pltpu.HBM)


def ones_where(mask):
    return jnp.where(mask, 1.0, 0.0).astype(jnp.bfloat16)


def routed(ids, block, experts_all):
    own = ids[:, pl.ds(pl.multiple_of(block * LANES, LANES), LANES)]
    expert = lax.broadcasted_iota(jnp.int32, (experts_all, LANES), 0)
    return own[0:1] == expert, own[1:2] == expert


def slots_of(hits):
    named = hits[0] | hits[1]
    before = lax.broadcasted_iota(jnp.int32, (LANES, LANES), 0)
    after = lax.broadcasted_iota(jnp.int32, (LANES, LANES), 1)
    rank = jnp.dot(ones_where(named), ones_where(before < after), preferred_element_type=jnp.float32)
    return jnp.where(named, rank, -1.0).astype(jnp.bfloat16)


def per_row(values, rows):
    experts_all = values.shape[0]
    row = lax.broadcasted_iota(jnp.int32, (rows, experts_all), 0) // (rows // experts_all)
    column = lax.broadcasted_iota(jnp.int32, (rows, experts_all), 1)
    return jnp.dot(ones_where(row == column), values, preferred_element_type=jnp.float32)


def early_rows(hits, rows):
    wanted = lax.broadcasted_iota(jnp.int32, (rows, LANES), 0) % EARLY
    return per_row(slots_of(hits), rows) == wanted.astype(jnp.float32)


def late_rows_of(hits, rows, at):
    place_in = lax.broadcasted_iota(jnp.int32, (rows, LANES), 0) % (LATE * len(OFFSETS))
    wanted = jnp.where(place_in // LATE == at, EARLY + place_in % LATE, -2)
    return per_row(slots_of(hits), rows) == wanted.astype(jnp.float32)


def weighted_sum(chosen, hits, route, block, rows):
    weight = route[:, pl.ds(pl.multiple_of(block * LANES, LANES), LANES)]
    mass = jnp.where(hits[0], weight[0:1], 0.0) + jnp.where(hits[1], weight[1:2], 0.0)
    high = mass.astype(jnp.bfloat16)
    low = (mass - high.astype(jnp.float32)).astype(jnp.bfloat16)
    total = None
    for part in (high, low):
        term = jnp.where(chosen, per_row(part, chosen.shape[0]), 0.0).astype(jnp.bfloat16)
        term = lax.dot_general(
            term, rows[...], (((0,), (0,)), ((), ())), preferred_element_type=jnp.float32
        )
        total = term if total is None else total + term
    return total


def block_at(me, by):
    return (me[0] + by + len(OFFSETS)) % len(OFFSETS)


def prepare_kernel(me, tokens, gain, ids, normed, sent):
    experts_all = sent.shape[0] // EARLY
    values = tokens[...].astype(jnp.float32)
    factor = lax.rsqrt(jnp.mean(values * values, axis=-1, keepdims=True) + norm_eps)
    normal = (values * factor * gain[...]).astype(jnp.bfloat16)
    normed[...] = normal
    chosen = ones_where(early_rows(routed(ids, me[0], experts_all), sent.shape[0]))
    sent[...] = jnp.dot(chosen, normal, preferred_element_type=jnp.float32).astype(jnp.bfloat16)


def prepare(tokens, norm_gain, expert_ids, me, experts_all):
    tok_count, d = tokens.shape
    rows = experts_all * EARLY
    return pl.pallas_call(
        prepare_kernel,
        in_specs=[pl.BlockSpec(memory_space=pltpu.SMEM)] + [VMEM_SPEC] * 3,
        out_specs=[VMEM_SPEC] * 2,
        out_shape=[
            jax.ShapeDtypeStruct((tok_count, d), jnp.bfloat16),
            jax.ShapeDtypeStruct((rows, d), jnp.bfloat16),
        ],
        compiler_params=pltpu.CompilerParams(vmem_limit_bytes=16 * MIB),
        cost_estimate=pl.CostEstimate(
            flops=2 * rows * tok_count * d, bytes_accessed=2 * d * (rows + 2 * tok_count), transcendentals=0
        ),
    )(me, *in_hbm(tokens, norm_gain.reshape(1, d), expert_ids))


def in_hbm(*values):
    return tuple(pltpu.with_memory_space_constraint(v, pltpu.HBM) for v in values)


def shift(value, by):
    size = lax.axis_size("tp")
    return lax.ppermute(value, "tp", [(i, (i + by) % size) for i in range(size)])


def exchange(rows):
    ep_size = lax.axis_size(EP)
    tiles = rows.reshape(ep_size, rows.shape[0] // ep_size, rows.shape[1])
    return lax.all_to_all(tiles, EP, 0, 0, tiled=True).reshape(rows.shape)


def gather_tp(rows):
    half = rows.shape[0] // 2
    from_left = shift(rows, 1)
    from_right = shift(rows, -1)
    far_a = shift(from_left[:half], 1)
    far_b = shift(from_right[half:], -1)
    return rows, from_left, from_right, far_a, far_b


def add_kernel(a, b, c, d, left, right):
    left[...] = (a[...].astype(jnp.float32) + b[...].astype(jnp.float32)).astype(left.dtype)
    right[...] = (c[...].astype(jnp.float32) + d[...].astype(jnp.float32)).astype(right.dtype)


def add_pairs(a, b, c, d):
    return pl.pallas_call(
        add_kernel,
        in_specs=[VMEM_SPEC] * 4,
        out_specs=[VMEM_SPEC] * 2,
        out_shape=[jax.ShapeDtypeStruct(v.shape, v.dtype) for v in (a, c)],
        compiler_params=pltpu.CompilerParams(vmem_limit_bytes=12 * MIB),
        cost_estimate=pl.CostEstimate(flops=2 * a.size, bytes_accessed=12 * a.size, transcendentals=0),
    )(a, b, c, d)


def place(target, blocks):
    at = 0
    for b in blocks:
        target[at : at + b.shape[0], :] = b[...]
        at += b.shape[0]


def cut(value, outs, columns=slice(None)):
    at = 0
    for o in outs:
        o[:, columns] = value[at : at + o.shape[0]].astype(o.dtype)
        at += o.shape[0]


def cols(t, width):
    return pl.ds(pl.multiple_of(t * width, width), width)


def expert_rows(rows, hidden, gates, ups, up_tiles, down_tile, outs):
    steps, downs = hidden.shape[1] // UP_TILE, outs[0].shape[1] // DOWN_TILE

    def multiply(t):
        w_gate, w_up = up_tiles(t)
        gate = jnp.dot(rows[...], w_gate[...], preferred_element_type=jnp.float32)
        up = jnp.dot(rows[...], w_up[...], preferred_element_type=jnp.float32)
        return gate, up

    def activate(t):
        gate, up = gates[t % 2], ups[t % 2]
        value = (gate / (1.0 + jnp.exp(-gate)) * up).astype(jnp.bfloat16)
        hidden[:, cols(t, UP_TILE)] = value

    def up_step(t, c):
        gate, up = multiply(t)
        activate(t - 1)
        gates[t % 2] = gate
        ups[t % 2] = up
        return c

    gates[0], ups[0] = multiply(0)
    lax.fori_loop(1, steps, up_step, 0)
    activate(steps - 1)

    def down_step(t, c):
        part = jnp.dot(hidden[...], down_tile(t)[...], preferred_element_type=jnp.float32)
        cut(part, outs, cols(t, DOWN_TILE))
        return c

    lax.fori_loop(0, downs, down_step, 0)


def stream_kernel(n_in, n_out, *refs):
    blocks, (w_gate, w_up, w_down) = refs[:n_in], refs[n_in : n_in + 3]
    outs = refs[n_in + 3 : n_in + 3 + n_out]
    gate_all, up_all, down_all, rows, hidden, gates, ups, sems = refs[n_in + 3 + n_out :]

    def load(kind, t):
        src, dst = ((w_gate, gate_all), (w_up, up_all), (w_down, down_all))[kind]
        at = cols(t, DOWN_TILE if kind == 2 else UP_TILE)
        return pltpu.make_async_copy(src.at[0, :, at], dst.at[:, at], sems.at[kind, t])

    def start_up(t, c):
        load(0, t).start()
        load(1, t).start()
        return c

    def start_down(t, c):
        load(2, t).start()
        return c

    lax.fori_loop(0, gate_all.shape[1] // UP_TILE, start_up, 0)
    lax.fori_loop(0, down_all.shape[1] // DOWN_TILE, start_down, 0)
    place(rows, blocks)

    def up_tiles_of(t):
        load(0, t).wait()
        load(1, t).wait()
        return gate_all.at[:, cols(t, UP_TILE)], up_all.at[:, cols(t, UP_TILE)]

    def down_tile_of(t):
        load(2, t).wait()
        return down_all.at[:, cols(t, DOWN_TILE)]

    expert_rows(rows, hidden, gates, ups, up_tiles_of, down_tile_of, outs)


def kept_kernel(n_in, *refs):
    blocks = refs[:n_in]
    w_gate, w_up, w_down = refs[n_in : n_in + 3]
    outs, rows = refs[n_in + 3 : -1], refs[-1]
    place(rows, blocks)
    gate = jnp.dot(rows[...], w_gate[...], preferred_element_type=jnp.float32)
    up = jnp.dot(rows[...], w_up[...], preferred_element_type=jnp.float32)
    hidden = (gate / (1.0 + jnp.exp(-gate)) * up).astype(jnp.bfloat16)
    cut(jnp.dot(hidden, w_down[...], preferred_element_type=jnp.float32), outs)


def expert_cost(m, d, ff, weights):
    return pl.CostEstimate(
        flops=6 * m * d * ff, bytes_accessed=6 * d * ff * weights + 4 * m * d, transcendentals=m * ff
    )


def row_buffers(m, d, ff):
    return [
        pltpu.VMEM((m, d), jnp.bfloat16),
        pltpu.VMEM((m, ff), jnp.bfloat16),
        pltpu.VMEM((2, m, UP_TILE), jnp.float32),
        pltpu.VMEM((2, m, UP_TILE), jnp.float32),
    ]


def expert_streamed(blocks, sizes, weights, keep):
    d, ff = weights[0].shape[1:]
    m = sum(b.shape[0] for b in blocks)
    steps, downs = ff // UP_TILE, d // DOWN_TILE
    tiles = [
        pltpu.VMEM((d, ff), jnp.bfloat16),
        pltpu.VMEM((d, ff), jnp.bfloat16),
        pltpu.VMEM((ff, d), jnp.bfloat16),
    ]
    return pl.pallas_call(
        functools.partial(stream_kernel, len(blocks), len(sizes)),
        in_specs=[VMEM_SPEC] * len(blocks) + [HBM_SPEC] * 3,
        out_specs=[VMEM_SPEC] * (len(sizes) + (3 if keep else 0)),
        out_shape=[pltpu.HBM((s, d), jnp.bfloat16) for s in sizes] + (tiles if keep else []),
        scratch_shapes=([] if keep else tiles)
        + row_buffers(m, d, ff)
        + [pltpu.SemaphoreType.DMA((3, max(steps, downs)))],
        compiler_params=pltpu.CompilerParams(vmem_limit_bytes=(12 if keep else 34) * MIB),
        cost_estimate=expert_cost(m, d, ff, 1),
    )(*blocks, *in_hbm(*weights))


def expert_kept(blocks, sizes, tiles):
    d, ff = tiles[0].shape
    m = sum(b.shape[0] for b in blocks)
    return pl.pallas_call(
        functools.partial(kept_kernel, len(blocks)),
        in_specs=[VMEM_SPEC] * (len(blocks) + 3),
        out_specs=[VMEM_SPEC] * len(sizes),
        out_shape=[jax.ShapeDtypeStruct((s, d), jnp.bfloat16) for s in sizes],
        scratch_shapes=[pltpu.VMEM((m, d), jnp.bfloat16)],
        compiler_params=pltpu.CompilerParams(vmem_limit_bytes=20 * MIB),
        cost_estimate=expert_cost(m, d, ff, 0),
    )(*blocks, *(pltpu.with_memory_space_constraint(w, pltpu.VMEM) for w in tiles))


def select_kernel(me, ids, *refs):
    blocks, out, rows, chosen = refs[:-3], refs[-3], refs[-2], refs[-1]
    experts_all = out.shape[0] // (LATE * len(OFFSETS))
    place(rows, blocks)
    for at, by in enumerate(OFFSETS):
        hits = routed(ids, block_at(me, by), experts_all)
        chosen[:, at * LANES : (at + 1) * LANES] = ones_where(late_rows_of(hits, out.shape[0], at))
    value = jnp.dot(chosen[...], rows[...], preferred_element_type=jnp.float32)
    out[...] = value.astype(out.dtype)


def select_late(me, expert_ids, blocks, experts_all):
    d = blocks[0].shape[1]
    n, m = experts_all * LATE * len(OFFSETS), LANES * len(OFFSETS)
    return pl.pallas_call(
        select_kernel,
        in_specs=[SMEM_SPEC] + [VMEM_SPEC] * (1 + len(blocks)),
        out_specs=VMEM_SPEC,
        out_shape=jax.ShapeDtypeStruct((n, d), jnp.bfloat16),
        scratch_shapes=[pltpu.VMEM((m, d), jnp.bfloat16), pltpu.VMEM((n, m), jnp.bfloat16)],
        compiler_params=pltpu.CompilerParams(vmem_limit_bytes=16 * MIB),
        cost_estimate=pl.CostEstimate(
            flops=2 * n * m * d, bytes_accessed=2 * d * (n + m), transcendentals=0
        ),
    )(me, expert_ids, *in_hbm(*blocks))


def weigh_kernel(me, ids, route, rows, own, *others):
    experts_all = rows.shape[0] // (LATE * len(OFFSETS))
    for at, by in enumerate(OFFSETS):
        block = block_at(me, by)
        hits = routed(ids, block, experts_all)
        chosen = late_rows_of(hits, rows.shape[0], at)
        value = weighted_sum(chosen, hits, route, block, rows)
        cut(value, [own] if at == 0 else others[2 * at - 2 : 2 * at])


def weigh_late(me, expert_ids, route_weight, rows):
    n, d = rows.shape
    sizes = [LANES] + [LANES // 2] * (2 * len(OFFSETS) - 2)
    return pl.pallas_call(
        weigh_kernel,
        in_specs=[SMEM_SPEC] + [VMEM_SPEC] * 3,
        out_specs=[VMEM_SPEC] * len(sizes),
        out_shape=[pltpu.HBM((s, d), jnp.bfloat16) for s in sizes],
        compiler_params=pltpu.CompilerParams(vmem_limit_bytes=16 * MIB),
        cost_estimate=pl.CostEstimate(
            flops=4 * n * LANES * len(OFFSETS) * d, bytes_accessed=6 * d * n, transcendentals=0
        ),
    )(me, expert_ids, route_weight, rows)


def finish_kernel(me, ids, route, rows, own, near_a, near_b, far_a, far_b, out):
    hits = routed(ids, me[0], rows.shape[0] // EARLY)
    value = weighted_sum(early_rows(hits, rows.shape[0]), hits, route, me[0], rows)
    value = value + own[...].astype(jnp.float32)
    half = out.shape[0] // 2
    top = near_a[...].astype(jnp.float32) + far_a[...].astype(jnp.float32)
    bottom = near_b[...].astype(jnp.float32) + far_b[...].astype(jnp.float32)
    out[:half, :] = (value[:half] + top).astype(out.dtype)
    out[half:, :] = (value[half:] + bottom).astype(out.dtype)


def finish(me, expert_ids, route_weight, rows, own, pieces):
    n, d = rows.shape
    return pl.pallas_call(
        finish_kernel,
        in_specs=[SMEM_SPEC] + [VMEM_SPEC] * 8,
        out_specs=VMEM_SPEC,
        out_shape=jax.ShapeDtypeStruct((LANES, d), jnp.bfloat16),
        compiler_params=pltpu.CompilerParams(vmem_limit_bytes=16 * MIB),
        cost_estimate=pl.CostEstimate(
            flops=4 * n * LANES * d, bytes_accessed=2 * d * (n + 4 * LANES), transcendentals=0
        ),
    )(me, expert_ids, route_weight, rows, own, *pieces)


def send_near(to_left, to_right):
    got_bottom = shift(to_left, -1)
    got_top = shift(to_right, 1)
    return got_top, got_bottom


def send_far(far_top, far_bottom):
    return shift(far_top, -1), shift(far_bottom, 1)


def send_on(to_left, to_right, via_right, via_left):
    left, right = add_pairs(to_left, via_right, to_right, via_left)
    return shift(left, -1), shift(right, 1)


def per_device(tokens, norm_gain, expert_ids, route_weight, exp_gate, exp_up, exp_down):
    experts_all = lax.axis_size(EP)
    me = lax.axis_index("tp").reshape(1)
    ids, route = expert_ids.T, route_weight.T

    normed, sent = prepare(tokens, norm_gain, ids, me, experts_all)
    blocks = gather_tp(normed)
    arrived = exchange(sent)
    arrived, blocks = lax.optimization_barrier((arrived, blocks))

    late_sent = select_late(me, ids, blocks, experts_all)
    late_arrived = exchange(late_sent)

    mid = arrived.shape[0] // 2
    top, bottom = arrived[:mid], arrived[mid:]
    left_top, right_bottom = shift(top, 1), shift(bottom, -1)
    left_bottom, right_top = shift(bottom, 1), shift(top, -1)
    far_top, far_bottom = shift(left_top, 1), shift(right_bottom, -1)
    weights = (exp_gate, exp_up, exp_down)
    *first, gate_tiles, up_tiles, down_tiles = expert_streamed(
        [left_top, right_bottom], [mid] * 2, weights, True
    )
    tiles = (gate_tiles, up_tiles, down_tiles)
    left_bottom, right_top, first = lax.optimization_barrier((left_bottom, right_top, first))
    second = expert_kept([left_bottom, right_top], [mid] * 2, tiles)
    near = send_near(*second)
    far_top, far_bottom, second = lax.optimization_barrier((far_top, far_bottom, second))
    third = expert_kept([far_top, far_bottom], [mid] * 2, tiles)
    via = send_far(*third)
    late_arrived, _ = lax.optimization_barrier((late_arrived, third))
    (late_part,) = expert_streamed([late_arrived], [late_arrived.shape[0]], weights, False)
    late_back = exchange(late_part)
    on = send_on(*first, *via)
    own_rows, _ = lax.optimization_barrier((arrived, (late_part, via)))
    (own_part,) = expert_streamed([own_rows], [2 * mid], weights, False)
    summed = jnp.concatenate(near, axis=0).astype(jnp.float32)
    summed = summed + jnp.concatenate(on, axis=0).astype(jnp.float32)
    summed = (summed + own_part.astype(jnp.float32)).astype(jnp.bfloat16)
    back = exchange(summed)

    late_back, _ = lax.optimization_barrier((late_back, own_part))
    sums = weigh_late(me, ids, route, late_back)
    token_own, left_top, left_bottom, right_top, right_bottom, far_top, far_bottom = sums
    token_via = send_far(far_top, far_bottom)
    token_near = send_near(left_bottom, right_top)
    token_on = send_on(left_top, right_bottom, *token_via)
    return finish(me, ids, route, back, token_own, token_near + token_on)


def solution(mesh):
    finer = Mesh(mesh.devices.reshape(4, 4, 2, mesh.shape["tp"]), ("ep_0", "ep_1", "ep_2", "tp"))
    return jax.shard_map(
        per_device,
        mesh=finer,
        in_specs=(
            P(EP_TP, None),
            P(),
            P(EP, None),
            P(EP, None),
            P(EP, None, "tp"),
            P(EP, None, "tp"),
            P(EP, "tp", None),
        ),
        out_specs=P(EP_TP, None),
        check_vma=False,
    )
```

time: 177 us -> 165 us (0.932)
  other arithmetic: 14.2 us -> 3.06 us
  Pallas kernels: 50.3 us -> 58.9 us
  waiting for transfers between devices: 44.8 us -> 39.3 us
  local copies, waits for them, and re-layouts: 9.47 us -> 4.07 us
  starting transfers between devices: 54.9 us -> 58.8 us
  matrix products: 2 us -> 0 us
    pallas_call x5 -> x9, Pallas kernels: 24.2 us -> 43.8 us  [the longest x3 30.7 us: expert_streamed(): pl.pallas_call(functools.partial(stream_kernel, len(blocks), len(sizes)),...]
    pallas_call x3 -> x2, Pallas kernels: 26.1 us -> 15.2 us  [expert_kept(): pl.pallas_call(functools.partial(kept_kernel, len(blocks)), in_specs=[VME...]
    convert_element_type x11 -> x0, other arithmetic: 10.2 us -> none  [the longest x4 5.02 us: add_rounded(): return (a.astype(jnp.float32) + b.astype(jnp.float32)).astype(jnp.bfloat16)]
    all_to_all x4, starting transfers between devices: 25.5 us -> 30.1 us  [exchange(): return lax.all_to_all(tiles, EP, 0, 0, tiled=True).reshape(rows.shape)]
    ppermute x22, waiting for transfers between devices: 43.6 us -> 39.3 us  [shift(): lax.ppermute(value, 'tp', [(i, (i + by) % size) for i in range(size)])]
    reshape x0 -> x1, other arithmetic: none -> 3.06 us  [exchange(): tiles = rows.reshape(ep_size, rows.shape[0] // ep_size, rows.shape[1])]
    reduce_sum x3 -> x0, other arithmetic: 2.54 us -> none  [the longest x2 1.31 us: per_device(): masses.append(jnp.sum(jnp.where(hits, weight.T[:, None, :], 0.0), axis=0))]
    dot_general x5 -> x0, matrix products: 2 us -> none  [the longest x1 1.46 us: per_device(): jnp.dot(chosen, normed, preferred_element_type=jnp.float32)]
  transfers between devices with their start and end apart: 26 -> 26, of which waited for: 9 -> 13; matrix products, arithmetic and copies ran while one was open for 11% -> 2% of each run, Pallas kernels for 27% -> 33%
where the time goes in v1:
time: 165 us; the launch traced here: 164 us
  Pallas kernels  58.9 us (36%)
  starting transfers between devices  58.8 us (36%)
  waiting for transfers between devices  39.3 us (24%)
  local copies, waits for them, and re-layouts  4.07 us (2%)
  other arithmetic  3.06 us (2%)
    ppermute x22, waiting for transfers between devices, shift(): lax.ppermute(value, 'tp', [(i, (i + by) % size) for i in range(size)])  39.3 us
    pallas_call x3, Pallas kernels, expert_streamed(): pl.pallas_call(functools.partial(stream_kernel, len(blocks), len(sizes)),...  30.7 us
    all_to_all x4, starting transfers between devices, exchange(): return lax.all_to_all(tiles, EP, 0, 0, tiled=True).reshape(rows.shape)  30.1 us
    ppermute x22, starting transfers between devices, shift(): lax.ppermute(value, 'tp', [(i, (i + by) % size) for i in range(size)])  28.7 us
    pallas_call x2, Pallas kernels, expert_kept(): pl.pallas_call(functools.partial(kept_kernel, len(blocks)), in_specs=[VME...  15.2 us
    pallas_call x1, Pallas kernels, select_late(): pl.pallas_call(select_kernel, in_specs=[SMEM_SPEC] + [VMEM_SPEC] * (1 + l...  3.57 us
    pallas_call x1, Pallas kernels, weigh_late(): pl.pallas_call(weigh_kernel, in_specs=[SMEM_SPEC] + [VMEM_SPEC] * 3, out_...  3.55 us
  transfers between devices with their start and end apart: 26, of which 13 were waited for; matrix products, arithmetic and copies ran while one was open for 2% of the time, Pallas kernels for 33%

profile of v1, /device:TPU:0, one launch (start us, length us, event | category | flops | bytes accessed | tf_op | source)
XLA Modules:
  0.0 164.4 jit_solution(14689541228962190240)
XLA Ops:
  0.0 2.7 %shard_map.73 = (bf16[128,2048]{1,0:T(8,128)(2,1)S(1)}, bf16[256,2048]{1,0:T(8,128)(2,1)}) custom-call(s32[1]{0:T(128)} %bitcast.me, bf16[128,2048]{1,0:T(8,128)(2,1)} %tokens.1, f32[1,2048]{1,0:T(1,128)} %bitcast.25, s32[2,512]{1,0:T(2,128)} %bitcast.18), custom_call_target="tpu_custom_call" | custom-call | flops 134217728 | bytes 2097152 | tf_op jit(solution)/shard_map/pallas_call | solution.py:98
  2.7 8.4 %all-to-all-start = ((bf16[32,8,2048]{2,1,0:T(8,128)(2,1)}), bf16[32,8,2048]{2,1,0:T(8,128)(2,1)S(1)}, u32[]{:S(2)}, u32[]{:S(2)}) async-start(bf16[32,8,2048]{2,1,0:T(8,128)(2,1)} %bitcast.4), calls=%async_computation | async-start | bytes 2097152 | tf_op jit(solution)/shard_map/all_to_all | solution.py:125
  11.2 2.8 %collective-permute-start.1 = (bf16[128,2048]{1,0:T(8,128)(2,1)S(1)}, bf16[128,2048]{1,0:T(8,128)(2,1)S(1)}, u32[]{:S(2)}, u32[]{:S(2)}) collective-permute-start(bf16[128,2048]{1,0:T(8,128)(2,1)S(1)} %get-tuple-element.62.refs_0_), channel_id=1, source_target_pairs={{0,3},{1,0},{2,1},{3,2},{4,7},{5,4},{6,5},{7,6},{8,11},{9,8},{10,9... | collective-permute-start | bytes 1572872 | tf_op jit(solution)/shard_map/ppermute | solution.py:119
  14.0 11.6 %collective-permute-done.1.refs_2_ = bf16[128,2048]{1,0:T(8,128)(2,1)S(1)} collective-permute-done((bf16[128,2048]{1,0:T(8,128)(2,1)S(1)}, bf16[128,2048]{1,0:T(8,128)(2,1)S(1)}, u32[]{:S(2)}, u32[]{:S(2)}) %collective-permute-start.1) | collective-permute-done | bytes 524320 | tf_op jit(solution)/shard_map/ppermute | solution.py:119
  25.7 3.8 %collective-permute-start.3 = (bf16[64,2048]{1,0:T(8,128)(2,1)S(1)}, bf16[64,2048]{1,0:T(8,128)(2,1)S(1)}, u32[]{:S(2)}, u32[]{:S(2)}) collective-permute-start(bf16[64,2048]{1,0:T(8,128)(2,1)S(1)} %slice.17), channel_id=1, source_target_pairs={{0,3},{1,0},{2,1},{3,2},{4,7},{5,4},{6,5},{7,6},{8,11},{9,8},{10,9... | collective-permute-start | bytes 786440 | tf_op jit(solution)/shard_map/ppermute | solution.py:119
  29.5 5.0 %collective-permute-done.3.refs_4_ = bf16[64,2048]{1,0:T(8,128)(2,1)S(1)} collective-permute-done((bf16[64,2048]{1,0:T(8,128)(2,1)S(1)}, bf16[64,2048]{1,0:T(8,128)(2,1)S(1)}, u32[]{:S(2)}, u32[]{:S(2)}) %collective-permute-start.3) | collective-permute-done | bytes 262176 | tf_op jit(solution)/shard_map/ppermute | solution.py:119
  34.6 3.5 %collective-permute-done.2.refs_3_ = bf16[64,2048]{1,0:T(8,128)(2,1)S(1)} collective-permute-done((bf16[64,2048]{1,0:T(8,128)(2,1)S(1)}, bf16[64,2048]{1,0:T(8,128)(2,1)S(1)}, u32[]{:S(2)}, u32[]{:S(2)}) %collective-permute-start.2) | collective-permute-done | bytes 262176 | tf_op jit(solution)/shard_map/ppermute | solution.py:119
  39.4 1.8 %collective-permute-start.6 = (bf16[128,2048]{1,0:T(8,128)(2,1)}, bf16[128,2048]{1,0:T(8,128)(2,1)S(1)}, u32[]{:S(2)}, u32[]{:S(2)}) collective-permute-start(bf16[128,2048]{1,0:T(8,128)(2,1)} %get-tuple-element.80), channel_id=1, source_target_pairs={{0,1},{1,2},{2,3},{3,0},{4,5},{5,6},{6,7},{7,4},{8,9},{9,10},{10,1... | collective-permute-start | bytes 1572872 | tf_op jit(solution)/shard_map/ppermute | solution.py:119
  41.2 3.2 %collective-permute-start.5 = (bf16[128,2048]{1,0:T(8,128)(2,1)}, bf16[128,2048]{1,0:T(8,128)(2,1)}, u32[]{:S(2)}, u32[]{:S(2)}) collective-permute-start(bf16[128,2048]{1,0:T(8,128)(2,1)} %get-tuple-element.80), channel_id=1, source_target_pairs={{0,3},{1,0},{2,1},{3,2},{4,7},{5,4},{6,5},{7,6},{8,11},{9,8},{10,9... | collective-permute-start | bytes 1572872 | tf_op jit(solution)/shard_map/ppermute | solution.py:119
  44.4 3.6 %shard_map.78 = bf16[256,2048]{1,0:T(8,128)(2,1)} custom-call(s32[1]{0:T(128)} %bitcast.me, s32[2,512]{1,0:T(2,128)S(1)} %bitcast.19, bf16[128,2048]{1,0:T(8,128)(2,1)} %copy-done.3, bf16[128,2048]{1,0:T(8,128)(2,1)} %copy-done.9, bf16[128,2048]{1,0:T(8,128)(2,1)} %copy-done.8, bf16[64,2048]{1,0:T(8,128)(2,1)} %copy-done.11, bf16[64,2048]{1,0:T(8,128)(2,1)} %copy-done.10), custom_call_target="tpu_custom_call" | custom-call | flops 536870912 | bytes 3145728 | tf_op jit(solution)/shard_map/pallas_call | solution.py:315
  48.0 7.1 %all-to-all-start.1 = ((bf16[32,8,2048]{2,1,0:T(8,128)(2,1)}), bf16[32,8,2048]{2,1,0:T(8,128)(2,1)S(1)}, u32[]{:S(2)}, u32[]{:S(2)}) async-start(bf16[32,8,2048]{2,1,0:T(8,128)(2,1)} %bitcast.6), calls=%async_computation.1 | async-start | bytes 2097152 | tf_op jit(solution)/shard_map/all_to_all | solution.py:125
  55.6 10.2 %shard_map.74 = (bf16[128,2048]{1,0:T(8,128)(2,1)}, bf16[128,2048]{1,0:T(8,128)(2,1)}, bf16[2048,1792]{1,0:T(8,128)(2,1)S(1)}, bf16[2048,1792]{1,0:T(8,128)(2,1)S(1)}, bf16[1792,2048]{1,0:T(8,128)(2,1)S(1)}) custom-call(bf16[128,2048]{1,0:T(8,128)(2,1)S(1)} %collective-permute-done.6.refs_0_, bf16[128,2048]{1,0:T(8,128)(2,1)S(1)} %collective-permute-done.7.refs_1_, ...), custom_call_target="tpu_custom_call" | custom-call | flops 5637144576 | bytes 24117248 | tf_op jit(solution)/shard_map/pallas_call | solution.py:274
  66.0 2.0 %collective-permute-start.10 = (bf16[128,2048]{1,0:T(8,128)(2,1)S(1)}, bf16[128,2048]{1,0:T(8,128)(2,1)S(1)}, u32[]{:S(2)}, u32[]{:S(2)}) collective-permute-start(bf16[128,2048]{1,0:T(8,128)(2,1)S(1)} %collective-permute-done.6.refs_0_), channel_id=1, source_target_pairs={{0,1},{1,2},{2,3},{3,0},{4,5},{5,6},{6,7},{7,4},{8,9},{9,10},{10,1... | collective-permute-start | bytes 1572872 | tf_op jit(solution)/shard_map/ppermute | solution.py:119
  68.0 8.2 %shard_map.75 = (bf16[128,2048]{1,0:T(8,128)(2,1)}, bf16[128,2048]{1,0:T(8,128)(2,1)}) custom-call(bf16[128,2048]{1,0:T(8,128)(2,1)} %collective-permute-done.4.refs_0_, bf16[128,2048]{1,0:T(8,128)(2,1)} %collective-permute-done.5.refs_1_, bf16[2048,1792]{1,0:T(8,128)(2,1)S(1)} %get-tuple-element.49.refs_2_, ...), custom_call_target="tpu_custom_call" | custom-call | flops 5637144576 | bytes 2097152 | tf_op jit(solution)/shard_map/pallas_call | solution.py:290
  76.7 2.7 %collective-permute-start.9 = (bf16[128,2048]{1,0:T(8,128)(2,1)}, bf16[128,2048]{1,0:T(8,128)(2,1)}, u32[]{:S(2)}, u32[]{:S(2)}) collective-permute-start(bf16[128,2048]{1,0:T(8,128)(2,1)} %get-tuple-element.53), channel_id=1, source_target_pairs={{0,3},{1,0},{2,1},{3,2},{4,7},{5,4},{6,5},{7,6},{8,11},{9,8},{10,9... | collective-permute-start | bytes 1572872 | tf_op jit(solution)/shard_map/ppermute | solution.py:119
  82.2 7.0 %shard_map.76 = (bf16[128,2048]{1,0:T(8,128)(2,1)}, bf16[128,2048]{1,0:T(8,128)(2,1)}) custom-call(bf16[128,2048]{1,0:T(8,128)(2,1)S(1)} %collective-permute-done.10.refs_0_, bf16[128,2048]{1,0:T(8,128)(2,1)S(1)} %collective-permute-done.11.refs_1_, bf16[2048,1792]{1,0:T(8,128)(2,1)S(1)} %get-tuple-element.49.refs_2_, ...), custom_call_target="tpu_custom_call" | custom-call | flops 5637144576 | bytes 2097152 | tf_op jit(solution)/shard_map/pallas_call | solution.py:290
  89.2 2.0 %collective-permute-start.13 = (bf16[128,2048]{1,0:T(8,128)(2,1)}, bf16[128,2048]{1,0:T(8,128)(2,1)}, u32[]{:S(2)}, u32[]{:S(2)}) collective-permute-start(bf16[128,2048]{1,0:T(8,128)(2,1)} %get-tuple-element.59), channel_id=1, source_target_pairs={{0,1},{1,2},{2,3},{3,0},{4,5},{5,6},{6,7},{7,4},{8,9},{9,10},{10,1... | collective-permute-start | bytes 1572872 | tf_op jit(solution)/shard_map/ppermute | solution.py:119
  91.2 10.3 %shard_map.79 = bf16[256,2048]{1,0:T(8,128)(2,1)} custom-call(bf16[256,2048]{1,0:T(8,128)(2,1)S(1)} %bitcast.15, bf16[1,2048,1792]{2,1,0:T(8,128)(2,1)} %refs_1_.3, bf16[1,2048,1792]{2,1,0:T(8,128)(2,1)} %refs_2_.5, bf16[1,1792,2048]{2,1,0:T(8,128)(2,1)} %refs_3_.5), custom_call_target="tpu_custom_call" | custom-call | flops 5637144576 | bytes 24117248 | tf_op jit(solution)/shard_map/pallas_call | solution.py:274
  101.5 7.2 %all-to-all-start.3 = ((bf16[32,8,2048]{2,1,0:T(8,128)(2,1)}), bf16[32,8,2048]{2,1,0:T(8,128)(2,1)S(1)}, u32[]{:S(2)}, u32[]{:S(2)}) async-start(bf16[32,8,2048]{2,1,0:T(8,128)(2,1)} %bitcast.24), calls=%async_computation.3 | async-start | bytes 2097152 | tf_op jit(solution)/shard_map/all_to_all | solution.py:125
  112.3 10.2 %shard_map.80 = bf16[256,2048]{1,0:T(8,128)(2,1)} custom-call(bf16[256,2048]{1,0:T(8,128)(2,1)S(1)} %bitcast.14, bf16[1,2048,1792]{2,1,0:T(8,128)(2,1)} %refs_1_.3, bf16[1,2048,1792]{2,1,0:T(8,128)(2,1)} %refs_2_.5, bf16[1,1792,2048]{2,1,0:T(8,128)(2,1)} %refs_3_.5), custom_call_target="tpu_custom_call" | custom-call | flops 5637144576 | bytes 24117248 | tf_op jit(solution)/shard_map/pallas_call | solution.py:274
  122.6 1.8 %collective-permute-done.14 = bf16[128,2048]{1,0:T(8,128)(2,1)S(1)} collective-permute-done((bf16[128,2048]{1,0:T(8,128)(2,1)S(1)}, bf16[128,2048]{1,0:T(8,128)(2,1)S(1)}, u32[]{:S(2)}, u32[]{:S(2)}) %collective-permute-start.14) | collective-permute-done | bytes 524320 | tf_op jit(solution)/shard_map/ppermute | solution.py:119
  124.4 2.1 %collective-permute-done.15 = bf16[128,2048]{1,0:T(8,128)(2,1)S(1)} collective-permute-done((bf16[128,2048]{1,0:T(8,128)(2,1)S(1)}, bf16[128,2048]{1,0:T(8,128)(2,1)S(1)}, u32[]{:S(2)}, u32[]{:S(2)}) %collective-permute-start.15) | collective-permute-done | bytes 524320 | tf_op jit(solution)/shard_map/ppermute | solution.py:119
  126.6 3.1 %fusion = bf16[32,8,2048]{2,1,0:T(8,128)(2,1)} fusion(bf16[256,2048]{1,0:T(8,128)(2,1)} %shard_map.80, bf16[128,2048]{1,0:T(8,128)(2,1)} %collective-permute-done.9, bf16[128,2048]{1,0:T(8,128)(2,1)} %collective-permute-done.8, bf16[128,2048]{1,0:T(8,128)(2,1)S(1)} %collective-permute-done.15, bf16[128,2048]{1,0:T(8,128)(2,1)S(1)} %collective-permute-done.14), kind=kLoop, calls=%fused_computation.1 | loop fusion | flops 6291456 | bytes 4194304 | tf_op jit(solution)/shard_map/reshape | solution.py:124
  129.6 7.4 %all-to-all-start.2 = ((bf16[32,8,2048]{2,1,0:T(8,128)(2,1)}), bf16[32,8,2048]{2,1,0:T(8,128)(2,1)S(1)}, u32[]{:S(2)}, u32[]{:S(2)}) async-start(bf16[32,8,2048]{2,1,0:T(8,128)(2,1)} %fusion), calls=%async_computation.2 | async-start | bytes 2097152 | tf_op jit(solution)/shard_map/all_to_all | solution.py:125
  137.0 3.5 %shard_map.81 = (bf16[128,2048]{1,0:T(8,128)(2,1)}, bf16[64,2048]{1,0:T(8,128)(2,1)}, bf16[64,2048]{1,0:T(8,128)(2,1)}, bf16[64,2048]{1,0:T(8,128)(2,1)}, bf16[6...) custom-call(s32[1]{0:T(128)} %bitcast.me, s32[2,512]{1,0:T(2,128)S(1)} %bitcast.20, ...), custom_call_target="tpu_custom_call" | custom-call | flops 1073741824 | bytes 3145728 | tf_op jit(solution)/shard_map/pallas_call | solution.py:341
  140.8 1.7 %collective-permute-start.19 = (bf16[64,2048]{1,0:T(8,128)(2,1)}, bf16[64,2048]{1,0:T(8,128)(2,1)S(1)}, u32[]{:S(2)}, u32[]{:S(2)}) collective-permute-start(bf16[64,2048]{1,0:T(8,128)(2,1)} %get-tuple-element.76), channel_id=1, source_target_pairs={{0,1},{1,2},{2,3},{3,0},{4,5},{5,6},{6,7},{7,4},{8,9},{9,10},{10,1... | collective-permute-start | bytes 786440 | tf_op jit(solution)/shard_map/ppermute | solution.py:119
  142.6 3.2 %collective-permute-start.17 = (bf16[64,2048]{1,0:T(8,128)(2,1)}, bf16[64,2048]{1,0:T(8,128)(2,1)S(1)}, u32[]{:S(2)}, u32[]{:S(2)}) collective-permute-start(bf16[64,2048]{1,0:T(8,128)(2,1)} %get-tuple-element.72), channel_id=1, source_target_pairs={{0,3},{1,0},{2,1},{3,2},{4,7},{5,4},{6,5},{7,6},{8,11},{9,8},{10,9... | collective-permute-start | bytes 786440 | tf_op jit(solution)/shard_map/ppermute | solution.py:119
  145.8 4.1 %collective-permute-done.18.b = bf16[64,2048]{1,0:T(8,128)(2,1)S(1)} collective-permute-done((bf16[64,2048]{1,0:T(8,128)(2,1)}, bf16[64,2048]{1,0:T(8,128)(2,1)S(1)}, u32[]{:S(2)}, u32[]{:S(2)}) %collective-permute-start.18) | collective-permute-done | bytes 262176 | tf_op jit(solution)/shard_map/ppermute | solution.py:119
  149.9 1.5 collective-permute-done.19.d
  153.5 2.0 %collective-permute-start.21 = (bf16[64,2048]{1,0:T(8,128)(2,1)S(1)}, bf16[64,2048]{1,0:T(8,128)(2,1)S(1)}, u32[]{:S(2)}, u32[]{:S(2)}) collective-permute-start(bf16[64,2048]{1,0:T(8,128)(2,1)S(1)} %get-tuple-element.78), channel_id=1, source_target_pairs={{0,1},{1,2},{2,3},{3,0},{4,5},{5,6},{6,7},{7,4},{8,9},{9,10},{10,1... | collective-permute-start | bytes 786440 | tf_op jit(solution)/shard_map/ppermute | solution.py:119
  156.4 4.1 %collective-permute-done.20.far_a = bf16[64,2048]{1,0:T(8,128)(2,1)S(1)} collective-permute-done((bf16[64,2048]{1,0:T(8,128)(2,1)S(1)}, bf16[64,2048]{1,0:T(8,128)(2,1)S(1)}, u32[]{:S(2)}, u32[]{:S(2)}) %collective-permute-start.20) | collective-permute-done | bytes 262176 | tf_op jit(solution)/shard_map/ppermute | solution.py:119
  162.7 1.7 %shard_map.83 = bf16[128,2048]{1,0:T(8,128)(2,1)} custom-call(s32[1]{0:T(128)} %bitcast.me, s32[2,512]{1,0:T(2,128)S(1)} %bitcast.21, f32[2,512]{1,0:T(2,128)S(1)} %bitcast.23, bf16[256,2048]{1,0:T(8,128)(2,1)S(1)} %bitcast.16, bf16[128,2048]{1,0:T(8,128)(2,1)S(1)} %copy-done.2, bf16[64,2048]{1,0:T(8,128)(2,1)S(1)} %collective-permute-done.16.near_a, ...), custom_call_target="tpu_custom_call" | custom-call | flops 268435456 | bytes 3145728 | tf_op jit(solution)/shard_map/pallas_call | solution.py:366
  (59 shorter events, 14.6 us)
Async XLA Ops:
  2.7 36.4 %copy-start.3 = (bf16[128,2048]{1,0:T(8,128)(2,1)}, bf16[128,2048]{1,0:T(8,128)(2,1)S(1)}, u32[]{:S(2)}) copy-start(bf16[128,2048]{1,0:T(8,128)(2,1)S(1)} %get-tuple-element.62.refs_0_) | copy-start | bytes 1572868
  2.7 35.4 %all-to-all-start = ((bf16[32,8,2048]{2,1,0:T(8,128)(2,1)}), bf16[32,8,2048]{2,1,0:T(8,128)(2,1)S(1)}, u32[]{:S(2)}, u32[]{:S(2)}) async-start(bf16[32,8,2048]{2,1,0:T(8,128)(2,1)} %bitcast.4), calls=%async_computation | async-start | bytes 2097152 | tf_op jit(solution)/shard_map/all_to_all | solution.py:125
  11.2 33.2 %copy-start.6 = (s32[512,2]{0,1:T(2,128)S(1)}, s32[512,2]{0,1:T(2,128)}, u32[]{:S(2)}) copy-start(s32[512,2]{0,1:T(2,128)} %param.9) | copy-start | bytes 12292
  11.2 14.4 %collective-permute-start.1 = (bf16[128,2048]{1,0:T(8,128)(2,1)S(1)}, bf16[128,2048]{1,0:T(8,128)(2,1)S(1)}, u32[]{:S(2)}, u32[]{:S(2)}) collective-permute-start(bf16[128,2048]{1,0:T(8,128)(2,1)S(1)} %get-tuple-element.62.refs_0_), channel_id=1, source_target_pairs={{0,3},{1,0},{2,1},{3,2},{4,7},{5,4},{6,5},{7,6},{8,11},{9,8},{10,9... | collective-permute-start | bytes 1572872 | tf_op jit(solution)/shard_map/ppermute | solution.py:119
  14.0 15.4 %collective-permute-start = (bf16[128,2048]{1,0:T(8,128)(2,1)S(1)}, bf16[128,2048]{1,0:T(8,128)(2,1)S(1)}, u32[]{:S(2)}, u32[]{:S(2)}) collective-permute-start(bf16[128,2048]{1,0:T(8,128)(2,1)S(1)} %get-tuple-element.62.refs_0_), channel_id=1, source_target_pairs={{0,1},{1,2},{2,3},{3,0},{4,5},{5,6},{6,7},{7,4},{8,9},{9,10},{10,1... | collective-permute-start | bytes 1572872 | tf_op jit(solution)/shard_map/ppermute | solution.py:119
  25.6 8.9 %copy-start.8 = (bf16[128,2048]{1,0:T(8,128)(2,1)}, bf16[128,2048]{1,0:T(8,128)(2,1)S(1)}, u32[]{:S(2)}) copy-start(bf16[128,2048]{1,0:T(8,128)(2,1)S(1)} %collective-permute-done.1.refs_2_) | copy-start | bytes 1572868
  25.7 8.9 %collective-permute-start.3 = (bf16[64,2048]{1,0:T(8,128)(2,1)S(1)}, bf16[64,2048]{1,0:T(8,128)(2,1)S(1)}, u32[]{:S(2)}, u32[]{:S(2)}) collective-permute-start(bf16[64,2048]{1,0:T(8,128)(2,1)S(1)} %slice.17), channel_id=1, source_target_pairs={{0,3},{1,0},{2,1},{3,2},{4,7},{5,4},{6,5},{7,6},{8,11},{9,8},{10,9... | collective-permute-start | bytes 786440 | tf_op jit(solution)/shard_map/ppermute | solution.py:119
  29.4 8.6 %collective-permute-start.2 = (bf16[64,2048]{1,0:T(8,128)(2,1)S(1)}, bf16[64,2048]{1,0:T(8,128)(2,1)S(1)}, u32[]{:S(2)}, u32[]{:S(2)}) collective-permute-start(bf16[64,2048]{1,0:T(8,128)(2,1)S(1)} %slice.16), channel_id=1, source_target_pairs={{0,1},{1,2},{2,3},{3,0},{4,5},{5,6},{6,7},{7,4},{8,9},{9,10},{10,1... | collective-permute-start | bytes 786440 | tf_op jit(solution)/shard_map/ppermute | solution.py:119
  34.6 9.8 %copy-start.10 = (bf16[64,2048]{1,0:T(8,128)(2,1)}, bf16[64,2048]{1,0:T(8,128)(2,1)S(1)}, u32[]{:S(2)}) copy-start(bf16[64,2048]{1,0:T(8,128)(2,1)S(1)} %collective-permute-done.3.refs_4_) | copy-start | bytes 786436
  39.1 15.9 %collective-permute-start.7 = (bf16[128,2048]{1,0:T(8,128)(2,1)}, bf16[128,2048]{1,0:T(8,128)(2,1)S(1)}, u32[]{:S(2)}, u32[]{:S(2)}) collective-permute-start(bf16[128,2048]{1,0:T(8,128)(2,1)} %get-tuple-element.79), channel_id=1, source_target_pairs={{0,3},{1,0},{2,1},{3,2},{4,7},{5,4},{6,5},{7,6},{8,11},{9,8},{10,9... | collective-permute-start | bytes 1572872 | tf_op jit(solution)/shard_map/ppermute | solution.py:119
  39.4 16.2 %collective-permute-start.6 = (bf16[128,2048]{1,0:T(8,128)(2,1)}, bf16[128,2048]{1,0:T(8,128)(2,1)S(1)}, u32[]{:S(2)}, u32[]{:S(2)}) collective-permute-start(bf16[128,2048]{1,0:T(8,128)(2,1)} %get-tuple-element.80), channel_id=1, source_target_pairs={{0,1},{1,2},{2,3},{3,0},{4,5},{5,6},{6,7},{7,4},{8,9},{9,10},{10,1... | collective-permute-start | bytes 1572872 | tf_op jit(solution)/shard_map/ppermute | solution.py:119
  41.2 24.7 %collective-permute-start.4 = (bf16[128,2048]{1,0:T(8,128)(2,1)}, bf16[128,2048]{1,0:T(8,128)(2,1)}, u32[]{:S(2)}, u32[]{:S(2)}) collective-permute-start(bf16[128,2048]{1,0:T(8,128)(2,1)} %get-tuple-element.79), channel_id=1, source_target_pairs={{0,1},{1,2},{2,3},{3,0},{4,5},{5,6},{6,7},{7,4},{8,9},{9,10},{10,1... | collective-permute-start | bytes 1572872 | tf_op jit(solution)/shard_map/ppermute | solution.py:119
  41.2 24.7 %collective-permute-start.5 = (bf16[128,2048]{1,0:T(8,128)(2,1)}, bf16[128,2048]{1,0:T(8,128)(2,1)}, u32[]{:S(2)}, u32[]{:S(2)}) collective-permute-start(bf16[128,2048]{1,0:T(8,128)(2,1)} %get-tuple-element.80), channel_id=1, source_target_pairs={{0,3},{1,0},{2,1},{3,2},{4,7},{5,4},{6,5},{7,6},{8,11},{9,8},{10,9... | collective-permute-start | bytes 1572872 | tf_op jit(solution)/shard_map/ppermute | solution.py:119
  48.0 43.2 %all-to-all-start.1 = ((bf16[32,8,2048]{2,1,0:T(8,128)(2,1)}), bf16[32,8,2048]{2,1,0:T(8,128)(2,1)S(1)}, u32[]{:S(2)}, u32[]{:S(2)}) async-start(bf16[32,8,2048]{2,1,0:T(8,128)(2,1)} %bitcast.6), calls=%async_computation.1 | async-start | bytes 2097152 | tf_op jit(solution)/shard_map/all_to_all | solution.py:125
  65.9 14.9 %collective-permute-start.11 = (bf16[128,2048]{1,0:T(8,128)(2,1)S(1)}, bf16[128,2048]{1,0:T(8,128)(2,1)S(1)}, u32[]{:S(2)}, u32[]{:S(2)}) collective-permute-start(bf16[128,2048]{1,0:T(8,128)(2,1)S(1)} %collective-permute-done.7.refs_1_), channel_id=1, source_target_pairs={{0,3},{1,0},{2,1},{3,2},{4,7},{5,4},{6,5},{7,6},{8,11},{9,8},{10,9... | collective-permute-start | bytes 1572872 | tf_op jit(solution)/shard_map/ppermute | solution.py:119
  66.0 16.3 %collective-permute-start.10 = (bf16[128,2048]{1,0:T(8,128)(2,1)S(1)}, bf16[128,2048]{1,0:T(8,128)(2,1)S(1)}, u32[]{:S(2)}, u32[]{:S(2)}) collective-permute-start(bf16[128,2048]{1,0:T(8,128)(2,1)S(1)} %collective-permute-done.6.refs_0_), channel_id=1, source_target_pairs={{0,1},{1,2},{2,3},{3,0},{4,5},{5,6},{6,7},{7,4},{8,9},{9,10},{10,1... | collective-permute-start | bytes 1572872 | tf_op jit(solution)/shard_map/ppermute | solution.py:119
  76.2 46.4 %collective-permute-start.8 = (bf16[128,2048]{1,0:T(8,128)(2,1)}, bf16[128,2048]{1,0:T(8,128)(2,1)}, u32[]{:S(2)}, u32[]{:S(2)}) collective-permute-start(bf16[128,2048]{1,0:T(8,128)(2,1)} %get-tuple-element.52), channel_id=1, source_target_pairs={{0,1},{1,2},{2,3},{3,0},{4,5},{5,6},{6,7},{7,4},{8,9},{9,10},{10,1... | collective-permute-start | bytes 1572872 | tf_op jit(solution)/shard_map/ppermute | solution.py:119
  76.7 45.9 %collective-permute-start.9 = (bf16[128,2048]{1,0:T(8,128)(2,1)}, bf16[128,2048]{1,0:T(8,128)(2,1)}, u32[]{:S(2)}, u32[]{:S(2)}) collective-permute-start(bf16[128,2048]{1,0:T(8,128)(2,1)} %get-tuple-element.53), channel_id=1, source_target_pairs={{0,3},{1,0},{2,1},{3,2},{4,7},{5,4},{6,5},{7,6},{8,11},{9,8},{10,9... | collective-permute-start | bytes 1572872 | tf_op jit(solution)/shard_map/ppermute | solution.py:119
  89.2 19.6 %collective-permute-start.12 = (bf16[128,2048]{1,0:T(8,128)(2,1)}, bf16[128,2048]{1,0:T(8,128)(2,1)}, u32[]{:S(2)}, u32[]{:S(2)}) collective-permute-start(bf16[128,2048]{1,0:T(8,128)(2,1)} %get-tuple-element.57), channel_id=1, source_target_pairs={{0,3},{1,0},{2,1},{3,2},{4,7},{5,4},{6,5},{7,6},{8,11},{9,8},{10,9... | collective-permute-start | bytes 1572872 | tf_op jit(solution)/shard_map/ppermute | solution.py:119
  89.2 19.6 %collective-permute-start.13 = (bf16[128,2048]{1,0:T(8,128)(2,1)}, bf16[128,2048]{1,0:T(8,128)(2,1)}, u32[]{:S(2)}, u32[]{:S(2)}) collective-permute-start(bf16[128,2048]{1,0:T(8,128)(2,1)} %get-tuple-element.59), channel_id=1, source_target_pairs={{0,1},{1,2},{2,3},{3,0},{4,5},{5,6},{6,7},{7,4},{8,9},{9,10},{10,1... | collective-permute-start | bytes 1572872 | tf_op jit(solution)/shard_map/ppermute | solution.py:119
  101.5 7.3 %copy-start = (bf16[128,2048]{1,0:T(8,128)(2,1)S(1)}, bf16[128,2048]{1,0:T(8,128)(2,1)}, u32[]{:S(2)}) copy-start(bf16[128,2048]{1,0:T(8,128)(2,1)} %get-tuple-element.54.a) | copy-start | bytes 1572868
  101.5 28.1 %all-to-all-start.3 = ((bf16[32,8,2048]{2,1,0:T(8,128)(2,1)}), bf16[32,8,2048]{2,1,0:T(8,128)(2,1)S(1)}, u32[]{:S(2)}, u32[]{:S(2)}) async-start(bf16[32,8,2048]{2,1,0:T(8,128)(2,1)} %bitcast.24), calls=%async_computation.3 | async-start | bytes 2097152 | tf_op jit(solution)/shard_map/all_to_all | solution.py:125
  110.2 14.2 %collective-permute-start.14 = (bf16[128,2048]{1,0:T(8,128)(2,1)S(1)}, bf16[128,2048]{1,0:T(8,128)(2,1)S(1)}, u32[]{:S(2)}, u32[]{:S(2)}) collective-permute-start(bf16[128,2048]{1,0:T(8,128)(2,1)S(1)} %get-tuple-element.60), channel_id=1, source_target_pairs={{0,3},{1,0},{2,1},{3,2},{4,7},{5,4},{6,5},{7,6},{8,11},{9,8},{10,9... | collective-permute-start | bytes 1572872 | tf_op jit(solution)/shard_map/ppermute | solution.py:119
  111.5 15.0 %collective-permute-start.15 = (bf16[128,2048]{1,0:T(8,128)(2,1)S(1)}, bf16[128,2048]{1,0:T(8,128)(2,1)S(1)}, u32[]{:S(2)}, u32[]{:S(2)}) collective-permute-start(bf16[128,2048]{1,0:T(8,128)(2,1)S(1)} %get-tuple-element.61), channel_id=1, source_target_pairs={{0,1},{1,2},{2,3},{3,0},{4,5},{5,6},{6,7},{7,4},{8,9},{9,10},{10,1... | collective-permute-start | bytes 1572872 | tf_op jit(solution)/shard_map/ppermute | solution.py:119
  129.6 7.4 %copy-start.7 = (f32[512,2]{0,1:T(2,128)S(1)}, f32[512,2]{0,1:T(2,128)}, u32[]{:S(2)}) copy-start(f32[512,2]{0,1:T(2,128)} %param.10) | copy-start | bytes 12292
  129.6 32.1 %all-to-all-start.2 = ((bf16[32,8,2048]{2,1,0:T(8,128)(2,1)}), bf16[32,8,2048]{2,1,0:T(8,128)(2,1)S(1)}, u32[]{:S(2)}, u32[]{:S(2)}) async-start(bf16[32,8,2048]{2,1,0:T(8,128)(2,1)} %fusion), calls=%async_computation.2 | async-start | bytes 2097152 | tf_op jit(solution)/shard_map/all_to_all | solution.py:125
  140.6 9.4 %collective-permute-start.18 = (bf16[64,2048]{1,0:T(8,128)(2,1)}, bf16[64,2048]{1,0:T(8,128)(2,1)S(1)}, u32[]{:S(2)}, u32[]{:S(2)}) collective-permute-start(bf16[64,2048]{1,0:T(8,128)(2,1)} %get-tuple-element.74), channel_id=1, source_target_pairs={{0,3},{1,0},{2,1},{3,2},{4,7},{5,4},{6,5},{7,6},{8,11},{9,8},{10,9... | collective-permute-start | bytes 786440 | tf_op jit(solution)/shard_map/ppermute | solution.py:119
  140.8 10.6 %collective-permute-start.19 = (bf16[64,2048]{1,0:T(8,128)(2,1)}, bf16[64,2048]{1,0:T(8,128)(2,1)S(1)}, u32[]{:S(2)}, u32[]{:S(2)}) collective-permute-start(bf16[64,2048]{1,0:T(8,128)(2,1)} %get-tuple-element.76), channel_id=1, source_target_pairs={{0,1},{1,2},{2,3},{3,0},{4,5},{5,6},{6,7},{7,4},{8,9},{9,10},{10,1... | collective-permute-start | bytes 786440 | tf_op jit(solution)/shard_map/ppermute | solution.py:119
  142.6 13.8 %collective-permute-start.16 = (bf16[64,2048]{1,0:T(8,128)(2,1)}, bf16[64,2048]{1,0:T(8,128)(2,1)S(1)}, u32[]{:S(2)}, u32[]{:S(2)}) collective-permute-start(bf16[64,2048]{1,0:T(8,128)(2,1)} %get-tuple-element.71), channel_id=1, source_target_pairs={{0,1},{1,2},{2,3},{3,0},{4,5},{5,6},{6,7},{7,4},{8,9},{9,10},{10,1... | collective-permute-start | bytes 786440 | tf_op jit(solution)/shard_map/ppermute | solution.py:119
  142.6 13.8 %collective-permute-start.17 = (bf16[64,2048]{1,0:T(8,128)(2,1)}, bf16[64,2048]{1,0:T(8,128)(2,1)S(1)}, u32[]{:S(2)}, u32[]{:S(2)}) collective-permute-start(bf16[64,2048]{1,0:T(8,128)(2,1)} %get-tuple-element.72), channel_id=1, source_target_pairs={{0,3},{1,0},{2,1},{3,2},{4,7},{5,4},{6,5},{7,6},{8,11},{9,8},{10,9... | collective-permute-start | bytes 786440 | tf_op jit(solution)/shard_map/ppermute | solution.py:119
  153.5 7.0 %collective-permute-start.20 = (bf16[64,2048]{1,0:T(8,128)(2,1)S(1)}, bf16[64,2048]{1,0:T(8,128)(2,1)S(1)}, u32[]{:S(2)}, u32[]{:S(2)}) collective-permute-start(bf16[64,2048]{1,0:T(8,128)(2,1)S(1)} %get-tuple-element.77), channel_id=1, source_target_pairs={{0,3},{1,0},{2,1},{3,2},{4,7},{5,4},{6,5},{7,6},{8,11},{9,8},{10,9... | collective-permute-start | bytes 786440 | tf_op jit(solution)/shard_map/ppermute | solution.py:119
  153.5 8.2 %collective-permute-start.21 = (bf16[64,2048]{1,0:T(8,128)(2,1)S(1)}, bf16[64,2048]{1,0:T(8,128)(2,1)S(1)}, u32[]{:S(2)}, u32[]{:S(2)}) collective-permute-start(bf16[64,2048]{1,0:T(8,128)(2,1)S(1)} %get-tuple-element.78), channel_id=1, source_target_pairs={{0,1},{1,2},{2,3},{3,0},{4,5},{5,6},{6,7},{7,4},{8,9},{9,10},{10,1... | collective-permute-start | bytes 786440 | tf_op jit(solution)/shard_map/ppermute | solution.py:119
  (6 other events, 16.7 us)

commit v2 on v1

--- a/solution.py
+++ b/solution.py
@@ -63,19 +63,18 @@
     return per_row(slots_of(hits), rows) == wanted.astype(jnp.float32)
 
 
-def weighted_sum(chosen, hits, route, block, rows):
+def weights_of(chosen, hits, route, block):
     weight = route[:, pl.ds(pl.multiple_of(block * LANES, LANES), LANES)]
     mass = jnp.where(hits[0], weight[0:1], 0.0) + jnp.where(hits[1], weight[1:2], 0.0)
     high = mass.astype(jnp.bfloat16)
     low = (mass - high.astype(jnp.float32)).astype(jnp.bfloat16)
-    total = None
-    for part in (high, low):
-        term = jnp.where(chosen, per_row(part, chosen.shape[0]), 0.0).astype(jnp.bfloat16)
-        term = lax.dot_general(
-            term, rows[...], (((0,), (0,)), ((), ())), preferred_element_type=jnp.float32
-        )
-        total = term if total is None else total + term
-    return total
+    terms = (jnp.where(chosen, per_row(t, chosen.shape[0]), 0.0) for t in (high, low))
+    return tuple(t.T.astype(jnp.bfloat16) for t in terms)
+
+
+def weighted_sum(high, low, rows):
+    value = jnp.dot(high, rows, preferred_element_type=jnp.float32)
+    return value + jnp.dot(low, rows, preferred_element_type=jnp.float32)
 
 
 def block_at(me, by):
@@ -298,61 +297,80 @@
     )(*blocks, *(pltpu.with_memory_space_constraint(w, pltpu.VMEM) for w in tiles))
 
 
-def select_kernel(me, ids, *refs):
-    blocks, out, rows, chosen = refs[:-3], refs[-3], refs[-2], refs[-1]
-    experts_all = out.shape[0] // (LATE * len(OFFSETS))
+def route_kernel(me, ids, route, late, late_high, late_low, high, low):
+    rows = late.shape[0]
+    experts_all = rows // (LATE * len(OFFSETS))
+    for at, by in enumerate(OFFSETS):
+        block = block_at(me, by)
+        hits = routed(ids, block, experts_all)
+        chosen = late_rows_of(hits, rows, at)
+        tokens = pl.ds(at * LANES, LANES)
+        late[:, tokens] = ones_where(chosen)
+        late_high[tokens, :], late_low[tokens, :] = weights_of(chosen, hits, route, block)
+        if at == 0:
+            chosen = early_rows(hits, high.shape[1])
+            high[...], low[...] = weights_of(chosen, hits, route, block)
+
+
+def route_tables(me, expert_ids, route_weight, experts_all):
+    rows, tokens = experts_all * LATE * len(OFFSETS), LANES * len(OFFSETS)
+    shapes = [(rows, tokens)] + [(tokens, rows)] * 2 + [(LANES, experts_all * EARLY)] * 2
+    return pl.pallas_call(
+        route_kernel,
+        in_specs=[SMEM_SPEC] + [VMEM_SPEC] * 2,
+        out_specs=[VMEM_SPEC] * len(shapes),
+        out_shape=[pltpu.HBM(s, jnp.bfloat16) for s in shapes],
+        compiler_params=pltpu.CompilerParams(vmem_limit_bytes=16 * MIB),
+        cost_estimate=pl.CostEstimate(
+            flops=4 * 10**9, bytes_accessed=6 * rows * tokens, transcendentals=0
+        ),
+    )(me, *in_hbm(expert_ids, route_weight))
+
+
+def select_kernel(chosen, *refs):
+    blocks, out, rows = refs[:-2], refs[-2], refs[-1]
     place(rows, blocks)
-    for at, by in enumerate(OFFSETS):
-        hits = routed(ids, block_at(me, by), experts_all)
-        chosen[:, at * LANES : (at + 1) * LANES] = ones_where(late_rows_of(hits, out.shape[0], at))
     value = jnp.dot(chosen[...], rows[...], preferred_element_type=jnp.float32)
     out[...] = value.astype(out.dtype)
 
 
-def select_late(me, expert_ids, blocks, experts_all):
+def select_late(chosen, blocks):
     d = blocks[0].shape[1]
-    n, m = experts_all * LATE * len(OFFSETS), LANES * len(OFFSETS)
+    n, m = chosen.shape
     return pl.pallas_call(
         select_kernel,
-        in_specs=[SMEM_SPEC] + [VMEM_SPEC] * (1 + len(blocks)),
+        in_specs=[VMEM_SPEC] * (1 + len(blocks)),
         out_specs=VMEM_SPEC,
-        out_shape=jax.ShapeDtypeStruct((n, d), jnp.bfloat16),
-        scratch_shapes=[pltpu.VMEM((m, d), jnp.bfloat16), pltpu.VMEM((n, m), jnp.bfloat16)],
+        out_shape=pltpu.HBM((n, d), jnp.bfloat16),
+        scratch_shapes=[pltpu.VMEM((m, d), jnp.bfloat16)],
         compiler_params=pltpu.CompilerParams(vmem_limit_bytes=16 * MIB),
         cost_estimate=pl.CostEstimate(
             flops=2 * n * m * d, bytes_accessed=2 * d * (n + m), transcendentals=0
         ),
-    )(me, expert_ids, *in_hbm(*blocks))
-
-
-def weigh_kernel(me, ids, route, rows, own, *others):
-    experts_all = rows.shape[0] // (LATE * len(OFFSETS))
-    for at, by in enumerate(OFFSETS):
-        block = block_at(me, by)
-        hits = routed(ids, block, experts_all)
-        chosen = late_rows_of(hits, rows.shape[0], at)
-        value = weighted_sum(chosen, hits, route, block, rows)
-        cut(value, [own] if at == 0 else others[2 * at - 2 : 2 * at])
-
-
-def weigh_late(me, expert_ids, route_weight, rows):
+    )(*in_hbm(chosen, *blocks))
+
+
+def weigh_kernel(high, low, rows, *outs):
+    cut(weighted_sum(high[...], low[...], rows[...]), outs)
+
+
+def weigh_late(high, low, rows):
     n, d = rows.shape
     sizes = [LANES] + [LANES // 2] * (2 * len(OFFSETS) - 2)
     return pl.pallas_call(
         weigh_kernel,
-        in_specs=[SMEM_SPEC] + [VMEM_SPEC] * 3,
+        in_specs=[VMEM_SPEC] * 3,
         out_specs=[VMEM_SPEC] * len(sizes),
         out_shape=[pltpu.HBM((s, d), jnp.bfloat16) for s in sizes],
         compiler_params=pltpu.CompilerParams(vmem_limit_bytes=16 * MIB),
         cost_estimate=pl.CostEstimate(
             flops=4 * n * LANES * len(OFFSETS) * d, bytes_accessed=6 * d * n, transcendentals=0
         ),
-    )(me, expert_ids, route_weight, rows)
-
-
-def finish_kernel(me, ids, route, rows, own, near_a, near_b, far_a, far_b, out):
-    hits = routed(ids, me[0], rows.shape[0] // EARLY)
-    value = weighted_sum(early_rows(hits, rows.shape[0]), hits, route, me[0], rows)
+    )(high, low, rows)
+
+
+def finish_kernel(high, low, rows, own, near_a, near_b, far_a, far_b, out):
+    value = weighted_sum(high[...], low[...], rows[...])
     value = value + own[...].astype(jnp.float32)
     half = out.shape[0] // 2
     top = near_a[...].astype(jnp.float32) + far_a[...].astype(jnp.float32)
@@ -361,18 +379,18 @@
     out[half:, :] = (value[half:] + bottom).astype(out.dtype)
 
 
-def finish(me, expert_ids, route_weight, rows, own, pieces):
+def finish(high, low, rows, own, pieces):
     n, d = rows.shape
     return pl.pallas_call(
         finish_kernel,
-        in_specs=[SMEM_SPEC] + [VMEM_SPEC] * 8,
+        in_specs=[VMEM_SPEC] * 8,
         out_specs=VMEM_SPEC,
         out_shape=jax.ShapeDtypeStruct((LANES, d), jnp.bfloat16),
         compiler_params=pltpu.CompilerParams(vmem_limit_bytes=16 * MIB),
         cost_estimate=pl.CostEstimate(
             flops=4 * n * LANES * d, bytes_accessed=2 * d * (n + 4 * LANES), transcendentals=0
         ),
-    )(me, expert_ids, route_weight, rows, own, *pieces)
+    )(high, low, rows, own, *pieces)
 
 
 def send_near(to_left, to_right):
@@ -400,7 +418,8 @@
     arrived = exchange(sent)
     arrived, blocks = lax.optimization_barrier((arrived, blocks))
 
-    late_sent = select_late(me, ids, blocks, experts_all)
+    late_chosen, late_high, late_low, high, low = route_tables(me, ids, route, experts_all)
+    late_sent = select_late(late_chosen, blocks)
     late_arrived = exchange(late_sent)
 
     mid = arrived.shape[0] // 2
@@ -431,12 +450,12 @@
     back = exchange(summed)
 
     late_back, _ = lax.optimization_barrier((late_back, own_part))
-    sums = weigh_late(me, ids, route, late_back)
+    sums = weigh_late(late_high, late_low, late_back)
     token_own, left_top, left_bottom, right_top, right_bottom, far_top, far_bottom = sums
     token_via = send_far(far_top, far_bottom)
     token_near = send_near(left_bottom, right_top)
     token_on = send_on(left_top, right_bottom, *token_via)
-    return finish(me, ids, route, back, token_own, token_near + token_on)
+    return finish(high, low, back, token_own, token_near + token_on)
 
 
 def solution(mesh):

time: 165 us -> 165 us (level)
    pallas_call x3 -> x4, Pallas kernels: 8.78 us -> 9.29 us  [the longest x1 3.28 us: select_late(): pl.pallas_call(select_kernel, in_specs=[VMEM_SPEC] * (1 + len(blocks)), o...]
  transfers between devices with their start and end apart: 26 -> 26, of which waited for: 13 -> 12; matrix products, arithmetic and copies ran while one was open for 2% -> 2% of each run, Pallas kernels for 33% -> 33%
where the time goes in v2:
time: 165 us
  starting transfers between devices  59.2 us (36%)
  Pallas kernels  58.9 us (36%)
  waiting for transfers between devices  39.1 us (24%)
  local copies, waits for them, and re-layouts  4.08 us (2%)
  other arithmetic  3.06 us (2%)
    ppermute x22, waiting for transfers between devices, shift(): lax.ppermute(value, 'tp', [(i, (i + by) % size) for i in range(size)])  39.1 us
    pallas_call x3, Pallas kernels, expert_streamed(): pl.pallas_call(functools.partial(stream_kernel, len(blocks), len(sizes)),...  30.5 us
    all_to_all x4, starting transfers between devices, exchange(): return lax.all_to_all(tiles, EP, 0, 0, tiled=True).reshape(rows.shape)  30.4 us
    ppermute x22, starting transfers between devices, shift(): lax.ppermute(value, 'tp', [(i, (i + by) % size) for i in range(size)])  28.8 us
    pallas_call x2, Pallas kernels, expert_kept(): pl.pallas_call(functools.partial(kept_kernel, len(blocks)), in_specs=[VME...  14.8 us
  transfers between devices with their start and end apart: 26, of which 12 were waited for; matrix products, arithmetic and copies ran while one was open for 2% of the time, Pallas kernels for 33%

profile of v2, /device:TPU:0, one launch (start us, length us, event | category | flops | bytes accessed | tf_op | source)
XLA Modules:
  0.0 164.6 jit_solution(8520721812439469319)
XLA Ops:
  0.0 2.7 %shard_map.74 = (bf16[128,2048]{1,0:T(8,128)(2,1)S(1)}, bf16[256,2048]{1,0:T(8,128)(2,1)}) custom-call(s32[1]{0:T(128)} %bitcast.me, bf16[128,2048]{1,0:T(8,128)(2,1)} %tokens.1, f32[1,2048]{1,0:T(1,128)} %bitcast.20, s32[2,512]{1,0:T(2,128)} %bitcast.21), custom_call_target="tpu_custom_call" | custom-call | flops 134217728 | bytes 2097152 | tf_op jit(solution)/shard_map/pallas_call | solution.py:97
  2.7 8.4 %all-to-all-start = ((bf16[32,8,2048]{2,1,0:T(8,128)(2,1)}), bf16[32,8,2048]{2,1,0:T(8,128)(2,1)S(1)}, u32[]{:S(2)}, u32[]{:S(2)}) async-start(bf16[32,8,2048]{2,1,0:T(8,128)(2,1)} %bitcast.4), calls=%async_computation | async-start | bytes 2097152 | tf_op jit(solution)/shard_map/all_to_all | solution.py:124
  11.2 2.8 %collective-permute-start.1 = (bf16[128,2048]{1,0:T(8,128)(2,1)S(1)}, bf16[128,2048]{1,0:T(8,128)(2,1)S(1)}, u32[]{:S(2)}, u32[]{:S(2)}) collective-permute-start(bf16[128,2048]{1,0:T(8,128)(2,1)S(1)} %get-tuple-element.70.refs_0_), channel_id=1, source_target_pairs={{0,3},{1,0},{2,1},{3,2},{4,7},{5,4},{6,5},{7,6},{8,11},{9,8},{10,9... | collective-permute-start | bytes 1572872 | tf_op jit(solution)/shard_map/ppermute | solution.py:118
  14.0 11.6 %collective-permute-done.1.refs_2_ = bf16[128,2048]{1,0:T(8,128)(2,1)S(1)} collective-permute-done((bf16[128,2048]{1,0:T(8,128)(2,1)S(1)}, bf16[128,2048]{1,0:T(8,128)(2,1)S(1)}, u32[]{:S(2)}, u32[]{:S(2)}) %collective-permute-start.1) | collective-permute-done | bytes 524320 | tf_op jit(solution)/shard_map/ppermute | solution.py:118
  25.6 3.8 %collective-permute-start.3 = (bf16[64,2048]{1,0:T(8,128)(2,1)S(1)}, bf16[64,2048]{1,0:T(8,128)(2,1)S(1)}, u32[]{:S(2)}, u32[]{:S(2)}) collective-permute-start(bf16[64,2048]{1,0:T(8,128)(2,1)S(1)} %slice.17), channel_id=1, source_target_pairs={{0,3},{1,0},{2,1},{3,2},{4,7},{5,4},{6,5},{7,6},{8,11},{9,8},{10,9... | collective-permute-start | bytes 786440 | tf_op jit(solution)/shard_map/ppermute | solution.py:118
  29.5 5.0 %collective-permute-done.3.refs_4_ = bf16[64,2048]{1,0:T(8,128)(2,1)S(1)} collective-permute-done((bf16[64,2048]{1,0:T(8,128)(2,1)S(1)}, bf16[64,2048]{1,0:T(8,128)(2,1)S(1)}, u32[]{:S(2)}, u32[]{:S(2)}) %collective-permute-start.3) | collective-permute-done | bytes 262176 | tf_op jit(solution)/shard_map/ppermute | solution.py:118
  34.6 3.6 %collective-permute-done.2.refs_3_ = bf16[64,2048]{1,0:T(8,128)(2,1)} collective-permute-done((bf16[64,2048]{1,0:T(8,128)(2,1)S(1)}, bf16[64,2048]{1,0:T(8,128)(2,1)}, u32[]{:S(2)}, u32[]{:S(2)}) %collective-permute-start.2) | collective-permute-done | bytes 262176 | tf_op jit(solution)/shard_map/ppermute | solution.py:118
  39.3 1.9 %collective-permute-start.6 = (bf16[128,2048]{1,0:T(8,128)(2,1)}, bf16[128,2048]{1,0:T(8,128)(2,1)S(1)}, u32[]{:S(2)}, u32[]{:S(2)}) collective-permute-start(bf16[128,2048]{1,0:T(8,128)(2,1)} %get-tuple-element.90), channel_id=1, source_target_pairs={{0,1},{1,2},{2,3},{3,0},{4,5},{5,6},{6,7},{7,4},{8,9},{9,10},{10,1... | collective-permute-start | bytes 1572872 | tf_op jit(solution)/shard_map/ppermute | solution.py:118
  41.3 2.3 %shard_map.73 = (bf16[256,512]{1,0:T(8,128)(2,1)}, bf16[512,256]{1,0:T(8,128)(2,1)}, bf16[512,256]{1,0:T(8,128)(2,1)}, bf16[128,256]{1,0:T(8,128)(2,1)}, bf16[128,256]{1,0:T(8,128)(2,1)}) custom-call(s32[1]{0:T(128)} %bitcast.me, s32[2,512]{1,0:T(2,128)} %bitcast.22, f32[2,512]{1,0:T(2,128)} %bitcast.23), custom_call_target="tpu_custom_call" | custom-call | flops 4000000000 | bytes 786432 | tf_op jit(solution)/shard_map/pallas_call | solution.py:318
  43.6 3.2 %collective-permute-start.5 = (bf16[128,2048]{1,0:T(8,128)(2,1)}, bf16[128,2048]{1,0:T(8,128)(2,1)}, u32[]{:S(2)}, u32[]{:S(2)}) collective-permute-start(bf16[128,2048]{1,0:T(8,128)(2,1)} %get-tuple-element.90), channel_id=1, source_target_pairs={{0,3},{1,0},{2,1},{3,2},{4,7},{5,4},{6,5},{7,6},{8,11},{9,8},{10,9... | collective-permute-start | bytes 1572872 | tf_op jit(solution)/shard_map/ppermute | solution.py:118
  46.9 3.3 %shard_map.79 = bf16[256,2048]{1,0:T(8,128)(2,1)} custom-call(bf16[256,512]{1,0:T(8,128)(2,1)} %get-tuple-element.69.chosen, bf16[128,2048]{1,0:T(8,128)(2,1)} %copy-done.3, bf16[128,2048]{1,0:T(8,128)(2,1)} %copy-done.11, bf16[128,2048]{1,0:T(8,128)(2,1)} %copy-done.10, bf16[64,2048]{1,0:T(8,128)(2,1)} %collective-permute-done.2.refs_3_, ...), custom_call_target="tpu_custom_call" | custom-call | flops 536870912 | bytes 3145728 | tf_op jit(solution)/shard_map/pallas_call | solution.py:340
  50.1 7.1 %all-to-all-start.1 = ((bf16[32,8,2048]{2,1,0:T(8,128)(2,1)}), bf16[32,8,2048]{2,1,0:T(8,128)(2,1)S(1)}, u32[]{:S(2)}, u32[]{:S(2)}) async-start(bf16[32,8,2048]{2,1,0:T(8,128)(2,1)} %bitcast.19), calls=%async_computation.1 | async-start | bytes 2097152 | tf_op jit(solution)/shard_map/all_to_all | solution.py:124
  57.3 10.1 %shard_map.75 = (bf16[128,2048]{1,0:T(8,128)(2,1)}, bf16[128,2048]{1,0:T(8,128)(2,1)}, bf16[2048,1792]{1,0:T(8,128)(2,1)S(1)}, bf16[2048,1792]{1,0:T(8,128)(2,1)S(1)}, bf16[1792,2048]{1,0:T(8,128)(2,1)S(1)}) custom-call(bf16[128,2048]{1,0:T(8,128)(2,1)S(1)} %collective-permute-done.6.refs_0_, bf16[128,2048]{1,0:T(8,128)(2,1)S(1)} %collective-permute-done.7.refs_1_, ...), custom_call_target="tpu_custom_call" | custom-call | flops 5637144576 | bytes 24117248 | tf_op jit(solution)/shard_map/pallas_call | solution.py:273
  67.6 1.9 %collective-permute-start.10 = (bf16[128,2048]{1,0:T(8,128)(2,1)S(1)}, bf16[128,2048]{1,0:T(8,128)(2,1)S(1)}, u32[]{:S(2)}, u32[]{:S(2)}) collective-permute-start(bf16[128,2048]{1,0:T(8,128)(2,1)S(1)} %collective-permute-done.6.refs_0_), channel_id=1, source_target_pairs={{0,1},{1,2},{2,3},{3,0},{4,5},{5,6},{6,7},{7,4},{8,9},{9,10},{10,1... | collective-permute-start | bytes 1572872 | tf_op jit(solution)/shard_map/ppermute | solution.py:118
  69.5 8.0 %shard_map.76 = (bf16[128,2048]{1,0:T(8,128)(2,1)}, bf16[128,2048]{1,0:T(8,128)(2,1)}) custom-call(bf16[128,2048]{1,0:T(8,128)(2,1)} %collective-permute-done.4.refs_0_, bf16[128,2048]{1,0:T(8,128)(2,1)} %collective-permute-done.5.refs_1_, bf16[2048,1792]{1,0:T(8,128)(2,1)S(1)} %get-tuple-element.56.refs_2_, ...), custom_call_target="tpu_custom_call" | custom-call | flops 5637144576 | bytes 2097152 | tf_op jit(solution)/shard_map/pallas_call | solution.py:289
  77.5 3.2 %collective-permute-start.9 = (bf16[128,2048]{1,0:T(8,128)(2,1)}, bf16[128,2048]{1,0:T(8,128)(2,1)}, u32[]{:S(2)}, u32[]{:S(2)}) collective-permute-start(bf16[128,2048]{1,0:T(8,128)(2,1)} %get-tuple-element.60), channel_id=1, source_target_pairs={{0,3},{1,0},{2,1},{3,2},{4,7},{5,4},{6,5},{7,6},{8,11},{9,8},{10,9... | collective-permute-start | bytes 1572872 | tf_op jit(solution)/shard_map/ppermute | solution.py:118
  80.8 1.5 collective-permute-done.11.refs_1_
  83.8 6.8 %shard_map.77 = (bf16[128,2048]{1,0:T(8,128)(2,1)}, bf16[128,2048]{1,0:T(8,128)(2,1)}) custom-call(bf16[128,2048]{1,0:T(8,128)(2,1)S(1)} %collective-permute-done.10.refs_0_, bf16[128,2048]{1,0:T(8,128)(2,1)S(1)} %collective-permute-done.11.refs_1_, bf16[2048,1792]{1,0:T(8,128)(2,1)S(1)} %get-tuple-element.56.refs_2_, ...), custom_call_target="tpu_custom_call" | custom-call | flops 5637144576 | bytes 2097152 | tf_op jit(solution)/shard_map/pallas_call | solution.py:289
  90.6 2.0 %collective-permute-start.13 = (bf16[128,2048]{1,0:T(8,128)(2,1)}, bf16[128,2048]{1,0:T(8,128)(2,1)}, u32[]{:S(2)}, u32[]{:S(2)}) collective-permute-start(bf16[128,2048]{1,0:T(8,128)(2,1)} %get-tuple-element.66), channel_id=1, source_target_pairs={{0,1},{1,2},{2,3},{3,0},{4,5},{5,6},{6,7},{7,4},{8,9},{9,10},{10,1... | collective-permute-start | bytes 1572872 | tf_op jit(solution)/shard_map/ppermute | solution.py:118
  92.6 10.2 %shard_map.80 = bf16[256,2048]{1,0:T(8,128)(2,1)} custom-call(bf16[256,2048]{1,0:T(8,128)(2,1)S(1)} %bitcast.16, bf16[1,2048,1792]{2,1,0:T(8,128)(2,1)} %refs_1_.3, bf16[1,2048,1792]{2,1,0:T(8,128)(2,1)} %refs_2_.5, bf16[1,1792,2048]{2,1,0:T(8,128)(2,1)} %refs_3_.5), custom_call_target="tpu_custom_call" | custom-call | flops 5637144576 | bytes 24117248 | tf_op jit(solution)/shard_map/pallas_call | solution.py:273
  102.8 7.5 %all-to-all-start.3 = ((bf16[32,8,2048]{2,1,0:T(8,128)(2,1)}), bf16[32,8,2048]{2,1,0:T(8,128)(2,1)S(1)}, u32[]{:S(2)}, u32[]{:S(2)}) async-start(bf16[32,8,2048]{2,1,0:T(8,128)(2,1)} %bitcast.18), calls=%async_computation.3 | async-start | bytes 2097152 | tf_op jit(solution)/shard_map/all_to_all | solution.py:124
  113.9 10.2 %shard_map.81 = bf16[256,2048]{1,0:T(8,128)(2,1)} custom-call(bf16[256,2048]{1,0:T(8,128)(2,1)S(1)} %bitcast.14, bf16[1,2048,1792]{2,1,0:T(8,128)(2,1)} %refs_1_.3, bf16[1,2048,1792]{2,1,0:T(8,128)(2,1)} %refs_2_.5, bf16[1,1792,2048]{2,1,0:T(8,128)(2,1)} %refs_3_.5), custom_call_target="tpu_custom_call" | custom-call | flops 5637144576 | bytes 24117248 | tf_op jit(solution)/shard_map/pallas_call | solution.py:273
  124.1 1.9 %collective-permute-done.14 = bf16[128,2048]{1,0:T(8,128)(2,1)S(1)} collective-permute-done((bf16[128,2048]{1,0:T(8,128)(2,1)S(1)}, bf16[128,2048]{1,0:T(8,128)(2,1)S(1)}, u32[]{:S(2)}, u32[]{:S(2)}) %collective-permute-start.14) | collective-permute-done | bytes 524320 | tf_op jit(solution)/shard_map/ppermute | solution.py:118
  126.0 2.1 %collective-permute-done.15 = bf16[128,2048]{1,0:T(8,128)(2,1)S(1)} collective-permute-done((bf16[128,2048]{1,0:T(8,128)(2,1)S(1)}, bf16[128,2048]{1,0:T(8,128)(2,1)S(1)}, u32[]{:S(2)}, u32[]{:S(2)}) %collective-permute-start.15) | collective-permute-done | bytes 524320 | tf_op jit(solution)/shard_map/ppermute | solution.py:118
  128.1 3.1 %fusion = bf16[32,8,2048]{2,1,0:T(8,128)(2,1)} fusion(bf16[256,2048]{1,0:T(8,128)(2,1)} %shard_map.81, bf16[128,2048]{1,0:T(8,128)(2,1)} %collective-permute-done.9, bf16[128,2048]{1,0:T(8,128)(2,1)} %collective-permute-done.8, bf16[128,2048]{1,0:T(8,128)(2,1)S(1)} %collective-permute-done.15, bf16[128,2048]{1,0:T(8,128)(2,1)S(1)} %collective-permute-done.14), kind=kLoop, calls=%fused_computation.1 | loop fusion | flops 6291456 | bytes 4194304 | tf_op jit(solution)/shard_map/reshape | solution.py:123
  131.2 7.4 %all-to-all-start.2 = ((bf16[32,8,2048]{2,1,0:T(8,128)(2,1)}), bf16[32,8,2048]{2,1,0:T(8,128)(2,1)S(1)}, u32[]{:S(2)}, u32[]{:S(2)}) async-start(bf16[32,8,2048]{2,1,0:T(8,128)(2,1)} %fusion), calls=%async_computation.2 | async-start | bytes 2097152 | tf_op jit(solution)/shard_map/all_to_all | solution.py:124
  138.6 2.5 %shard_map.82 = (bf16[128,2048]{1,0:T(8,128)(2,1)}, bf16[64,2048]{1,0:T(8,128)(2,1)}, bf16[64,2048]{1,0:T(8,128)(2,1)}, bf16[64,2048]{1,0:T(8,128)(2,1)}, bf16[6...) custom-call(bf16[512,256]{1,0:T(8,128)(2,1)S(1)} %copy-done.8, ...), custom_call_target="tpu_custom_call" | custom-call | flops 1073741824 | bytes 3145728 | tf_op jit(solution)/shard_map/pallas_call | solution.py:360
  141.4 1.7 %collective-permute-start.19 = (bf16[64,2048]{1,0:T(8,128)(2,1)}, bf16[64,2048]{1,0:T(8,128)(2,1)S(1)}, u32[]{:S(2)}, u32[]{:S(2)}) collective-permute-start(bf16[64,2048]{1,0:T(8,128)(2,1)} %get-tuple-element.86), channel_id=1, source_target_pairs={{0,1},{1,2},{2,3},{3,0},{4,5},{5,6},{6,7},{7,4},{8,9},{9,10},{10,1... | collective-permute-start | bytes 786440 | tf_op jit(solution)/shard_map/ppermute | solution.py:118
  143.1 3.2 %collective-permute-start.17 = (bf16[64,2048]{1,0:T(8,128)(2,1)}, bf16[64,2048]{1,0:T(8,128)(2,1)S(1)}, u32[]{:S(2)}, u32[]{:S(2)}) collective-permute-start(bf16[64,2048]{1,0:T(8,128)(2,1)} %get-tuple-element.82), channel_id=1, source_target_pairs={{0,3},{1,0},{2,1},{3,2},{4,7},{5,4},{6,5},{7,6},{8,11},{9,8},{10,9... | collective-permute-start | bytes 786440 | tf_op jit(solution)/shard_map/ppermute | solution.py:118
  146.4 4.1 %collective-permute-done.18.b = bf16[64,2048]{1,0:T(8,128)(2,1)S(1)} collective-permute-done((bf16[64,2048]{1,0:T(8,128)(2,1)}, bf16[64,2048]{1,0:T(8,128)(2,1)S(1)}, u32[]{:S(2)}, u32[]{:S(2)}) %collective-permute-start.18) | collective-permute-done | bytes 262176 | tf_op jit(solution)/shard_map/ppermute | solution.py:118
  154.1 2.0 %collective-permute-start.21 = (bf16[64,2048]{1,0:T(8,128)(2,1)S(1)}, bf16[64,2048]{1,0:T(8,128)(2,1)S(1)}, u32[]{:S(2)}, u32[]{:S(2)}) collective-permute-start(bf16[64,2048]{1,0:T(8,128)(2,1)S(1)} %get-tuple-element.88), channel_id=1, source_target_pairs={{0,1},{1,2},{2,3},{3,0},{4,5},{5,6},{6,7},{7,4},{8,9},{9,10},{10,1... | collective-permute-start | bytes 786440 | tf_op jit(solution)/shard_map/ppermute | solution.py:118
  156.9 4.1 %collective-permute-done.20.far_a = bf16[64,2048]{1,0:T(8,128)(2,1)S(1)} collective-permute-done((bf16[64,2048]{1,0:T(8,128)(2,1)S(1)}, bf16[64,2048]{1,0:T(8,128)(2,1)S(1)}, u32[]{:S(2)}, u32[]{:S(2)}) %collective-permute-start.20) | collective-permute-done | bytes 262176 | tf_op jit(solution)/shard_map/ppermute | solution.py:118
  (62 shorter events, 14.8 us)
Async XLA Ops:
  2.7 36.5 %copy-start.3 = (bf16[128,2048]{1,0:T(8,128)(2,1)}, bf16[128,2048]{1,0:T(8,128)(2,1)S(1)}, u32[]{:S(2)}) copy-start(bf16[128,2048]{1,0:T(8,128)(2,1)S(1)} %get-tuple-element.70.refs_0_) | copy-start | bytes 1572868
  2.7 35.5 %all-to-all-start = ((bf16[32,8,2048]{2,1,0:T(8,128)(2,1)}), bf16[32,8,2048]{2,1,0:T(8,128)(2,1)S(1)}, u32[]{:S(2)}, u32[]{:S(2)}) async-start(bf16[32,8,2048]{2,1,0:T(8,128)(2,1)} %bitcast.4), calls=%async_computation | async-start | bytes 2097152 | tf_op jit(solution)/shard_map/all_to_all | solution.py:124
  11.2 14.4 %collective-permute-start.1 = (bf16[128,2048]{1,0:T(8,128)(2,1)S(1)}, bf16[128,2048]{1,0:T(8,128)(2,1)S(1)}, u32[]{:S(2)}, u32[]{:S(2)}) collective-permute-start(bf16[128,2048]{1,0:T(8,128)(2,1)S(1)} %get-tuple-element.70.refs_0_), channel_id=1, source_target_pairs={{0,3},{1,0},{2,1},{3,2},{4,7},{5,4},{6,5},{7,6},{8,11},{9,8},{10,9... | collective-permute-start | bytes 1572872 | tf_op jit(solution)/shard_map/ppermute | solution.py:118
  14.0 15.4 %collective-permute-start = (bf16[128,2048]{1,0:T(8,128)(2,1)S(1)}, bf16[128,2048]{1,0:T(8,128)(2,1)S(1)}, u32[]{:S(2)}, u32[]{:S(2)}) collective-permute-start(bf16[128,2048]{1,0:T(8,128)(2,1)S(1)} %get-tuple-element.70.refs_0_), channel_id=1, source_target_pairs={{0,1},{1,2},{2,3},{3,0},{4,5},{5,6},{6,7},{7,4},{8,9},{9,10},{10,1... | collective-permute-start | bytes 1572872 | tf_op jit(solution)/shard_map/ppermute | solution.py:118
  25.6 17.9 %copy-start.10 = (bf16[128,2048]{1,0:T(8,128)(2,1)}, bf16[128,2048]{1,0:T(8,128)(2,1)S(1)}, u32[]{:S(2)}) copy-start(bf16[128,2048]{1,0:T(8,128)(2,1)S(1)} %collective-permute-done.1.refs_2_) | copy-start | bytes 1572868
  25.6 8.9 %collective-permute-start.3 = (bf16[64,2048]{1,0:T(8,128)(2,1)S(1)}, bf16[64,2048]{1,0:T(8,128)(2,1)S(1)}, u32[]{:S(2)}, u32[]{:S(2)}) collective-permute-start(bf16[64,2048]{1,0:T(8,128)(2,1)S(1)} %slice.17), channel_id=1, source_target_pairs={{0,3},{1,0},{2,1},{3,2},{4,7},{5,4},{6,5},{7,6},{8,11},{9,8},{10,9... | collective-permute-start | bytes 786440 | tf_op jit(solution)/shard_map/ppermute | solution.py:118
  29.4 14.1 %copy-start.11 = (bf16[128,2048]{1,0:T(8,128)(2,1)}, bf16[128,2048]{1,0:T(8,128)(2,1)S(1)}, u32[]{:S(2)}) copy-start(bf16[128,2048]{1,0:T(8,128)(2,1)S(1)} %collective-permute-done.refs_1_) | copy-start | bytes 1572868
  29.4 8.7 %collective-permute-start.2 = (bf16[64,2048]{1,0:T(8,128)(2,1)S(1)}, bf16[64,2048]{1,0:T(8,128)(2,1)}, u32[]{:S(2)}, u32[]{:S(2)}) collective-permute-start(bf16[64,2048]{1,0:T(8,128)(2,1)S(1)} %slice.16), channel_id=1, source_target_pairs={{0,1},{1,2},{2,3},{3,0},{4,5},{5,6},{6,7},{7,4},{8,9},{9,10},{10,1... | collective-permute-start | bytes 786440 | tf_op jit(solution)/shard_map/ppermute | solution.py:118
  34.5 9.0 %copy-start.12 = (bf16[64,2048]{1,0:T(8,128)(2,1)}, bf16[64,2048]{1,0:T(8,128)(2,1)S(1)}, u32[]{:S(2)}) copy-start(bf16[64,2048]{1,0:T(8,128)(2,1)S(1)} %collective-permute-done.3.refs_4_) | copy-start | bytes 786436
  39.2 18.0 %collective-permute-start.7 = (bf16[128,2048]{1,0:T(8,128)(2,1)}, bf16[128,2048]{1,0:T(8,128)(2,1)S(1)}, u32[]{:S(2)}, u32[]{:S(2)}) collective-permute-start(bf16[128,2048]{1,0:T(8,128)(2,1)} %get-tuple-element.89), channel_id=1, source_target_pairs={{0,3},{1,0},{2,1},{3,2},{4,7},{5,4},{6,5},{7,6},{8,11},{9,8},{10,9... | collective-permute-start | bytes 1572872 | tf_op jit(solution)/shard_map/ppermute | solution.py:118
  39.3 17.9 %collective-permute-start.6 = (bf16[128,2048]{1,0:T(8,128)(2,1)}, bf16[128,2048]{1,0:T(8,128)(2,1)S(1)}, u32[]{:S(2)}, u32[]{:S(2)}) collective-permute-start(bf16[128,2048]{1,0:T(8,128)(2,1)} %get-tuple-element.90), channel_id=1, source_target_pairs={{0,1},{1,2},{2,3},{3,0},{4,5},{5,6},{6,7},{7,4},{8,9},{9,10},{10,1... | collective-permute-start | bytes 1572872 | tf_op jit(solution)/shard_map/ppermute | solution.py:118
  43.6 23.8 %collective-permute-start.4 = (bf16[128,2048]{1,0:T(8,128)(2,1)}, bf16[128,2048]{1,0:T(8,128)(2,1)}, u32[]{:S(2)}, u32[]{:S(2)}) collective-permute-start(bf16[128,2048]{1,0:T(8,128)(2,1)} %get-tuple-element.89), channel_id=1, source_target_pairs={{0,1},{1,2},{2,3},{3,0},{4,5},{5,6},{6,7},{7,4},{8,9},{9,10},{10,1... | collective-permute-start | bytes 1572872 | tf_op jit(solution)/shard_map/ppermute | solution.py:118
  43.6 23.8 %collective-permute-start.5 = (bf16[128,2048]{1,0:T(8,128)(2,1)}, bf16[128,2048]{1,0:T(8,128)(2,1)}, u32[]{:S(2)}, u32[]{:S(2)}) collective-permute-start(bf16[128,2048]{1,0:T(8,128)(2,1)} %get-tuple-element.90), channel_id=1, source_target_pairs={{0,3},{1,0},{2,1},{3,2},{4,7},{5,4},{6,5},{7,6},{8,11},{9,8},{10,9... | collective-permute-start | bytes 1572872 | tf_op jit(solution)/shard_map/ppermute | solution.py:118
  50.1 42.5 %all-to-all-start.1 = ((bf16[32,8,2048]{2,1,0:T(8,128)(2,1)}), bf16[32,8,2048]{2,1,0:T(8,128)(2,1)S(1)}, u32[]{:S(2)}, u32[]{:S(2)}) async-start(bf16[32,8,2048]{2,1,0:T(8,128)(2,1)} %bitcast.19), calls=%async_computation.1 | async-start | bytes 2097152 | tf_op jit(solution)/shard_map/all_to_all | solution.py:124
  67.4 14.9 %collective-permute-start.11 = (bf16[128,2048]{1,0:T(8,128)(2,1)S(1)}, bf16[128,2048]{1,0:T(8,128)(2,1)S(1)}, u32[]{:S(2)}, u32[]{:S(2)}) collective-permute-start(bf16[128,2048]{1,0:T(8,128)(2,1)S(1)} %collective-permute-done.7.refs_1_), channel_id=1, source_target_pairs={{0,3},{1,0},{2,1},{3,2},{4,7},{5,4},{6,5},{7,6},{8,11},{9,8},{10,9... | collective-permute-start | bytes 1572872 | tf_op jit(solution)/shard_map/ppermute | solution.py:118
  67.6 16.2 %collective-permute-start.10 = (bf16[128,2048]{1,0:T(8,128)(2,1)S(1)}, bf16[128,2048]{1,0:T(8,128)(2,1)S(1)}, u32[]{:S(2)}, u32[]{:S(2)}) collective-permute-start(bf16[128,2048]{1,0:T(8,128)(2,1)S(1)} %collective-permute-done.6.refs_0_), channel_id=1, source_target_pairs={{0,1},{1,2},{2,3},{3,0},{4,5},{5,6},{6,7},{7,4},{8,9},{9,10},{10,1... | collective-permute-start | bytes 1572872 | tf_op jit(solution)/shard_map/ppermute | solution.py:118
  77.5 46.6 %collective-permute-start.8 = (bf16[128,2048]{1,0:T(8,128)(2,1)}, bf16[128,2048]{1,0:T(8,128)(2,1)}, u32[]{:S(2)}, u32[]{:S(2)}) collective-permute-start(bf16[128,2048]{1,0:T(8,128)(2,1)} %get-tuple-element.59), channel_id=1, source_target_pairs={{0,1},{1,2},{2,3},{3,0},{4,5},{5,6},{6,7},{7,4},{8,9},{9,10},{10,1... | collective-permute-start | bytes 1572872 | tf_op jit(solution)/shard_map/ppermute | solution.py:118
  77.5 46.6 %collective-permute-start.9 = (bf16[128,2048]{1,0:T(8,128)(2,1)}, bf16[128,2048]{1,0:T(8,128)(2,1)}, u32[]{:S(2)}, u32[]{:S(2)}) collective-permute-start(bf16[128,2048]{1,0:T(8,128)(2,1)} %get-tuple-element.60), channel_id=1, source_target_pairs={{0,3},{1,0},{2,1},{3,2},{4,7},{5,4},{6,5},{7,6},{8,11},{9,8},{10,9... | collective-permute-start | bytes 1572872 | tf_op jit(solution)/shard_map/ppermute | solution.py:118
  90.6 19.8 %collective-permute-start.12 = (bf16[128,2048]{1,0:T(8,128)(2,1)}, bf16[128,2048]{1,0:T(8,128)(2,1)}, u32[]{:S(2)}, u32[]{:S(2)}) collective-permute-start(bf16[128,2048]{1,0:T(8,128)(2,1)} %get-tuple-element.64), channel_id=1, source_target_pairs={{0,3},{1,0},{2,1},{3,2},{4,7},{5,4},{6,5},{7,6},{8,11},{9,8},{10,9... | collective-permute-start | bytes 1572872 | tf_op jit(solution)/shard_map/ppermute | solution.py:118
  90.6 19.8 %collective-permute-start.13 = (bf16[128,2048]{1,0:T(8,128)(2,1)}, bf16[128,2048]{1,0:T(8,128)(2,1)}, u32[]{:S(2)}, u32[]{:S(2)}) collective-permute-start(bf16[128,2048]{1,0:T(8,128)(2,1)} %get-tuple-element.66), channel_id=1, source_target_pairs={{0,1},{1,2},{2,3},{3,0},{4,5},{5,6},{6,7},{7,4},{8,9},{9,10},{10,1... | collective-permute-start | bytes 1572872 | tf_op jit(solution)/shard_map/ppermute | solution.py:118
  102.8 28.4 %all-to-all-start.3 = ((bf16[32,8,2048]{2,1,0:T(8,128)(2,1)}), bf16[32,8,2048]{2,1,0:T(8,128)(2,1)S(1)}, u32[]{:S(2)}, u32[]{:S(2)}) async-start(bf16[32,8,2048]{2,1,0:T(8,128)(2,1)} %bitcast.18), calls=%async_computation.3 | async-start | bytes 2097152 | tf_op jit(solution)/shard_map/all_to_all | solution.py:124
  111.8 14.2 %collective-permute-start.14 = (bf16[128,2048]{1,0:T(8,128)(2,1)S(1)}, bf16[128,2048]{1,0:T(8,128)(2,1)S(1)}, u32[]{:S(2)}, u32[]{:S(2)}) collective-permute-start(bf16[128,2048]{1,0:T(8,128)(2,1)S(1)} %get-tuple-element.67), channel_id=1, source_target_pairs={{0,3},{1,0},{2,1},{3,2},{4,7},{5,4},{6,5},{7,6},{8,11},{9,8},{10,9... | collective-permute-start | bytes 1572872 | tf_op jit(solution)/shard_map/ppermute | solution.py:118
  113.1 15.0 %collective-permute-start.15 = (bf16[128,2048]{1,0:T(8,128)(2,1)S(1)}, bf16[128,2048]{1,0:T(8,128)(2,1)S(1)}, u32[]{:S(2)}, u32[]{:S(2)}) collective-permute-start(bf16[128,2048]{1,0:T(8,128)(2,1)S(1)} %get-tuple-element.68), channel_id=1, source_target_pairs={{0,1},{1,2},{2,3},{3,0},{4,5},{5,6},{6,7},{7,4},{8,9},{9,10},{10,1... | collective-permute-start | bytes 1572872 | tf_op jit(solution)/shard_map/ppermute | solution.py:118
  131.2 31.0 %all-to-all-start.2 = ((bf16[32,8,2048]{2,1,0:T(8,128)(2,1)}), bf16[32,8,2048]{2,1,0:T(8,128)(2,1)S(1)}, u32[]{:S(2)}, u32[]{:S(2)}) async-start(bf16[32,8,2048]{2,1,0:T(8,128)(2,1)} %fusion), calls=%async_computation.2 | async-start | bytes 2097152 | tf_op jit(solution)/shard_map/all_to_all | solution.py:124
  138.6 23.6 %copy-start.6 = (bf16[128,256]{1,0:T(8,128)(2,1)S(1)}, bf16[128,256]{1,0:T(8,128)(2,1)}, u32[]{:S(2)}) copy-start(bf16[128,256]{1,0:T(8,128)(2,1)} %get-tuple-element.47.high) | copy-start | bytes 196612
  138.6 23.6 %copy-start.7 = (bf16[128,256]{1,0:T(8,128)(2,1)S(1)}, bf16[128,256]{1,0:T(8,128)(2,1)}, u32[]{:S(2)}) copy-start(bf16[128,256]{1,0:T(8,128)(2,1)} %get-tuple-element.48.low) | copy-start | bytes 196612
  141.1 9.4 %collective-permute-start.18 = (bf16[64,2048]{1,0:T(8,128)(2,1)}, bf16[64,2048]{1,0:T(8,128)(2,1)S(1)}, u32[]{:S(2)}, u32[]{:S(2)}) collective-permute-start(bf16[64,2048]{1,0:T(8,128)(2,1)} %get-tuple-element.84), channel_id=1, source_target_pairs={{0,3},{1,0},{2,1},{3,2},{4,7},{5,4},{6,5},{7,6},{8,11},{9,8},{10,9... | collective-permute-start | bytes 786440 | tf_op jit(solution)/shard_map/ppermute | solution.py:118
  141.4 10.6 %collective-permute-start.19 = (bf16[64,2048]{1,0:T(8,128)(2,1)}, bf16[64,2048]{1,0:T(8,128)(2,1)S(1)}, u32[]{:S(2)}, u32[]{:S(2)}) collective-permute-start(bf16[64,2048]{1,0:T(8,128)(2,1)} %get-tuple-element.86), channel_id=1, source_target_pairs={{0,1},{1,2},{2,3},{3,0},{4,5},{5,6},{6,7},{7,4},{8,9},{9,10},{10,1... | collective-permute-start | bytes 786440 | tf_op jit(solution)/shard_map/ppermute | solution.py:118
  143.1 13.8 %collective-permute-start.16 = (bf16[64,2048]{1,0:T(8,128)(2,1)}, bf16[64,2048]{1,0:T(8,128)(2,1)S(1)}, u32[]{:S(2)}, u32[]{:S(2)}) collective-permute-start(bf16[64,2048]{1,0:T(8,128)(2,1)} %get-tuple-element.81), channel_id=1, source_target_pairs={{0,1},{1,2},{2,3},{3,0},{4,5},{5,6},{6,7},{7,4},{8,9},{9,10},{10,1... | collective-permute-start | bytes 786440 | tf_op jit(solution)/shard_map/ppermute | solution.py:118
  143.1 13.8 %collective-permute-start.17 = (bf16[64,2048]{1,0:T(8,128)(2,1)}, bf16[64,2048]{1,0:T(8,128)(2,1)S(1)}, u32[]{:S(2)}, u32[]{:S(2)}) collective-permute-start(bf16[64,2048]{1,0:T(8,128)(2,1)} %get-tuple-element.82), channel_id=1, source_target_pairs={{0,3},{1,0},{2,1},{3,2},{4,7},{5,4},{6,5},{7,6},{8,11},{9,8},{10,9... | collective-permute-start | bytes 786440 | tf_op jit(solution)/shard_map/ppermute | solution.py:118
  154.0 7.0 %collective-permute-start.20 = (bf16[64,2048]{1,0:T(8,128)(2,1)S(1)}, bf16[64,2048]{1,0:T(8,128)(2,1)S(1)}, u32[]{:S(2)}, u32[]{:S(2)}) collective-permute-start(bf16[64,2048]{1,0:T(8,128)(2,1)S(1)} %get-tuple-element.87), channel_id=1, source_target_pairs={{0,3},{1,0},{2,1},{3,2},{4,7},{5,4},{6,5},{7,6},{8,11},{9,8},{10,9... | collective-permute-start | bytes 786440 | tf_op jit(solution)/shard_map/ppermute | solution.py:118
  154.1 8.2 %collective-permute-start.21 = (bf16[64,2048]{1,0:T(8,128)(2,1)S(1)}, bf16[64,2048]{1,0:T(8,128)(2,1)S(1)}, u32[]{:S(2)}, u32[]{:S(2)}) collective-permute-start(bf16[64,2048]{1,0:T(8,128)(2,1)S(1)} %get-tuple-element.88), channel_id=1, source_target_pairs={{0,1},{1,2},{2,3},{3,0},{4,5},{5,6},{6,7},{7,4},{8,9},{9,10},{10,1... | collective-permute-start | bytes 786440 | tf_op jit(solution)/shard_map/ppermute | solution.py:118
  (7 other events, 32.9 us)

commit v3 on v2

--- a/solution.py
+++ b/solution.py
@@ -146,7 +146,7 @@
         out_shape=[jax.ShapeDtypeStruct(v.shape, v.dtype) for v in (a, c)],
         compiler_params=pltpu.CompilerParams(vmem_limit_bytes=12 * MIB),
         cost_estimate=pl.CostEstimate(flops=2 * a.size, bytes_accessed=12 * a.size, transcendentals=0),
-    )(a, b, c, d)
+    )(*in_hbm(a, b, c, d))
 
 
 def place(target, blocks):
@@ -356,7 +356,7 @@
 
 def weigh_late(high, low, rows):
     n, d = rows.shape
-    sizes = [LANES] + [LANES // 2] * (2 * len(OFFSETS) - 2)
+    sizes = [LANES] * len(OFFSETS)
     return pl.pallas_call(
         weigh_kernel,
         in_specs=[VMEM_SPEC] * 3,
@@ -369,28 +369,25 @@
     )(high, low, rows)
 
 
-def finish_kernel(high, low, rows, own, near_a, near_b, far_a, far_b, out):
+def finish_kernel(high, low, rows, own, left, right, far, out):
     value = weighted_sum(high[...], low[...], rows[...])
-    value = value + own[...].astype(jnp.float32)
-    half = out.shape[0] // 2
-    top = near_a[...].astype(jnp.float32) + far_a[...].astype(jnp.float32)
-    bottom = near_b[...].astype(jnp.float32) + far_b[...].astype(jnp.float32)
-    out[:half, :] = (value[:half] + top).astype(out.dtype)
-    out[half:, :] = (value[half:] + bottom).astype(out.dtype)
-
-
-def finish(high, low, rows, own, pieces):
+    for part in (own, left, right, far):
+        value = value + part[...].astype(jnp.float32)
+    out[...] = value.astype(out.dtype)
+
+
+def finish(high, low, rows, parts):
     n, d = rows.shape
     return pl.pallas_call(
         finish_kernel,
-        in_specs=[VMEM_SPEC] * 8,
+        in_specs=[VMEM_SPEC] * (3 + len(parts)),
         out_specs=VMEM_SPEC,
         out_shape=jax.ShapeDtypeStruct((LANES, d), jnp.bfloat16),
         compiler_params=pltpu.CompilerParams(vmem_limit_bytes=16 * MIB),
         cost_estimate=pl.CostEstimate(
             flops=4 * n * LANES * d, bytes_accessed=2 * d * (n + 4 * LANES), transcendentals=0
         ),
-    )(high, low, rows, own, *pieces)
+    )(high, low, rows, *parts)
 
 
 def send_near(to_left, to_right):
@@ -451,11 +448,10 @@
 
     late_back, _ = lax.optimization_barrier((late_back, own_part))
     sums = weigh_late(late_high, late_low, late_back)
-    token_own, left_top, left_bottom, right_top, right_bottom, far_top, far_bottom = sums
-    token_via = send_far(far_top, far_bottom)
-    token_near = send_near(left_bottom, right_top)
-    token_on = send_on(left_top, right_bottom, *token_via)
-    return finish(high, low, back, token_own, token_near + token_on)
+    token_own, left, right, far = sums
+    token_far = shift(far, 2)
+    token_left, token_right = shift(left, -1), shift(right, 1)
+    return finish(high, low, back, (token_own, token_left, token_right, token_far))
 
 
 def solution(mesh):

time: 165 us -> 171 us (1.036)
  waiting for transfers between devices: 39.1 us -> 52.3 us
  starting transfers between devices: 59.2 us -> 53.8 us
  local copies, waits for them, and re-layouts: 4.08 us -> 2.17 us
    ppermute x22 -> x19, waiting for transfers between devices: 39.1 us -> 52.3 us  [shift(): lax.ppermute(value, 'tp', [(i, (i + by) % size) for i in range(size)])]
    ppermute x22 -> x19, starting transfers between devices: 28.8 us -> 23.5 us  [shift(): lax.ppermute(value, 'tp', [(i, (i + by) % size) for i in range(size)])]
    unnamed x26 -> x20, local copies, waits for them, and re-layouts: 2.98 us -> 1.07 us
  transfers between devices with their start and end apart: 26 -> 23, of which waited for: 12 -> 9; matrix products, arithmetic and copies ran while one was open for 2% -> 2% of each run, Pallas kernels for 33% -> 32%
where the time goes in v3:
time: 171 us; the launch traced here: 170 us
  Pallas kernels  58.3 us (34%)
  starting transfers between devices  53.8 us (31%)
  waiting for transfers between devices  52.3 us (31%)
  other arithmetic  3.05 us (2%)
  local copies, waits for them, and re-layouts  2.17 us (1%)
    ppermute x19, waiting for transfers between devices, shift(): lax.ppermute(value, 'tp', [(i, (i + by) % size) for i in range(size)])  52.3 us
    pallas_call x3, Pallas kernels, expert_streamed(): pl.pallas_call(functools.partial(stream_kernel, len(blocks), len(sizes)),...  30.5 us
    all_to_all x4, starting transfers between devices, exchange(): return lax.all_to_all(tiles, EP, 0, 0, tiled=True).reshape(rows.shape)  30.3 us
    ppermute x19, starting transfers between devices, shift(): lax.ppermute(value, 'tp', [(i, (i + by) % size) for i in range(size)])  23.5 us
    pallas_call x2, Pallas kernels, expert_kept(): pl.pallas_call(functools.partial(kept_kernel, len(blocks)), in_specs=[VME...  13.8 us
  transfers between devices with their start and end apart: 23, of which 9 were waited for; matrix products, arithmetic and copies ran while one was open for 2% of the time, Pallas kernels for 32%

profile of v3, /device:TPU:0, one launch (start us, length us, event | category | flops | bytes accessed | tf_op | source)
XLA Modules:
  0.0 169.9 jit_solution(14301269589333846824)
XLA Ops:
  0.0 2.7 %shard_map.74 = (bf16[128,2048]{1,0:T(8,128)(2,1)S(1)}, bf16[256,2048]{1,0:T(8,128)(2,1)}) custom-call(s32[1]{0:T(128)} %bitcast.me, bf16[128,2048]{1,0:T(8,128)(2,1)} %tokens.1, f32[1,2048]{1,0:T(1,128)} %bitcast.20, s32[2,512]{1,0:T(2,128)} %bitcast.21), custom_call_target="tpu_custom_call" | custom-call | flops 134217728 | bytes 2097152 | tf_op jit(solution)/shard_map/pallas_call | solution.py:97
  2.7 8.4 %all-to-all-start = ((bf16[32,8,2048]{2,1,0:T(8,128)(2,1)}), bf16[32,8,2048]{2,1,0:T(8,128)(2,1)S(1)}, u32[]{:S(2)}, u32[]{:S(2)}) async-start(bf16[32,8,2048]{2,1,0:T(8,128)(2,1)} %bitcast.4), calls=%async_computation | async-start | bytes 2097152 | tf_op jit(solution)/shard_map/all_to_all | solution.py:124
  11.2 2.8 %collective-permute-start.1 = (bf16[128,2048]{1,0:T(8,128)(2,1)S(1)}, bf16[128,2048]{1,0:T(8,128)(2,1)S(1)}, u32[]{:S(2)}, u32[]{:S(2)}) collective-permute-start(bf16[128,2048]{1,0:T(8,128)(2,1)S(1)} %get-tuple-element.65.refs_0_), channel_id=1, source_target_pairs={{0,3},{1,0},{2,1},{3,2},{4,7},{5,4},{6,5},{7,6},{8,11},{9,8},{10,9... | collective-permute-start | bytes 1572872 | tf_op jit(solution)/shard_map/ppermute | solution.py:118
  14.0 11.6 %collective-permute-done.1.refs_2_ = bf16[128,2048]{1,0:T(8,128)(2,1)S(1)} collective-permute-done((bf16[128,2048]{1,0:T(8,128)(2,1)S(1)}, bf16[128,2048]{1,0:T(8,128)(2,1)S(1)}, u32[]{:S(2)}, u32[]{:S(2)}) %collective-permute-start.1) | collective-permute-done | bytes 524320 | tf_op jit(solution)/shard_map/ppermute | solution.py:118
  25.6 3.8 %collective-permute-start.3 = (bf16[64,2048]{1,0:T(8,128)(2,1)S(1)}, bf16[64,2048]{1,0:T(8,128)(2,1)S(1)}, u32[]{:S(2)}, u32[]{:S(2)}) collective-permute-start(bf16[64,2048]{1,0:T(8,128)(2,1)S(1)} %slice.17), channel_id=1, source_target_pairs={{0,3},{1,0},{2,1},{3,2},{4,7},{5,4},{6,5},{7,6},{8,11},{9,8},{10,9... | collective-permute-start | bytes 786440 | tf_op jit(solution)/shard_map/ppermute | solution.py:118
  29.5 5.0 %collective-permute-done.3.refs_4_ = bf16[64,2048]{1,0:T(8,128)(2,1)S(1)} collective-permute-done((bf16[64,2048]{1,0:T(8,128)(2,1)S(1)}, bf16[64,2048]{1,0:T(8,128)(2,1)S(1)}, u32[]{:S(2)}, u32[]{:S(2)}) %collective-permute-start.3) | collective-permute-done | bytes 262176 | tf_op jit(solution)/shard_map/ppermute | solution.py:118
  34.6 3.5 %collective-permute-done.2.refs_3_ = bf16[64,2048]{1,0:T(8,128)(2,1)S(1)} collective-permute-done((bf16[64,2048]{1,0:T(8,128)(2,1)S(1)}, bf16[64,2048]{1,0:T(8,128)(2,1)S(1)}, u32[]{:S(2)}, u32[]{:S(2)}) %collective-permute-start.2) | collective-permute-done | bytes 262176 | tf_op jit(solution)/shard_map/ppermute | solution.py:118
  39.4 1.8 %collective-permute-start.6 = (bf16[128,2048]{1,0:T(8,128)(2,1)}, bf16[128,2048]{1,0:T(8,128)(2,1)S(1)}, u32[]{:S(2)}, u32[]{:S(2)}) collective-permute-start(bf16[128,2048]{1,0:T(8,128)(2,1)} %get-tuple-element.80), channel_id=1, source_target_pairs={{0,1},{1,2},{2,3},{3,0},{4,5},{5,6},{6,7},{7,4},{8,9},{9,10},{10,1... | collective-permute-start | bytes 1572872 | tf_op jit(solution)/shard_map/ppermute | solution.py:118
  41.2 2.3 %shard_map.73 = (bf16[256,512]{1,0:T(8,128)(2,1)}, bf16[512,256]{1,0:T(8,128)(2,1)}, bf16[512,256]{1,0:T(8,128)(2,1)}, bf16[128,256]{1,0:T(8,128)(2,1)}, bf16[128,256]{1,0:T(8,128)(2,1)}) custom-call(s32[1]{0:T(128)} %bitcast.me, s32[2,512]{1,0:T(2,128)} %bitcast.22, f32[2,512]{1,0:T(2,128)} %bitcast.23), custom_call_target="tpu_custom_call" | custom-call | flops 4000000000 | bytes 786432 | tf_op jit(solution)/shard_map/pallas_call | solution.py:318
  43.5 3.2 %collective-permute-start.5 = (bf16[128,2048]{1,0:T(8,128)(2,1)}, bf16[128,2048]{1,0:T(8,128)(2,1)}, u32[]{:S(2)}, u32[]{:S(2)}) collective-permute-start(bf16[128,2048]{1,0:T(8,128)(2,1)} %get-tuple-element.80), channel_id=1, source_target_pairs={{0,3},{1,0},{2,1},{3,2},{4,7},{5,4},{6,5},{7,6},{8,11},{9,8},{10,9... | collective-permute-start | bytes 1572872 | tf_op jit(solution)/shard_map/ppermute | solution.py:118
  46.8 3.3 %shard_map.79 = bf16[256,2048]{1,0:T(8,128)(2,1)} custom-call(bf16[256,512]{1,0:T(8,128)(2,1)} %get-tuple-element.64.chosen, bf16[128,2048]{1,0:T(8,128)(2,1)} %copy-done, bf16[128,2048]{1,0:T(8,128)(2,1)} %copy-done.7, bf16[128,2048]{1,0:T(8,128)(2,1)} %copy-done.6, bf16[64,2048]{1,0:T(8,128)(2,1)} %copy-done.9, bf16[64,2048]{1,0:T(8,128)(2,1)} %copy-done.8), custom_call_target="tpu_custom_call" | custom-call | flops 536870912 | bytes 3145728 | tf_op jit(solution)/shard_map/pallas_call | solution.py:340
  50.0 7.1 %all-to-all-start.1 = ((bf16[32,8,2048]{2,1,0:T(8,128)(2,1)}), bf16[32,8,2048]{2,1,0:T(8,128)(2,1)S(1)}, u32[]{:S(2)}, u32[]{:S(2)}) async-start(bf16[32,8,2048]{2,1,0:T(8,128)(2,1)} %bitcast.19), calls=%async_computation.1 | async-start | bytes 2097152 | tf_op jit(solution)/shard_map/all_to_all | solution.py:124
  57.1 10.2 %shard_map.75 = (bf16[128,2048]{1,0:T(8,128)(2,1)}, bf16[128,2048]{1,0:T(8,128)(2,1)}, bf16[2048,1792]{1,0:T(8,128)(2,1)S(1)}, bf16[2048,1792]{1,0:T(8,128)(2,1)S(1)}, bf16[1792,2048]{1,0:T(8,128)(2,1)S(1)}) custom-call(bf16[128,2048]{1,0:T(8,128)(2,1)S(1)} %collective-permute-done.6.refs_0_, bf16[128,2048]{1,0:T(8,128)(2,1)S(1)} %collective-permute-done.7.refs_1_, ...), custom_call_target="tpu_custom_call" | custom-call | flops 5637144576 | bytes 24117248 | tf_op jit(solution)/shard_map/pallas_call | solution.py:273
  67.7 1.7 %collective-permute-start.10 = (bf16[128,2048]{1,0:T(8,128)(2,1)S(1)}, bf16[128,2048]{1,0:T(8,128)(2,1)S(1)}, u32[]{:S(2)}, u32[]{:S(2)}) collective-permute-start(bf16[128,2048]{1,0:T(8,128)(2,1)S(1)} %collective-permute-done.6.refs_0_), channel_id=1, source_target_pairs={{0,1},{1,2},{2,3},{3,0},{4,5},{5,6},{6,7},{7,4},{8,9},{9,10},{10,1... | collective-permute-start | bytes 1572872 | tf_op jit(solution)/shard_map/ppermute | solution.py:118
  69.4 8.0 %shard_map.76 = (bf16[128,2048]{1,0:T(8,128)(2,1)}, bf16[128,2048]{1,0:T(8,128)(2,1)}) custom-call(bf16[128,2048]{1,0:T(8,128)(2,1)} %collective-permute-done.4.refs_0_, bf16[128,2048]{1,0:T(8,128)(2,1)} %collective-permute-done.5.refs_1_, bf16[2048,1792]{1,0:T(8,128)(2,1)S(1)} %get-tuple-element.51.refs_2_, ...), custom_call_target="tpu_custom_call" | custom-call | flops 5637144576 | bytes 2097152 | tf_op jit(solution)/shard_map/pallas_call | solution.py:289
  77.4 3.2 %collective-permute-start.9 = (bf16[128,2048]{1,0:T(8,128)(2,1)}, bf16[128,2048]{1,0:T(8,128)(2,1)}, u32[]{:S(2)}, u32[]{:S(2)}) collective-permute-start(bf16[128,2048]{1,0:T(8,128)(2,1)} %get-tuple-element.55), channel_id=1, source_target_pairs={{0,3},{1,0},{2,1},{3,2},{4,7},{5,4},{6,5},{7,6},{8,11},{9,8},{10,9... | collective-permute-start | bytes 1572872 | tf_op jit(solution)/shard_map/ppermute | solution.py:118
  80.6 1.5 collective-permute-done.11.refs_1_
  83.7 5.9 %shard_map.77 = (bf16[128,2048]{1,0:T(8,128)(2,1)S(1)}, bf16[128,2048]{1,0:T(8,128)(2,1)S(1)}) custom-call(bf16[128,2048]{1,0:T(8,128)(2,1)S(1)} %collective-permute-done.10.refs_0_, bf16[128,2048]{1,0:T(8,128)(2,1)S(1)} %collective-permute-done.11.refs_1_, bf16[2048,1792]{1,0:T(8,128)(2,1)S(1)} %get-tuple-element.51.refs_2_, ...), custom_call_target="tpu_custom_call" | custom-call | flops 5637144576 | bytes 2097152 | tf_op jit(solution)/shard_map/pallas_call | solution.py:289
  89.6 2.0 %collective-permute-start.13 = (bf16[128,2048]{1,0:T(8,128)(2,1)S(1)}, bf16[128,2048]{1,0:T(8,128)(2,1)}, u32[]{:S(2)}, u32[]{:S(2)}) collective-permute-start(bf16[128,2048]{1,0:T(8,128)(2,1)S(1)} %get-tuple-element.61), channel_id=1, source_target_pairs={{0,1},{1,2},{2,3},{3,0},{4,5},{5,6},{6,7},{7,4},{8,9},{9,10},{10,1... | collective-permute-start | bytes 1572872 | tf_op jit(solution)/shard_map/ppermute | solution.py:118
  91.6 10.2 %shard_map.80 = bf16[256,2048]{1,0:T(8,128)(2,1)} custom-call(bf16[256,2048]{1,0:T(8,128)(2,1)S(1)} %bitcast.15, bf16[1,2048,1792]{2,1,0:T(8,128)(2,1)} %refs_1_.3, bf16[1,2048,1792]{2,1,0:T(8,128)(2,1)} %refs_2_.5, bf16[1,1792,2048]{2,1,0:T(8,128)(2,1)} %refs_3_.5), custom_call_target="tpu_custom_call" | custom-call | flops 5637144576 | bytes 24117248 | tf_op jit(solution)/shard_map/pallas_call | solution.py:273
  101.8 7.4 %all-to-all-start.3 = ((bf16[32,8,2048]{2,1,0:T(8,128)(2,1)}), bf16[32,8,2048]{2,1,0:T(8,128)(2,1)S(1)}, u32[]{:S(2)}, u32[]{:S(2)}) async-start(bf16[32,8,2048]{2,1,0:T(8,128)(2,1)} %bitcast.18), calls=%async_computation.3 | async-start | bytes 2097152 | tf_op jit(solution)/shard_map/all_to_all | solution.py:124
  109.3 1.8 %shard_map.78 = (bf16[128,2048]{1,0:T(8,128)(2,1)S(1)}, bf16[128,2048]{1,0:T(8,128)(2,1)S(1)}) custom-call(bf16[128,2048]{1,0:T(8,128)(2,1)} %get-tuple-element.56.a, bf16[128,2048]{1,0:T(8,128)(2,1)} %collective-permute-done.12.b, bf16[128,2048]{1,0:T(8,128)(2,1)} %get-tuple-element.60.c, bf16[128,2048]{1,0:T(8,128)(2,1)} %collective-permute-done.13.d), custom_call_target="tpu_custom_call" | custom-call | flops 524288 | bytes 3145728 | tf_op jit(solution)/shard_map/pallas_call | solution.py:142
  111.0 1.6 collective-permute-start.14
  113.1 10.2 %shard_map.81 = bf16[256,2048]{1,0:T(8,128)(2,1)} custom-call(bf16[256,2048]{1,0:T(8,128)(2,1)S(1)} %bitcast.14, bf16[1,2048,1792]{2,1,0:T(8,128)(2,1)} %refs_1_.3, bf16[1,2048,1792]{2,1,0:T(8,128)(2,1)} %refs_2_.5, bf16[1,1792,2048]{2,1,0:T(8,128)(2,1)} %refs_3_.5), custom_call_target="tpu_custom_call" | custom-call | flops 5637144576 | bytes 24117248 | tf_op jit(solution)/shard_map/pallas_call | solution.py:273
  123.3 1.9 %collective-permute-done.14 = bf16[128,2048]{1,0:T(8,128)(2,1)S(1)} collective-permute-done((bf16[128,2048]{1,0:T(8,128)(2,1)S(1)}, bf16[128,2048]{1,0:T(8,128)(2,1)S(1)}, u32[]{:S(2)}, u32[]{:S(2)}) %collective-permute-start.14) | collective-permute-done | bytes 524320 | tf_op jit(solution)/shard_map/ppermute | solution.py:118
  125.2 2.4 %collective-permute-done.15 = bf16[128,2048]{1,0:T(8,128)(2,1)S(1)} collective-permute-done((bf16[128,2048]{1,0:T(8,128)(2,1)S(1)}, bf16[128,2048]{1,0:T(8,128)(2,1)S(1)}, u32[]{:S(2)}, u32[]{:S(2)}) %collective-permute-start.15) | collective-permute-done | bytes 524320 | tf_op jit(solution)/shard_map/ppermute | solution.py:118
  127.7 3.1 %fusion = bf16[32,8,2048]{2,1,0:T(8,128)(2,1)} fusion(bf16[256,2048]{1,0:T(8,128)(2,1)} %shard_map.81, bf16[128,2048]{1,0:T(8,128)(2,1)} %collective-permute-done.9, bf16[128,2048]{1,0:T(8,128)(2,1)} %collective-permute-done.8, bf16[128,2048]{1,0:T(8,128)(2,1)S(1)} %collective-permute-done.15, bf16[128,2048]{1,0:T(8,128)(2,1)S(1)} %collective-permute-done.14), kind=kLoop, calls=%fused_computation.1 | loop fusion | flops 6291456 | bytes 4194304 | tf_op jit(solution)/shard_map/reshape | solution.py:123
  130.7 7.4 %all-to-all-start.2 = ((bf16[32,8,2048]{2,1,0:T(8,128)(2,1)}), bf16[32,8,2048]{2,1,0:T(8,128)(2,1)S(1)}, u32[]{:S(2)}, u32[]{:S(2)}) async-start(bf16[32,8,2048]{2,1,0:T(8,128)(2,1)} %fusion), calls=%async_computation.2 | async-start | bytes 2097152 | tf_op jit(solution)/shard_map/all_to_all | solution.py:124
  138.1 2.5 %shard_map.82 = (bf16[128,2048]{1,0:T(8,128)(2,1)}, bf16[128,2048]{1,0:T(8,128)(2,1)}, bf16[128,2048]{1,0:T(8,128)(2,1)}, bf16[128,2048]{1,0:T(8,128)(2,1)}) custom-call(bf16[512,256]{1,0:T(8,128)(2,1)S(1)} %copy-done.4, bf16[512,256]{1,0:T(8,128)(2,1)S(1)} %copy-done.5, bf16[256,2048]{1,0:T(8,128)(2,1)S(1)} %bitcast.17), custom_call_target="tpu_custom_call" | custom-call | flops 1073741824 | bytes 3145728 | tf_op jit(solution)/shard_map/pallas_call | solution.py:360
  140.9 1.7 %collective-permute-start.17 = (bf16[128,2048]{1,0:T(8,128)(2,1)}, bf16[128,2048]{1,0:T(8,128)(2,1)S(1)}, u32[]{:S(2)}, u32[]{:S(2)}) collective-permute-start(bf16[128,2048]{1,0:T(8,128)(2,1)} %get-tuple-element.77), channel_id=1, source_target_pairs={{0,1},{1,2},{2,3},{3,0},{4,5},{5,6},{6,7},{7,4},{8,9},{9,10},{10,1... | collective-permute-start | bytes 1572872 | tf_op jit(solution)/shard_map/ppermute | solution.py:118
  142.7 13.0 %collective-permute-done.16.left = bf16[128,2048]{1,0:T(8,128)(2,1)S(1)} collective-permute-done((bf16[128,2048]{1,0:T(8,128)(2,1)}, bf16[128,2048]{1,0:T(8,128)(2,1)S(1)}, u32[]{:S(2)}, u32[]{:S(2)}) %collective-permute-start.16) | collective-permute-done | bytes 524320 | tf_op jit(solution)/shard_map/ppermute | solution.py:118
  155.6 11.8 %collective-permute-done.17.right = bf16[128,2048]{1,0:T(8,128)(2,1)S(1)} collective-permute-done((bf16[128,2048]{1,0:T(8,128)(2,1)}, bf16[128,2048]{1,0:T(8,128)(2,1)S(1)}, u32[]{:S(2)}, u32[]{:S(2)}) %collective-permute-start.17) | collective-permute-done | bytes 524320 | tf_op jit(solution)/shard_map/ppermute | solution.py:118
  (49 shorter events, 6.8 us)
Async XLA Ops:
  2.7 36.4 %copy-start = (bf16[128,2048]{1,0:T(8,128)(2,1)}, bf16[128,2048]{1,0:T(8,128)(2,1)S(1)}, u32[]{:S(2)}) copy-start(bf16[128,2048]{1,0:T(8,128)(2,1)S(1)} %get-tuple-element.65.refs_0_) | copy-start | bytes 1572868
  2.7 35.3 %all-to-all-start = ((bf16[32,8,2048]{2,1,0:T(8,128)(2,1)}), bf16[32,8,2048]{2,1,0:T(8,128)(2,1)S(1)}, u32[]{:S(2)}, u32[]{:S(2)}) async-start(bf16[32,8,2048]{2,1,0:T(8,128)(2,1)} %bitcast.4), calls=%async_computation | async-start | bytes 2097152 | tf_op jit(solution)/shard_map/all_to_all | solution.py:124
  11.2 14.4 %collective-permute-start.1 = (bf16[128,2048]{1,0:T(8,128)(2,1)S(1)}, bf16[128,2048]{1,0:T(8,128)(2,1)S(1)}, u32[]{:S(2)}, u32[]{:S(2)}) collective-permute-start(bf16[128,2048]{1,0:T(8,128)(2,1)S(1)} %get-tuple-element.65.refs_0_), channel_id=1, source_target_pairs={{0,3},{1,0},{2,1},{3,2},{4,7},{5,4},{6,5},{7,6},{8,11},{9,8},{10,9... | collective-permute-start | bytes 1572872 | tf_op jit(solution)/shard_map/ppermute | solution.py:118
  14.0 15.4 %collective-permute-start = (bf16[128,2048]{1,0:T(8,128)(2,1)S(1)}, bf16[128,2048]{1,0:T(8,128)(2,1)S(1)}, u32[]{:S(2)}, u32[]{:S(2)}) collective-permute-start(bf16[128,2048]{1,0:T(8,128)(2,1)S(1)} %get-tuple-element.65.refs_0_), channel_id=1, source_target_pairs={{0,1},{1,2},{2,3},{3,0},{4,5},{5,6},{6,7},{7,4},{8,9},{9,10},{10,1... | collective-permute-start | bytes 1572872 | tf_op jit(solution)/shard_map/ppermute | solution.py:118
  25.6 17.8 %copy-start.6 = (bf16[128,2048]{1,0:T(8,128)(2,1)}, bf16[128,2048]{1,0:T(8,128)(2,1)S(1)}, u32[]{:S(2)}) copy-start(bf16[128,2048]{1,0:T(8,128)(2,1)S(1)} %collective-permute-done.1.refs_2_) | copy-start | bytes 1572868
  25.6 8.9 %collective-permute-start.3 = (bf16[64,2048]{1,0:T(8,128)(2,1)S(1)}, bf16[64,2048]{1,0:T(8,128)(2,1)S(1)}, u32[]{:S(2)}, u32[]{:S(2)}) collective-permute-start(bf16[64,2048]{1,0:T(8,128)(2,1)S(1)} %slice.17), channel_id=1, source_target_pairs={{0,3},{1,0},{2,1},{3,2},{4,7},{5,4},{6,5},{7,6},{8,11},{9,8},{10,9... | collective-permute-start | bytes 786440 | tf_op jit(solution)/shard_map/ppermute | solution.py:118
  29.4 5.1 %copy-start.7 = (bf16[128,2048]{1,0:T(8,128)(2,1)}, bf16[128,2048]{1,0:T(8,128)(2,1)S(1)}, u32[]{:S(2)}) copy-start(bf16[128,2048]{1,0:T(8,128)(2,1)S(1)} %collective-permute-done.refs_1_) | copy-start | bytes 1572868
  29.4 8.6 %collective-permute-start.2 = (bf16[64,2048]{1,0:T(8,128)(2,1)S(1)}, bf16[64,2048]{1,0:T(8,128)(2,1)S(1)}, u32[]{:S(2)}, u32[]{:S(2)}) collective-permute-start(bf16[64,2048]{1,0:T(8,128)(2,1)S(1)} %slice.16), channel_id=1, source_target_pairs={{0,1},{1,2},{2,3},{3,0},{4,5},{5,6},{6,7},{7,4},{8,9},{9,10},{10,1... | collective-permute-start | bytes 786440 | tf_op jit(solution)/shard_map/ppermute | solution.py:118
  34.5 8.9 %copy-start.8 = (bf16[64,2048]{1,0:T(8,128)(2,1)}, bf16[64,2048]{1,0:T(8,128)(2,1)S(1)}, u32[]{:S(2)}) copy-start(bf16[64,2048]{1,0:T(8,128)(2,1)S(1)} %collective-permute-done.3.refs_4_) | copy-start | bytes 786436
  38.1 1.1 copy-start.9
  39.1 18.0 %collective-permute-start.7 = (bf16[128,2048]{1,0:T(8,128)(2,1)}, bf16[128,2048]{1,0:T(8,128)(2,1)S(1)}, u32[]{:S(2)}, u32[]{:S(2)}) collective-permute-start(bf16[128,2048]{1,0:T(8,128)(2,1)} %get-tuple-element.79), channel_id=1, source_target_pairs={{0,3},{1,0},{2,1},{3,2},{4,7},{5,4},{6,5},{7,6},{8,11},{9,8},{10,9... | collective-permute-start | bytes 1572872 | tf_op jit(solution)/shard_map/ppermute | solution.py:118
  39.4 17.7 %collective-permute-start.6 = (bf16[128,2048]{1,0:T(8,128)(2,1)}, bf16[128,2048]{1,0:T(8,128)(2,1)S(1)}, u32[]{:S(2)}, u32[]{:S(2)}) collective-permute-start(bf16[128,2048]{1,0:T(8,128)(2,1)} %get-tuple-element.80), channel_id=1, source_target_pairs={{0,1},{1,2},{2,3},{3,0},{4,5},{5,6},{6,7},{7,4},{8,9},{9,10},{10,1... | collective-permute-start | bytes 1572872 | tf_op jit(solution)/shard_map/ppermute | solution.py:118
  43.5 23.9 %collective-permute-start.4 = (bf16[128,2048]{1,0:T(8,128)(2,1)}, bf16[128,2048]{1,0:T(8,128)(2,1)}, u32[]{:S(2)}, u32[]{:S(2)}) collective-permute-start(bf16[128,2048]{1,0:T(8,128)(2,1)} %get-tuple-element.79), channel_id=1, source_target_pairs={{0,1},{1,2},{2,3},{3,0},{4,5},{5,6},{6,7},{7,4},{8,9},{9,10},{10,1... | collective-permute-start | bytes 1572872 | tf_op jit(solution)/shard_map/ppermute | solution.py:118
  43.5 23.8 %collective-permute-start.5 = (bf16[128,2048]{1,0:T(8,128)(2,1)}, bf16[128,2048]{1,0:T(8,128)(2,1)}, u32[]{:S(2)}, u32[]{:S(2)}) collective-permute-start(bf16[128,2048]{1,0:T(8,128)(2,1)} %get-tuple-element.80), channel_id=1, source_target_pairs={{0,3},{1,0},{2,1},{3,2},{4,7},{5,4},{6,5},{7,6},{8,11},{9,8},{10,9... | collective-permute-start | bytes 1572872 | tf_op jit(solution)/shard_map/ppermute | solution.py:118
  50.0 41.6 %all-to-all-start.1 = ((bf16[32,8,2048]{2,1,0:T(8,128)(2,1)}), bf16[32,8,2048]{2,1,0:T(8,128)(2,1)S(1)}, u32[]{:S(2)}, u32[]{:S(2)}) async-start(bf16[32,8,2048]{2,1,0:T(8,128)(2,1)} %bitcast.19), calls=%async_computation.1 | async-start | bytes 2097152 | tf_op jit(solution)/shard_map/all_to_all | solution.py:124
  67.3 14.9 %collective-permute-start.11 = (bf16[128,2048]{1,0:T(8,128)(2,1)S(1)}, bf16[128,2048]{1,0:T(8,128)(2,1)S(1)}, u32[]{:S(2)}, u32[]{:S(2)}) collective-permute-start(bf16[128,2048]{1,0:T(8,128)(2,1)S(1)} %collective-permute-done.7.refs_1_), channel_id=1, source_target_pairs={{0,3},{1,0},{2,1},{3,2},{4,7},{5,4},{6,5},{7,6},{8,11},{9,8},{10,9... | collective-permute-start | bytes 1572872 | tf_op jit(solution)/shard_map/ppermute | solution.py:118
  67.7 16.0 %collective-permute-start.10 = (bf16[128,2048]{1,0:T(8,128)(2,1)S(1)}, bf16[128,2048]{1,0:T(8,128)(2,1)S(1)}, u32[]{:S(2)}, u32[]{:S(2)}) collective-permute-start(bf16[128,2048]{1,0:T(8,128)(2,1)S(1)} %collective-permute-done.6.refs_0_), channel_id=1, source_target_pairs={{0,1},{1,2},{2,3},{3,0},{4,5},{5,6},{6,7},{7,4},{8,9},{9,10},{10,1... | collective-permute-start | bytes 1572872 | tf_op jit(solution)/shard_map/ppermute | solution.py:118
  77.4 45.9 %collective-permute-start.8 = (bf16[128,2048]{1,0:T(8,128)(2,1)}, bf16[128,2048]{1,0:T(8,128)(2,1)}, u32[]{:S(2)}, u32[]{:S(2)}) collective-permute-start(bf16[128,2048]{1,0:T(8,128)(2,1)} %get-tuple-element.54), channel_id=1, source_target_pairs={{0,1},{1,2},{2,3},{3,0},{4,5},{5,6},{6,7},{7,4},{8,9},{9,10},{10,1... | collective-permute-start | bytes 1572872 | tf_op jit(solution)/shard_map/ppermute | solution.py:118
  77.4 45.9 %collective-permute-start.9 = (bf16[128,2048]{1,0:T(8,128)(2,1)}, bf16[128,2048]{1,0:T(8,128)(2,1)}, u32[]{:S(2)}, u32[]{:S(2)}) collective-permute-start(bf16[128,2048]{1,0:T(8,128)(2,1)} %get-tuple-element.55), channel_id=1, source_target_pairs={{0,3},{1,0},{2,1},{3,2},{4,7},{5,4},{6,5},{7,6},{8,11},{9,8},{10,9... | collective-permute-start | bytes 1572872 | tf_op jit(solution)/shard_map/ppermute | solution.py:118
  89.5 19.7 %collective-permute-start.12 = (bf16[128,2048]{1,0:T(8,128)(2,1)S(1)}, bf16[128,2048]{1,0:T(8,128)(2,1)}, u32[]{:S(2)}, u32[]{:S(2)}) collective-permute-start(bf16[128,2048]{1,0:T(8,128)(2,1)S(1)} %get-tuple-element.59), channel_id=1, source_target_pairs={{0,3},{1,0},{2,1},{3,2},{4,7},{5,4},{6,5},{7,6},{8,11},{9,8},{10,9... | collective-permute-start | bytes 1572872 | tf_op jit(solution)/shard_map/ppermute | solution.py:118
  89.6 19.6 %collective-permute-start.13 = (bf16[128,2048]{1,0:T(8,128)(2,1)S(1)}, bf16[128,2048]{1,0:T(8,128)(2,1)}, u32[]{:S(2)}, u32[]{:S(2)}) collective-permute-start(bf16[128,2048]{1,0:T(8,128)(2,1)S(1)} %get-tuple-element.61), channel_id=1, source_target_pairs={{0,1},{1,2},{2,3},{3,0},{4,5},{5,6},{6,7},{7,4},{8,9},{9,10},{10,1... | collective-permute-start | bytes 1572872 | tf_op jit(solution)/shard_map/ppermute | solution.py:118
  101.8 28.9 %all-to-all-start.3 = ((bf16[32,8,2048]{2,1,0:T(8,128)(2,1)}), bf16[32,8,2048]{2,1,0:T(8,128)(2,1)S(1)}, u32[]{:S(2)}, u32[]{:S(2)}) async-start(bf16[32,8,2048]{2,1,0:T(8,128)(2,1)} %bitcast.18), calls=%async_computation.3 | async-start | bytes 2097152 | tf_op jit(solution)/shard_map/all_to_all | solution.py:124
  111.0 14.2 %collective-permute-start.14 = (bf16[128,2048]{1,0:T(8,128)(2,1)S(1)}, bf16[128,2048]{1,0:T(8,128)(2,1)S(1)}, u32[]{:S(2)}, u32[]{:S(2)}) collective-permute-start(bf16[128,2048]{1,0:T(8,128)(2,1)S(1)} %get-tuple-element.62), channel_id=1, source_target_pairs={{0,3},{1,0},{2,1},{3,2},{4,7},{5,4},{6,5},{7,6},{8,11},{9,8},{10,9... | collective-permute-start | bytes 1572872 | tf_op jit(solution)/shard_map/ppermute | solution.py:118
  112.6 15.0 %collective-permute-start.15 = (bf16[128,2048]{1,0:T(8,128)(2,1)S(1)}, bf16[128,2048]{1,0:T(8,128)(2,1)S(1)}, u32[]{:S(2)}, u32[]{:S(2)}) collective-permute-start(bf16[128,2048]{1,0:T(8,128)(2,1)S(1)} %get-tuple-element.63), channel_id=1, source_target_pairs={{0,1},{1,2},{2,3},{3,0},{4,5},{5,6},{6,7},{7,4},{8,9},{9,10},{10,1... | collective-permute-start | bytes 1572872 | tf_op jit(solution)/shard_map/ppermute | solution.py:118
  130.7 7.4 %copy-start.4 = (bf16[512,256]{1,0:T(8,128)(2,1)S(1)}, bf16[512,256]{1,0:T(8,128)(2,1)}, u32[]{:S(2)}) copy-start(bf16[512,256]{1,0:T(8,128)(2,1)} %get-tuple-element.72.high) | copy-start | bytes 786436
  130.7 7.4 %copy-start.5 = (bf16[512,256]{1,0:T(8,128)(2,1)S(1)}, bf16[512,256]{1,0:T(8,128)(2,1)}, u32[]{:S(2)}) copy-start(bf16[512,256]{1,0:T(8,128)(2,1)} %get-tuple-element.73.low) | copy-start | bytes 786436
  130.7 36.7 %all-to-all-start.2 = ((bf16[32,8,2048]{2,1,0:T(8,128)(2,1)}), bf16[32,8,2048]{2,1,0:T(8,128)(2,1)S(1)}, u32[]{:S(2)}, u32[]{:S(2)}) async-start(bf16[32,8,2048]{2,1,0:T(8,128)(2,1)} %fusion), calls=%async_computation.2 | async-start | bytes 2097152 | tf_op jit(solution)/shard_map/all_to_all | solution.py:124
  138.1 29.3 %copy-start.2 = (bf16[128,256]{1,0:T(8,128)(2,1)S(1)}, bf16[128,256]{1,0:T(8,128)(2,1)}, u32[]{:S(2)}) copy-start(bf16[128,256]{1,0:T(8,128)(2,1)} %get-tuple-element.42.high) | copy-start | bytes 196612
  138.1 29.3 %copy-start.3 = (bf16[128,256]{1,0:T(8,128)(2,1)S(1)}, bf16[128,256]{1,0:T(8,128)(2,1)}, u32[]{:S(2)}) copy-start(bf16[128,256]{1,0:T(8,128)(2,1)} %get-tuple-element.43.low) | copy-start | bytes 196612
  140.6 15.0 %collective-permute-start.16 = (bf16[128,2048]{1,0:T(8,128)(2,1)}, bf16[128,2048]{1,0:T(8,128)(2,1)S(1)}, u32[]{:S(2)}, u32[]{:S(2)}) collective-permute-start(bf16[128,2048]{1,0:T(8,128)(2,1)} %get-tuple-element.76), channel_id=1, source_target_pairs={{0,3},{1,0},{2,1},{3,2},{4,7},{5,4},{6,5},{7,6},{8,11},{9,8},{10,9... | collective-permute-start | bytes 1572872 | tf_op jit(solution)/shard_map/ppermute | solution.py:118
  140.9 26.5 %collective-permute-start.17 = (bf16[128,2048]{1,0:T(8,128)(2,1)}, bf16[128,2048]{1,0:T(8,128)(2,1)S(1)}, u32[]{:S(2)}, u32[]{:S(2)}) collective-permute-start(bf16[128,2048]{1,0:T(8,128)(2,1)} %get-tuple-element.77), channel_id=1, source_target_pairs={{0,1},{1,2},{2,3},{3,0},{4,5},{5,6},{6,7},{7,4},{8,9},{9,10},{10,1... | collective-permute-start | bytes 1572872 | tf_op jit(solution)/shard_map/ppermute | solution.py:118
  142.7 24.7 %collective-permute-start.18 = (bf16[128,2048]{1,0:T(8,128)(2,1)}, bf16[128,2048]{1,0:T(8,128)(2,1)S(1)}, u32[]{:S(2)}, u32[]{:S(2)}) collective-permute-start(bf16[128,2048]{1,0:T(8,128)(2,1)} %get-tuple-element.78), channel_id=1, source_target_pairs={{0,2},{1,3},{2,0},{3,1},{4,6},{5,7},{6,4},{7,5},{8,10},{9,11},{10,... | collective-permute-start | bytes 1572872 | tf_op jit(solution)/shard_map/ppermute | solution.py:118
  (1 other events, 1.0 us)
